TPU v7x, 32 devices: a whole 2x2x4 slice. The times are simulated.
32 devices in a mesh: sp: 4 (over z), fs: 4 (over y, x), tp: 2 (over core).
Axes of the slice: x: 2, y: 2, z: 4, core: 2. Of those that a mesh axis runs over, the one named last changes fastest.
Arguments:
- hidden_in: bfloat16 [4, 1024, 2048], P('fs', 'sp', 'tp'), may hold values from -6 to 6
- sb_query_w: bfloat16 [2048, 1024], P('fs', 'tp'), may hold values from -0.21875 to 0.21875
- sb_key_w: bfloat16 [2048, 1024], P('fs', 'tp'), may hold values from -0.21875 to 0.21875
- sb_value_w: bfloat16 [2048, 1024], P('fs', 'tp'), may hold values from -0.125 to 0.125
- sb_offset: float32 [16], P('tp'), may hold values from -16 to -6
- delta_query_w: bfloat16 [2048, 1024], P('fs', 'tp'), may hold values from -0.125 to 0.125
- delta_key_w: bfloat16 [2048, 1024], P('fs', 'tp'), may hold values from -0.125 to 0.125
- delta_value_w: bfloat16 [2048, 1024], P('fs', 'tp'), may hold values from -0.125 to 0.125
- decay_w: bfloat16 [2048, 8], P(None, 'tp'), may hold values from -0.125 to 0.125
- write_w: bfloat16 [2048, 8], P(None, 'tp'), may hold values from -0.125 to 0.125
- write_bias: float32 [8], P('tp'), may hold values from -7 to 1.5
- decay_log_scale: float32 [8], P('tp'), may hold values from -14 to -3
- decay_shift: float32 [4, 8, 1024], P('fs', 'tp', 'sp'), may hold values from -3 to 0
- head_gain: float32 [128], replicated, may hold values from 0.1 to 1.9
- sb_out_w: bfloat16 [1024, 2048], P('tp'), may hold values from -0.125 to 0.125
- delta_out_w: bfloat16 [1024, 2048], P('tp'), may hold values from -0.125 to 0.125
Outputs:
- mixed_out: bfloat16 [4, 1024, 2048], P('fs', ('sp', 'tp'))
All inputs are finite; a program needn't handle non-finite values.
Results may differ from a plain program's by a relative error of at most 0.015.
Values may be sent and summed in bfloat16 or wider, within the bound.
A program may use at most 128 MiB of HBM per device.

v0:
```python
import jax
import jax.numpy as jnp
from jax import lax
from jax.experimental import pallas as pl
from jax.experimental.pallas import tpu as pltpu
from jax.sharding import PartitionSpec as P

MESH = pl.DeviceIdType.MESH
ALL_VMEM = 67043328

SB_DIM = 64
GDN_DIM = 128
BLOCK = 64


EXACT_MATMUL = lax.Precision.HIGHEST
NORM_EPS = 1e-06


def carried_in(value, axis, combine, identity):
    devices, index = (lax.axis_size(axis), lax.axis_index(axis))
    everything = jax.tree.map(
        lambda part, kind: lax.all_gather(part.astype(kind), axis),
        value,
        (jnp.bfloat16, jnp.bfloat16),
    )
    start = jax.tree.map(
        lambda part, zero: jnp.broadcast_to(jnp.asarray(zero, part.dtype), part.shape),
        value,
        identity,
    )

    def lap(k, before):
        reached = k < index
        new = combine(
            before, jax.tree.map(lambda part, own: part[k].astype(own.dtype), everything, value)
        )
        return jax.tree.map(lambda a, b: jnp.where(reached, a, b), new, before)

    return lax.fori_loop(0, devices, lap, start)


def unit_lower_inverse(strict_part):
    order_size = strict_part.shape[-1]
    powered = strict_part
    inverse = jnp.eye(order_size, dtype=strict_part.dtype) - strict_part
    for repeat_number in range(max(1, (order_size - 1).bit_length()) - 1):
        powered = jnp.einsum("...ij,...jk->...ik", powered, powered, precision=EXACT_MATMUL)
        inverse = inverse + jnp.einsum(
            "...ij,...jk->...ik", inverse, powered, precision=EXACT_MATMUL
        )
    return inverse


def to_blocks(row_data, block_span):
    blocks_count = row_data.shape[0] // block_span
    shaped = row_data.reshape((blocks_count, block_span) + row_data.shape[1:])
    return jnp.swapaxes(shaped, 1, 2)


def from_blocks(blocked):
    swapped = jnp.swapaxes(blocked, 1, 2)
    return swapped.reshape((-1,) + swapped.shape[2:])


def unit_rows(vectors):
    return vectors * lax.rsqrt(jnp.sum(vectors * vectors, axis=-1, keepdims=True) + NORM_EPS)


def delta_inputs(
    query_proj,
    key_proj,
    value_proj,
    decay_pre,
    write_pre,
    write_bias,
    decay_log_scale,
    shift_rows,
    head_count,
    head_size,
):
    query_act = jax.nn.silu(query_proj.astype(jnp.float32)).reshape(-1, head_count, head_size)
    key_act = jax.nn.silu(key_proj.astype(jnp.float32)).reshape(-1, head_count, head_size)
    value_rows = jax.nn.silu(value_proj.astype(jnp.float32)).reshape(-1, head_count, head_size)
    queries = unit_rows(query_act) * head_size ** (-0.5)
    key_rows = unit_rows(key_act)
    log_decay = -jnp.exp(decay_log_scale) * jax.nn.softplus(decay_pre) + shift_rows
    strength = jax.nn.sigmoid(write_pre + write_bias)
    return (queries, key_rows, value_rows, log_decay, strength)


def delta_prepare(queries, key_rows, value_rows, log_decay, strength):
    block_span = queries.shape[2]
    cumulative = jnp.cumsum(log_decay, axis=-1)
    row_place = lax.broadcasted_iota(jnp.int32, (block_span, block_span), 0)
    col_place = lax.broadcasted_iota(jnp.int32, (block_span, block_span), 1)
    inclusive = col_place <= row_place
    strictly = col_place < row_place
    spread = cumulative[..., :, None] - cumulative[..., None, :]
    decay_table = jnp.where(inclusive, jnp.exp(jnp.where(inclusive, spread, 0.0)), 0.0)
    keys_beta = key_rows * strength[..., None]
    lower_part = jnp.where(
        strictly,
        jnp.einsum("nhik,nhjk->nhij", keys_beta, key_rows, precision=EXACT_MATMUL) * decay_table,
        0.0,
    )
    inverse = unit_lower_inverse(lower_part)
    growth = jnp.exp(cumulative)
    state_updates = jnp.einsum(
        "nhij,nhjv->nhiv", inverse, value_rows * strength[..., None], precision=EXACT_MATMUL
    )
    erase_term = jnp.einsum(
        "nhij,nhjk->nhik", inverse, keys_beta * growth[..., None], precision=EXACT_MATMUL
    )
    inside_block = (
        jnp.einsum("nhik,nhjk->nhij", queries, key_rows, precision=EXACT_MATMUL) * decay_table
    )
    boosted_query = queries * growth[..., None]
    damped_keys = key_rows * jnp.exp(cumulative[..., -1:] - cumulative)[..., None]
    decay_per_block = jnp.exp(cumulative[..., -1])
    return (state_updates, erase_term, inside_block, boosted_query, damped_keys, decay_per_block)


def delta_step(memory_state, inputs):
    state_updates, erase_term, inside_block, boosted_query, damped_keys, decay_per_block = inputs
    fixed_values = state_updates - jnp.einsum(
        "mzq,mqc->mzc", erase_term, memory_state, precision=EXACT_MATMUL
    )
    produced_rows = jnp.einsum(
        "mzq,mqc->mzc", boosted_query, memory_state, precision=EXACT_MATMUL
    ) + jnp.einsum("efq,eqn->efn", inside_block, fixed_values, precision=EXACT_MATMUL)
    memory_state = memory_state * decay_per_block[:, None, None] + jnp.einsum(
        "wam,waz->wmz", damped_keys, fixed_values, precision=EXACT_MATMUL
    )
    return (memory_state, produced_rows)


def transition_step(carried, inputs):
    memory_state, transfer = carried
    state_updates, erase_term, inside_block, boosted_query, damped_keys, decay_per_block = inputs
    fixed_values = state_updates - jnp.einsum(
        "mzq,mqc->mzc", erase_term, memory_state, precision=EXACT_MATMUL
    )
    coupling = jnp.einsum("hik,hil->hkl", damped_keys, erase_term, precision=EXACT_MATMUL)
    memory_state = memory_state * decay_per_block[:, None, None] + jnp.einsum(
        "wam,waz->wmz", damped_keys, fixed_values, precision=EXACT_MATMUL
    )
    transfer = transfer * decay_per_block[:, None, None] - jnp.einsum(
        "hkl,hlm->hkm", coupling, transfer, precision=EXACT_MATMUL
    )
    return ((memory_state, transfer), None)


def compose(prior_blocks, following_blocks):
    joined_map = jnp.einsum(
        "hkl,hlm->hkm", following_blocks[0], prior_blocks[0], precision=EXACT_MATMUL
    )
    joined_state = (
        jnp.einsum("djo,dog->djg", following_blocks[0], prior_blocks[1], precision=EXACT_MATMUL)
        + following_blocks[1]
    )
    return (joined_map, joined_state)


def stick_block(queries, key_rows, value_rows, query_place, key_place, offsets):
    scale_factor = queries.shape[-1] ** (-0.5)
    scores = (
        jnp.einsum("qhd,khd->hqk", queries, key_rows, preferred_element_type=jnp.float32)
        * scale_factor
        + offsets[:, None, None]
    )
    visible = key_place[None, :] < query_place[:, None]
    skipped = jnp.where(visible, jax.nn.log_sigmoid(-scores), 0.0)
    beyond = lax.cumsum(skipped, axis=2, reverse=True) - skipped
    weights = jnp.where(visible, jnp.exp(jax.nn.log_sigmoid(scores) + beyond), 0.0).astype(
        jnp.bfloat16
    )
    partial_value = jnp.einsum(
        "hqk,khd->qhd", weights, value_rows, preferred_element_type=jnp.float32
    )
    return (partial_value, jnp.sum(skipped, axis=2).T)


def stick_combine(partials, totals):
    beyond = jnp.cumsum(totals[::-1], axis=0)[::-1] - totals
    return jnp.sum(partials * jnp.exp(beyond)[..., None], axis=0)


def on_device_split(
    hidden_in,
    sb_query_w,
    sb_key_w,
    sb_value_w,
    sb_offset,
    delta_query_w,
    delta_key_w,
    delta_value_w,
    decay_w,
    write_w,
    write_bias,
    decay_log_scale,
    decay_shift,
    head_gain,
    sb_out_w,
    delta_out_w,
):
    token_rows = hidden_in.shape[1]
    local_in = hidden_in.reshape(token_rows, hidden_in.shape[2])
    gathered = (
        lax.all_gather(sb_query_w, "fs", axis=0, tiled=True),
        lax.all_gather(sb_key_w, "fs", axis=0, tiled=True),
        lax.all_gather(sb_value_w, "fs", axis=0, tiled=True),
        lax.all_gather(delta_query_w, "fs", axis=0, tiled=True),
        lax.all_gather(delta_key_w, "fs", axis=0, tiled=True),
        lax.all_gather(delta_value_w, "fs", axis=0, tiled=True),
    )
    in_weights = tuple(gathered) + (decay_w, write_w)
    portion = lax.all_gather(local_in, "tp", axis=1, tiled=True)
    projected = tuple(
        (jnp.dot(portion, weight, preferred_element_type=jnp.float32) for weight in in_weights)
    )
    sb_heads = sb_offset.shape[0]
    delta_heads = decay_log_scale.shape[0]
    sb_query = projected[0].astype(jnp.bfloat16).reshape(token_rows, sb_heads, SB_DIM)
    sb_keys = projected[1].astype(jnp.bfloat16)
    sb_values = projected[2].astype(jnp.bfloat16)
    shift_rows = decay_shift.reshape(delta_heads, token_rows).T
    queries, key_rows, value_rows, log_decay, strength = delta_inputs(
        projected[3].astype(jnp.bfloat16),
        projected[4].astype(jnp.bfloat16),
        projected[5].astype(jnp.bfloat16),
        projected[6],
        projected[7],
        write_bias,
        decay_log_scale,
        shift_rows,
        delta_heads,
        GDN_DIM,
    )
    prepared = delta_prepare(
        to_blocks(queries, BLOCK),
        to_blocks(key_rows, BLOCK),
        to_blocks(value_rows, BLOCK),
        to_blocks(log_decay, BLOCK),
        to_blocks(strength, BLOCK),
    )
    identity_map = jnp.broadcast_to(
        jnp.eye(GDN_DIM, dtype=jnp.float32), (delta_heads, GDN_DIM, GDN_DIM)
    )
    empty_state = jnp.zeros((delta_heads, GDN_DIM, GDN_DIM), jnp.float32)
    (local_end, local_map), unused_out = lax.scan(
        transition_step, (empty_state, identity_map), prepared
    )
    own_first = lax.axis_index("sp") * token_rows
    query_place = own_first + lax.iota(jnp.int32, token_rows)
    sp_count = lax.axis_size("sp")
    slot_out = jnp.zeros((sp_count, token_rows, sb_heads, SB_DIM), jnp.float32)
    slot_total = jnp.zeros((sp_count, token_rows, sb_heads), jnp.float32)

    def absorb(slot_arrays, address_portion, value_part, shard_first):

        def active(current):
            partial_value, totals = stick_block(
                sb_query,
                address_portion.reshape(token_rows, sb_heads, SB_DIM),
                value_part.reshape(token_rows, sb_heads, SB_DIM),
                query_place,
                shard_first + lax.iota(jnp.int32, token_rows),
                sb_offset,
            )
            slot_index = shard_first // token_rows
            return (
                lax.dynamic_update_index_in_dim(current[0], partial_value, slot_index, 0),
                lax.dynamic_update_index_in_dim(current[1], totals, slot_index, 0),
            )

        def inactive(current):
            return current

        usable = jnp.logical_and(shard_first >= 0, shard_first <= own_first)
        return lax.cond(usable, active, inactive, slot_arrays)

    key_block = lax.all_gather(sb_keys, "sp", axis=0, tiled=True)
    value_block = lax.all_gather(sb_values, "sp", axis=0, tiled=True)

    def per_shard(shard_number, current):
        row_begin = shard_number * token_rows
        return absorb(
            current,
            lax.dynamic_slice_in_dim(key_block, row_begin, token_rows, 0),
            lax.dynamic_slice_in_dim(value_block, row_begin, token_rows, 0),
            row_begin,
        )

    slot_arrays = lax.fori_loop(
        0, key_block.shape[0] // token_rows, per_shard, (slot_out, slot_total)
    )
    unused_map, incoming = carried_in(
        (local_map, local_end), "sp", compose, (identity_map, empty_state)
    )
    sb_mixed = (
        stick_combine(slot_arrays[0], slot_arrays[1])
        .astype(jnp.bfloat16)
        .reshape(token_rows, sb_heads * SB_DIM)
    )
    unused_end, produced_rows = lax.scan(delta_step, incoming, prepared)
    produced_rows = from_blocks(produced_rows)
    normed = (
        produced_rows
        * lax.rsqrt(jnp.mean(produced_rows * produced_rows, axis=-1, keepdims=True) + NORM_EPS)
        * head_gain
    )
    delta_mixed = normed.astype(jnp.bfloat16).reshape(token_rows, delta_heads * GDN_DIM)
    result = lax.psum_scatter(
        (
            jnp.dot(sb_mixed, sb_out_w, preferred_element_type=jnp.float32)
            + jnp.dot(delta_mixed, delta_out_w, preferred_element_type=jnp.float32)
        ).astype(jnp.bfloat16),
        "tp",
        scatter_dimension=0,
        tiled=True,
    ).astype(jnp.float32)
    return result.astype(jnp.bfloat16).reshape(1, result.shape[0], result.shape[1])


def remote(src, dst, send, recv, axis, index):
    return pltpu.make_async_remote_copy(
        src_ref=src, dst_ref=dst, send_sem=send, recv_sem=recv,
        device_id={axis: index}, device_id_type=MESH,
    )


def greet(axes):
    barrier = pltpu.get_barrier_semaphore()
    count = 0
    for axis in axes:
        size, me = lax.axis_size(axis), lax.axis_index(axis)
        for k in range(1, size):
            pl.semaphore_signal(
                barrier, inc=1, device_id={axis: lax.rem(me + k, size)}, device_id_type=MESH
            )
            count += 1
    pl.semaphore_wait(barrier, count)


def project_kernel(
    x_ref, w0, w1, w2, w3, w4, w5, decay_w_ref, write_w_ref, shift_ref,
    p_ref, decay_pre_ref, write_pre_ref, shifts_ref,
    xs, ws, decay_w, write_w,
    x_send, x_recv, f_send, f_recv, w_send, w_recv, s_send, s_recv, l_sem, lw_sem,
):
    weights = (w0, w1, w2, w3, w4, w5)
    sp, tp = lax.axis_size("sp"), lax.axis_size("tp")
    z, f, t = lax.axis_index("sp"), lax.axis_index("fs"), lax.axis_index("tp")
    rows, half = x_ref.shape
    depth = w0.shape[0]
    cols = ws.shape[1] // len(weights)
    parts = x_send.shape[2]
    slot = pl.ds(pl.multiple_of(t * half, half), half)
    local = [
        pltpu.make_async_copy(x_ref, xs.at[z, :, slot], l_sem.at[0]),
        pltpu.make_async_copy(shift_ref, shifts_ref.at[z], l_sem.at[1]),
        pltpu.make_async_copy(decay_w_ref, decay_w, l_sem.at[2]),
        pltpu.make_async_copy(write_w_ref, write_w, l_sem.at[3]),
    ]

    def w_src(i):
        return weights[i].at[:, pl.ds(pl.multiple_of(z * cols, cols), cols)]

    def w_at(i, who):
        return ws.at[pl.ds(pl.multiple_of(who * depth, depth), depth), pl.ds(i * cols, cols)]

    local += [
        pltpu.make_async_copy(w_src(i), w_at(i, f), lw_sem.at[i]) for i in range(len(weights))
    ]
    for c in local:
        c.start()
    greet(("sp", "fs", "tp"))

    near = (f + 1 - 2 * (f % 2), f + 2 - 4 * (f // 2))
    count = len(weights)
    orders = (tuple(range(count)), tuple(range(count // 2, count)) + tuple(range(count // 2)))

    def x_copy(way, step, part):
        block = z - (step - 1) if way == 0 else z + (step - 1)
        piece = pl.ds(part * (rows // parts), rows // parts)
        there = xs.at[block, piece, slot]
        return remote(
            x_ref.at[piece, :] if step == 1 else there, there,
            x_send.at[way, step, part], x_recv.at[way, step, part],
            "sp", z + 1 if way == 0 else z - 1,
        )

    def onward(way):
        return z + 1 < sp if way == 0 else z > 0

    def comes(way, step):
        return z >= step if way == 0 else z + step < sp

    def sends(way, step):
        return jnp.logical_and(onward(way), comes(way, step - 1))

    def forward(way, step, part):
        block = z - step if way == 0 else z + step
        piece = pl.ds(part * (rows // parts), rows // parts)
        there = xs.at[block, piece, slot]
        return remote(
            x_ref.at[piece, :] if step == 0 else there, there,
            f_send.at[way, step, part], f_recv.at[way, step, part], "tp", lax.rem(t + 1, tp),
        )

    for part in range(parts):
        for way in range(2):
            @pl.when(onward(way))
            def _():
                x_copy(way, 1, part).start()

    w_copies = {}
    for order_at in range(count):
        for side in range(2):
            i = orders[side][order_at]
            c = remote(
                w_src(i), w_at(i, f), w_send.at[side, i], w_recv.at[side, i], "fs", near[side]
            )
            c.start()
            w_copies[side, i] = c
    s_copies = []
    for k in range(1, sp):
        c = remote(
            shift_ref, shifts_ref.at[z], s_send.at[k], s_recv.at[k], "sp", lax.rem(z + k, sp)
        )
        c.start()
        s_copies.append(c)
    for part in range(parts):
        forward(0, 0, part).start()

    relays = []

    def relay(position):
        for side in range(2):
            i = orders[side][position]
            w_copies[side, i].wait_recv()
            there = w_at(i, near[side])
            c = remote(
                there, there, w_send.at[2 + side, i], w_recv.at[2 + side, i],
                "fs", near[1 - side],
            )
            c.start()
            relays.append(c)

    for step in range(1, sp):
        relay(step - 1)
        for part in range(parts):
            for way in range(2):
                @pl.when(comes(way, step))
                def _():
                    x_copy(way, step, part).wait_recv()
                    forward(way, step, part).start()
                    if step + 1 < sp:
                        @pl.when(onward(way))
                        def _():
                            x_copy(way, step + 1, part).start()
    for position in range(sp - 1, count // 2):
        relay(position)
    for c in local:
        c.wait()
    for side in range(2):
        for position in range(count // 2, count):
            w_copies[side, orders[side][position]].wait_recv()
    for c in relays:
        c.wait_recv()

    def project(block):
        at = pl.ds(pl.multiple_of(block * rows, rows), rows)
        for i in range(0, count, 2):
            out = jnp.dot(
                xs[block], ws[:, i * cols : (i + 2) * cols], preferred_element_type=jnp.float32
            ).astype(jnp.bfloat16)
            p_ref[i, at, :] = out[:, :cols]
            p_ref[i + 1, at, :] = out[:, cols:]
        decay_pre_ref[at, :] = lax.dot_general(
            xs[block], decay_w[...], (((1,), (1,)), ((), ())),
            preferred_element_type=jnp.float32,
        )
        write_pre_ref[at, :] = lax.dot_general(
            xs[block], write_w[...], (((1,), (1,)), ((), ())),
            preferred_element_type=jnp.float32,
        )

    for part in range(parts):
        forward(0, 0, part).wait_recv()
    project(z)
    for step in range(1, sp):
        for way in range(2):
            @pl.when(comes(way, step))
            def _():
                for part in range(parts):
                    forward(way, step, part).wait_recv()
                project(z - step if way == 0 else z + step)
    for c in s_copies:
        c.wait_recv()
    for c in list(w_copies.values()) + relays + s_copies:
        c.wait_send()
    for part in range(parts):
        forward(0, 0, part).wait_send()
        for step in range(1, sp):
            for way in range(2):
                @pl.when(sends(way, step))
                def _():
                    x_copy(way, step, part).wait_send()

                @pl.when(comes(way, step))
                def _():
                    forward(way, step, part).wait_send()


def stick_kernel(offset_ref, p_ref, out_ref):
    rows = out_ref.shape[0]
    i = pl.program_id(0)
    lane = lax.broadcasted_iota(jnp.int32, (rows, out_ref.shape[1]), 1)
    heads = offset_ref.shape[0]
    size = out_ref.shape[1] // heads
    below = lax.broadcasted_iota(jnp.int32, (rows, rows), 0)
    across = lax.broadcasted_iota(jnp.int32, (rows, rows), 1)
    after = jnp.where(below >= across, 1.0, 0.0).astype(jnp.bfloat16)
    scale = size ** (-0.5)
    q = p_ref[0, pl.ds(pl.multiple_of(i * rows, rows), rows), :]
    queries = [
        jnp.where(lane // size == h, q, jnp.zeros_like(q)) for h in range(heads)
    ]

    def block(j, carry, masked):
        at = pl.ds(pl.multiple_of(j * rows, rows), rows)
        keys, values = p_ref[1, at, :], p_ref[2, at, :]
        new = []
        for h in range(heads):
            acc, later = carry[h]
            score = (
                lax.dot_general(
                    queries[h], keys, (((1,), (1,)), ((), ())),
                    preferred_element_type=jnp.float32,
                ) * scale + offset_ref[h]
            )
            skip = -(jnp.maximum(score, 0.0) + jnp.log(1.0 + jnp.exp(-jnp.abs(score))))
            if masked:
                skip = jnp.where(across < below, skip, 0.0)
            high = skip.astype(jnp.bfloat16)
            low = (skip - high.astype(jnp.float32)).astype(jnp.bfloat16)
            total = jnp.dot(high, after, preferred_element_type=jnp.float32) + jnp.dot(
                low, after, preferred_element_type=jnp.float32
            )
            weight = jnp.exp(score + total)
            if masked:
                weight = jnp.where(across < below, weight, 0.0)
            part = jnp.dot(
                weight.astype(jnp.bfloat16), values, preferred_element_type=jnp.float32
            )
            new.append((acc + part * jnp.exp(later), later + total[:, :1]))
        return tuple(new)

    start = tuple(
        (jnp.zeros(out_ref.shape, jnp.float32), jnp.zeros((rows, 1), jnp.float32))
        for h in range(heads)
    )
    carry = block(i, start, True)
    carry = lax.fori_loop(0, i, lambda n, c: block(i - 1 - n, c, False), carry)
    mixed = carry[0][0]
    for h in range(1, heads):
        mixed = jnp.where(lane // size == h, carry[h][0], mixed)
    out_ref[...] = mixed.astype(out_ref.dtype)


def halves(a):
    high = a.astype(jnp.bfloat16)
    return high, (a - high.astype(jnp.float32)).astype(jnp.bfloat16)


def product(a, b, dims=((1,), (0,))):
    def one(x, y):
        return lax.dot_general(x, y, (dims, ((), ())), preferred_element_type=jnp.float32)

    return one(a[0], b[0]) + (one(a[0], b[1]) + one(a[1], b[0]))


def delta_kernel(
    decay_scale_ref, write_bias_ref, p_ref, decay_pre_ref, write_pre_ref, shifts_ref, gain_ref,
    out_ref, maps, adds, decays, strengths,
):
    z = lax.axis_index("sp")
    length, size = out_ref.shape
    span = BLOCK
    group = 4
    row = lax.broadcasted_iota(jnp.int32, (span, span), 0)
    col = lax.broadcasted_iota(jnp.int32, (span, span), 1)
    inclusive, strictly = col <= row, col < row
    lower = jnp.where(inclusive, 1.0, 0.0)
    unit = jnp.where(col == row, 1.0, 0.0)
    diagonal = lax.broadcasted_iota(jnp.int32, (size, size), 0) == lax.broadcasted_iota(
        jnp.int32, (size, size), 1
    )

    def silu(a):
        a = a.astype(jnp.float32)
        return a * (1.0 / (1.0 + jnp.exp(-a)))

    def unit_of(a):
        return a * lax.rsqrt(jnp.sum(a * a, axis=-1, keepdims=True) + NORM_EPS)

    heads = decay_pre_ref.shape[1]
    rows = shifts_ref.shape[2]
    mine = lax.broadcasted_iota(jnp.int32, (rows, heads), 1) == z
    square = lax.broadcasted_iota(jnp.int32, (rows, rows), 0) == lax.broadcasted_iota(
        jnp.int32, (rows, rows), 1
    )
    rate = jnp.exp(jnp.full((rows, 1), decay_scale_ref[z], jnp.float32))
    for part in range(length // rows):
        at = slice(part * rows, (part + 1) * rows)

        def chosen(ref):
            return jnp.sum(jnp.where(mine, ref[at, :], 0.0), axis=1, keepdims=True)

        shift = jnp.sum(
            jnp.where(square, shifts_ref[part, pl.ds(z, 1), :], 0.0), axis=1, keepdims=True
        )
        pre = chosen(decay_pre_ref)
        soft = jnp.maximum(pre, 0.0) + jnp.log(1.0 + jnp.exp(-jnp.abs(pre)))
        decays[at, :] = shift - rate * soft
        write = chosen(write_pre_ref) + write_bias_ref[z]
        strengths[at, :] = 1.0 / (1.0 + jnp.exp(-write))

    def prepare(step, carry):
        blocks = []
        for b in range(group):
            at = pl.ds(pl.multiple_of((step * group + b) * span, span), span)
            q = unit_of(silu(p_ref[3, at, :])) * size ** (-0.5)
            k = unit_of(silu(p_ref[4, at, :]))
            v = silu(p_ref[5, at, :])
            decay = jnp.broadcast_to(decays[at, :], (span, size))
            strength = strengths[at, :]
            cumulative = jnp.dot(lower, decay, precision=EXACT_MATMUL)
            narrow = cumulative[:, :span]
            spread = narrow - narrow.T
            table = jnp.where(inclusive, jnp.exp(jnp.where(inclusive, spread, 0.0)), 0.0)
            growth = jnp.exp(cumulative)
            last = cumulative[span - 1 : span, :]
            beta = k * strength
            ks = halves(k)
            near = product(halves(beta), ks, ((1,), (1,)))
            strict = jnp.where(strictly, near * table, 0.0)
            inside = product(halves(q), ks, ((1,), (1,))) * table
            right = jnp.concatenate([v * strength, beta * growth], axis=1)
            damped = k * jnp.exp(last - cumulative)
            blocks.append([strict, inside, right, damped, q * growth, jnp.exp(last)])
        inverses = [unit - b[0] for b in blocks]
        powers = [halves(b[0]) for b in blocks]
        for level in range(max(1, (span - 1).bit_length()) - 1):
            powers = [halves(product(a, a)) for a in powers]
            inverses = [a + product(halves(a), c) for a, c in zip(inverses, powers)]
        for b in range(group):
            strict, inside, right, damped, boosted, keep = blocks[b]
            solved = halves(product(halves(inverses[b]), halves(right)))
            state = product(halves(damped), solved, ((0,), (0,)))
            seen = product(halves(inside), solved)
            step_map = jnp.where(diagonal, keep, 0.0) - state[:, size:]
            high, low = halves(step_map)
            qhigh, qlow = halves(boosted - seen[:, size:])
            n = step * group + b
            maps[n, 0, :size, :] = high
            maps[n, 0, size:, :] = qhigh
            maps[n, 1, :size, :] = low
            maps[n, 1, size:, :] = qlow
            adds[n, :size, :] = state[:, :size]
            adds[n, size:, :] = seen[:, :size]
        return carry

    lax.fori_loop(0, length // (span * group), prepare, 0)

    def walk(n, memory):
        new = product((maps[n, 0], maps[n, 1]), halves(memory)) + adds[n]
        made = new[size:]
        made = made * lax.rsqrt(jnp.mean(made * made, axis=-1, keepdims=True) + NORM_EPS)
        at = pl.ds(pl.multiple_of(n * span, span), span)
        out_ref[at, :] = (made * gain_ref[...]).astype(out_ref.dtype)
        return new[:size]

    lax.fori_loop(0, length // span, walk, jnp.zeros((size, size), jnp.float32))


def output_kernel(
    stick_ref, delta_ref, sw_hbm, dw_hbm, out_ref,
    sticks, deltas, sw_ref, dw_ref, outgoing, incoming, own,
    a_send, a_recv, l_sem, c_send, c_recv,
):
    sp, tp = lax.axis_size("sp"), lax.axis_size("tp")
    z, t = lax.axis_index("sp"), lax.axis_index("tp")
    rows = sticks.shape[0]
    half = rows // tp
    pieces = ((stick_ref, sticks), (delta_ref, deltas))

    def source(ref, who):
        return ref.at[pl.ds(pl.multiple_of(who * rows, rows), rows), :]

    def slot(ref):
        cols = stick_ref.shape[1]
        return ref.at[:, pl.ds(pl.multiple_of(z * cols, cols), cols)]

    local = [
        pltpu.make_async_copy(source(a, z), slot(b), l_sem.at[i])
        for i, (a, b) in enumerate(pieces)
    ]
    local += [
        pltpu.make_async_copy(sw_hbm, sw_ref, l_sem.at[2]),
        pltpu.make_async_copy(dw_hbm, dw_ref, l_sem.at[3]),
    ]
    for c in local:
        c.start()
    greet(("sp", "tp"))
    copies = []
    for k in range(1, sp):
        who = lax.rem(z + k, sp)
        for i, (a, b) in enumerate(pieces):
            c = remote(source(a, who), slot(b), a_send.at[k, i], a_recv.at[k, i], "sp", who)
            c.start()
            copies.append(c)
    for c in local:
        c.wait()
    for c in copies:
        c.wait_recv()
    chunks, width = outgoing.shape[0], outgoing.shape[2]
    mine = pl.ds(pl.multiple_of(t * half, half), half)
    partner = lax.rem(t + 1, tp)
    theirs = pl.ds(pl.multiple_of(partner * half, half), half)
    sends = []
    for c in range(chunks):
        columns = slice(c * width, (c + 1) * width)
        for which, target in ((theirs, outgoing), (mine, own)):
            target[c] = (
                jnp.dot(sticks[which, :], sw_ref[:, columns], preferred_element_type=jnp.float32)
                + jnp.dot(
                    deltas[which, :], dw_ref[:, columns], preferred_element_type=jnp.float32
                )
            ).astype(jnp.bfloat16)
        sends.append(
            remote(
                outgoing.at[c], incoming.at[c], c_send.at[c], c_recv.at[c], "tp", partner
            )
        )
        if c > 0:
            sends[c - 1].start()
    for c in copies:
        c.wait_send()
    sends[chunks - 1].start()
    for c in range(chunks):
        sends[c].wait_recv()
        out_ref[:, c * width : (c + 1) * width] = (
            own[c].astype(jnp.float32) + incoming[c].astype(jnp.float32)
        ).astype(out_ref.dtype)
    for c in sends:
        c.wait_send()


ANYWHERE = pl.BlockSpec(memory_space=pltpu.HBM)
ON_CORE = pl.BlockSpec(memory_space=pltpu.VMEM)


def on_device_heads(
    hidden_in, sb_query_w, sb_key_w, sb_value_w, sb_offset,
    delta_query_w, delta_key_w, delta_value_w, decay_w, write_w, write_bias,
    decay_log_scale, decay_shift, head_gain, sb_out_w, delta_out_w,
):
    sp, fs, tp = lax.axis_size("sp"), lax.axis_size("fs"), lax.axis_size("tp")
    z = lax.axis_index("sp")
    rows, half = hidden_in.shape[1:]
    width = half * tp
    length = rows * sp
    heads = decay_log_scale.shape[0]
    sb_heads = sb_offset.shape[0] // sp
    cols = sb_query_w.shape[1] // sp
    parts = 2
    dma = pltpu.SemaphoreType.DMA
    projected, decay_pre, write_pre, shifts = pl.pallas_call(
        project_kernel,
        name="project",
        out_shape=(
            jax.ShapeDtypeStruct((6, length, cols), jnp.bfloat16),
            jax.ShapeDtypeStruct((length, heads), jnp.float32),
            jax.ShapeDtypeStruct((length, heads), jnp.float32),
            jax.ShapeDtypeStruct((sp, heads, rows), jnp.float32),
        ),
        in_specs=[ANYWHERE] * 10,
        out_specs=(ON_CORE,) * 4,
        scratch_shapes=[
            pltpu.VMEM((sp, rows, width), jnp.bfloat16),
            pltpu.VMEM((width, 6 * cols), jnp.bfloat16),
            pltpu.VMEM((heads, width), jnp.bfloat16),
            pltpu.VMEM((heads, width), jnp.bfloat16),
            dma((2, sp, parts)), dma((2, sp, parts)), dma((2, sp, parts)), dma((2, sp, parts)),
            dma((fs, 6)), dma((fs, 6)), dma((sp,)), dma((sp,)), dma((4,)), dma((6,)),
        ],
        compiler_params=pltpu.CompilerParams(
            collective_id=0, has_side_effects=True, vmem_limit_bytes=ALL_VMEM
        ),
    )(
        hidden_in.reshape(rows, half), sb_query_w, sb_key_w, sb_value_w,
        delta_query_w, delta_key_w, delta_value_w, decay_w.T, write_w.T, decay_shift.reshape(heads, rows),
    )

    def pick(a, start, count, axis):
        return lax.dynamic_slice_in_dim(a, start, count, axis)

    stick = pl.pallas_call(
        stick_kernel,
        name="stick",
        grid=(sp,),
        out_shape=jax.ShapeDtypeStruct((length, cols), jnp.bfloat16),
        in_specs=[
            pl.BlockSpec(memory_space=pltpu.SMEM),
            pl.BlockSpec((3, length, cols), lambda i: (0, 0, 0)),
        ],
        out_specs=pl.BlockSpec((rows, cols), lambda i: (i, 0)),
        compiler_params=pltpu.CompilerParams(vmem_limit_bytes=ALL_VMEM),
    )(pick(sb_offset, z * sb_heads, sb_heads, 0), projected)
    delta = pl.pallas_call(
        delta_kernel,
        name="delta",
        out_shape=jax.ShapeDtypeStruct((length, cols), jnp.bfloat16),
        in_specs=[pl.BlockSpec(memory_space=pltpu.SMEM)] * 2 + [ON_CORE] * 5,
        out_specs=ON_CORE,
        scratch_shapes=[
            pltpu.VMEM((length // BLOCK, 2, cols + BLOCK, cols), jnp.bfloat16),
            pltpu.VMEM((length // BLOCK, cols + BLOCK, cols), jnp.float32),
            pltpu.VMEM((length, 1), jnp.float32),
            pltpu.VMEM((length, 1), jnp.float32),
        ],
        compiler_params=pltpu.CompilerParams(vmem_limit_bytes=ALL_VMEM),
    )(
        decay_log_scale, write_bias, projected, decay_pre, write_pre, shifts,
        head_gain.reshape(1, -1),
    )
    chunks = 4
    result = pl.pallas_call(
        output_kernel,
        name="output",
        out_shape=jax.ShapeDtypeStruct((rows // tp, width), jnp.bfloat16),
        in_specs=[ON_CORE, ON_CORE, ANYWHERE, ANYWHERE],
        out_specs=ON_CORE,
        scratch_shapes=[
            pltpu.VMEM((rows, cols * sp), jnp.bfloat16),
            pltpu.VMEM((rows, cols * sp), jnp.bfloat16),
            pltpu.VMEM(sb_out_w.shape, jnp.bfloat16),
            pltpu.VMEM(delta_out_w.shape, jnp.bfloat16),
            pltpu.VMEM((chunks, rows // tp, width // chunks), jnp.bfloat16),
            pltpu.VMEM((chunks, rows // tp, width // chunks), jnp.bfloat16),
            pltpu.VMEM((chunks, rows // tp, width // chunks), jnp.bfloat16),
            dma((sp, 2)), dma((sp, 2)), dma((4,)), dma((chunks,)), dma((chunks,)),
        ],
        compiler_params=pltpu.CompilerParams(
            collective_id=1, has_side_effects=True, vmem_limit_bytes=ALL_VMEM
        ),
    )(stick, delta, sb_out_w, delta_out_w)
    return result.reshape(1, rows // tp, width)


def on_device(*inputs):
    delta_heads = inputs[11].shape[0]
    square = lax.axis_size("fs") == 4 and lax.axis_size("tp") == 2
    if square and delta_heads == lax.axis_size("sp") and inputs[4].shape[0] % delta_heads == 0:
        return on_device_heads(*inputs)
    return on_device_split(*inputs)


def solution(mesh):
    return jax.shard_map(
        on_device,
        mesh=mesh,
        in_specs=(
            P("fs", "sp", "tp"),
            P("fs", "tp"),
            P("fs", "tp"),
            P("fs", "tp"),
            P("tp"),
            P("fs", "tp"),
            P("fs", "tp"),
            P("fs", "tp"),
            P(None, "tp"),
            P(None, "tp"),
            P("tp"),
            P("tp"),
            P("fs", "tp", "sp"),
            P(),
            P("tp", None),
            P("tp", None),
        ),
        out_specs=P("fs", ("sp", "tp"), None),
        check_vma=False,
    )
```

profile of v0, /device:TPU:0, one launch (start us, length us, event | category | flops | bytes accessed | tf_op | source)
XLA Modules:
  0.0 100.1 jit_solution(6572988500747065769)
XLA Ops:
  0.0 49.3 %project.1 = (bf16[6,1024,128]{2,1,0:T(8,128)(2,1)}, f32[1024,4]{1,0:T(8,128)}, f32[1024,4]{1,0:T(8,128)}, f32[4,4,256]{2,1,0:T(4,128)}) custom-call(bf16[256,1024]{1,0:T(8,128)(2,1)} %bitcast.7, bf16[512,512]{1,0:T(8,128)(2,1)} %w0.1, bf16[512,512]{1,0:T(8,128)(2,1)} %w1.1, bf16[512,512]{1,0:T(8,128)(2,1)} %w2.1, bf16[512,512]{1,0:T(8,128)(2,1)} %w3.1, ...), custom_call_target="tpu_custom_call" | custom-call | tf_op jit(solution)/shard_map/project/pallas_call | solution.py:781
  49.3 18.1 %delta.1.delta_ref = bf16[1024,128]{1,0:T(8,128)(2,1)} custom-call(f32[4]{0:T(128)} %decay_scale_ref.1, f32[4]{0:T(128)} %write_bias_ref.1, bf16[6,1024,128]{2,1,0:T(8,128)(2,1)} %get-tuple-element.9.p_ref, f32[1024,4]{1,0:T(8,128)} %get-tuple-element.10.decay_pre_ref, f32[1024,4]{1,0:T(8,128)} %get-tuple-element.11.write_pre_ref, ...), custom_call_target="tpu_custom_call" | custom-call | tf_op jit(solution)/shard_map/delta/pallas_call | solution.py:823
  67.4 1.3 %dynamic_slice.3.offset_ref = f32[2]{0:T(128)} dynamic-slice(f32[8]{0:T(128)} %param.20, s32[]{:T(128)S(6)} %select_n.3), dynamic_slice_sizes={2} | dynamic-slice | bytes 20 | tf_op jit(solution)/shard_map/dynamic_slice | solution.py:809
  68.7 12.8 %stick.1.stick_ref = bf16[1024,128]{1,0:T(8,128)(2,1)} custom-call(f32[2]{0:T(128)} %dynamic_slice.3.offset_ref, bf16[6,1024,128]{2,1,0:T(8,128)(2,1)} %get-tuple-element.9.p_ref), custom_call_target="tpu_custom_call" | custom-call | tf_op jit(solution)/shard_map/stick/pallas_call | solution.py:811
  81.5 16.7 %output.1 = bf16[128,2048]{1,0:T(8,128)(2,1)} custom-call(bf16[1024,128]{1,0:T(8,128)(2,1)} %stick.1.stick_ref, bf16[1024,128]{1,0:T(8,128)(2,1)} %delta.1.delta_ref, bf16[512,2048]{1,0:T(8,128)(2,1)} %sw_hbm.1, bf16[512,2048]{1,0:T(8,128)(2,1)} %dw_hbm.1), custom_call_target="tpu_custom_call" | custom-call | tf_op jit(solution)/shard_map/output/pallas_call | solution.py:841
  98.2 1.9 %copy.18 = bf16[1,128,2048]{2,1,0:T(8,128)(2,1)} copy(bf16[1,128,2048]{2,1,0:T(8,128)(2,1)} %bitcast.6) | data formatting | bytes 1048576
where the time goes:
time: 100 us
  Pallas kernels  96.9 us (97%)
  local copies, waits for them, and re-layouts  3.19 us (3%)
    pallas_call x1, Pallas kernels, on_device_heads(): pl.pallas_call(project_kernel, name='project', out_shape=(jax.ShapeDtypeS...  49.3 us
    pallas_call x1, Pallas kernels, on_device_heads(): pl.pallas_call(delta_kernel, name='delta', out_shape=jax.ShapeDtypeStruct...  18.1 us
    pallas_call x1, Pallas kernels, on_device_heads(): pl.pallas_call(output_kernel, name='output', out_shape=jax.ShapeDtypeStru...  16.7 us
    pallas_call x1, Pallas kernels, on_device_heads(): pl.pallas_call(stick_kernel, name='stick', grid=(sp,), out_shape=jax.Shap...  12.8 us

commit v1 on v0

--- a/solution.py
+++ b/solution.py
@@ -343,11 +343,35 @@
     pl.semaphore_wait(barrier, count)
 
 
-def project_kernel(
-    x_ref, w0, w1, w2, w3, w4, w5, decay_w_ref, write_w_ref, shift_ref,
-    p_ref, decay_pre_ref, write_pre_ref, shifts_ref,
-    xs, ws, decay_w, write_w,
+def halves(a):
+    high = a.astype(jnp.bfloat16)
+    return high, (a - high.astype(jnp.float32)).astype(jnp.bfloat16)
+
+
+def dot_f32(a, b, dims=((1,), (0,))):
+    return lax.dot_general(a, b, (dims, ((), ())), preferred_element_type=jnp.float32)
+
+
+def wide_rhs(high, low, axis):
+    top = jnp.concatenate([high, low], axis=axis)
+    bottom = jnp.concatenate([high, jnp.zeros_like(low)], axis=axis)
+    return jnp.concatenate([top, bottom], axis=1 - axis)
+
+
+def folded(a):
+    half = a.shape[1] // 2
+    return a[:, :half] + a[:, half:]
+
+
+def layer_kernel(
+    offset_ref, decay_scale_ref, write_bias_ref,
+    x_ref, w0, w1, w2, w3, w4, w5, decay_w_ref, write_w_ref, shift_ref, gain_ref, sw_hbm, dw_hbm,
+    out_ref,
+    xs, ws, gate_w, gates, shifts_ref,
+    proj, acc, later, maps, adds, stick_out, delta_out,
+    sticks, deltas, sw_ref, dw_ref, partial, outgoing, incoming, own,
     x_send, x_recv, f_send, f_recv, w_send, w_recv, s_send, s_recv, l_sem, lw_sem,
+    a_send, a_recv, c_send, c_recv,
 ):
     weights = (w0, w1, w2, w3, w4, w5)
     sp, tp = lax.axis_size("sp"), lax.axis_size("tp")
@@ -356,12 +380,17 @@
     depth = w0.shape[0]
     cols = ws.shape[1] // len(weights)
     parts = x_send.shape[2]
+    heads = decay_w_ref.shape[0]
     slot = pl.ds(pl.multiple_of(t * half, half), half)
     local = [
         pltpu.make_async_copy(x_ref, xs.at[z, :, slot], l_sem.at[0]),
         pltpu.make_async_copy(shift_ref, shifts_ref.at[z], l_sem.at[1]),
-        pltpu.make_async_copy(decay_w_ref, decay_w, l_sem.at[2]),
-        pltpu.make_async_copy(write_w_ref, write_w, l_sem.at[3]),
+        pltpu.make_async_copy(decay_w_ref, gate_w.at[0], l_sem.at[2]),
+        pltpu.make_async_copy(write_w_ref, gate_w.at[1], l_sem.at[3]),
+    ]
+    late = [
+        pltpu.make_async_copy(sw_hbm, sw_ref, l_sem.at[4]),
+        pltpu.make_async_copy(dw_hbm, dw_ref, l_sem.at[5]),
     ]
 
     def w_src(i):
@@ -433,6 +462,8 @@
         s_copies.append(c)
     for part in range(parts):
         forward(0, 0, part).start()
+    for c in late:
+        c.start()
 
     relays = []
 
@@ -448,20 +479,24 @@
             c.start()
             relays.append(c)
 
-    for step in range(1, sp):
-        relay(step - 1)
-        for part in range(parts):
-            for way in range(2):
-                @pl.when(comes(way, step))
-                def _():
-                    x_copy(way, step, part).wait_recv()
-                    forward(way, step, part).start()
-                    if step + 1 < sp:
-                        @pl.when(onward(way))
-                        def _():
-                            x_copy(way, step + 1, part).start()
-    for position in range(sp - 1, count // 2):
+    def arrive(step, part):
+        for way in range(2):
+            @pl.when(comes(way, step))
+            def _():
+                x_copy(way, step, part).wait_recv()
+                forward(way, step, part).start()
+                if step + 1 < sp:
+                    @pl.when(onward(way))
+                    def _():
+                        x_copy(way, step + 1, part).start()
+
+    early = [(step, part) for step in range(1, sp - 1) for part in range(parts)]
+    relay(0)
+    arrive(*early[0])
+    for position in range(1, count // 2):
         relay(position)
+    for step, part in early[1:]:
+        arrive(step, part)
     for c in local:
         c.wait()
     for side in range(2):
@@ -469,37 +504,341 @@
             w_copies[side, orders[side][position]].wait_recv()
     for c in relays:
         c.wait_recv()
-
-    def project(block):
-        at = pl.ds(pl.multiple_of(block * rows, rows), rows)
-        for i in range(0, count, 2):
-            out = jnp.dot(
-                xs[block], ws[:, i * cols : (i + 2) * cols], preferred_element_type=jnp.float32
-            ).astype(jnp.bfloat16)
-            p_ref[i, at, :] = out[:, :cols]
-            p_ref[i + 1, at, :] = out[:, cols:]
-        decay_pre_ref[at, :] = lax.dot_general(
-            xs[block], decay_w[...], (((1,), (1,)), ((), ())),
-            preferred_element_type=jnp.float32,
-        )
-        write_pre_ref[at, :] = lax.dot_general(
-            xs[block], write_w[...], (((1,), (1,)), ((), ())),
-            preferred_element_type=jnp.float32,
-        )
-
+    for c in s_copies:
+        c.wait_recv()
     for part in range(parts):
         forward(0, 0, part).wait_recv()
-    project(z)
-    for step in range(1, sp):
-        for way in range(2):
-            @pl.when(comes(way, step))
-            def _():
-                for part in range(parts):
-                    forward(way, step, part).wait_recv()
-                project(z - step if way == 0 else z + step)
-    for c in s_copies:
-        c.wait_recv()
-    for c in list(w_copies.values()) + relays + s_copies:
+
+    size = offset_ref.shape[0] // sp
+    sb_size = cols // size
+    scale = sb_size ** (-0.5)
+    tile = rows // 2
+    below = lax.broadcasted_iota(jnp.int32, (rows, rows), 0)
+    across = lax.broadcasted_iota(jnp.int32, (rows, rows), 1)
+    after = jnp.where(below > across, 1.0, 0.0).astype(jnp.bfloat16)
+
+    def at_block(b, start=0, extent=rows):
+        return pl.ds(pl.multiple_of(b * rows + start, extent), extent)
+
+    def pair(i, j, masked):
+        for part in range(rows // tile):
+            span = (part + 1) * tile if masked else rows
+            mine = at_block(i, part * tile, tile)
+            q = proj[0, mine, :]
+            keys, values = proj[1, at_block(j), :], proj[2, at_block(j), :]
+            keys, values = keys[:span], values[:span]
+            lane = lax.broadcasted_iota(jnp.int32, (tile, cols), 1)
+            if masked:
+                seen = across[:tile, :span] < below[:tile, :span] + part * tile
+            mixed = total = None
+            for h in range(size):
+                query = jnp.where(lane // sb_size == h, q, jnp.zeros_like(q))
+                score = dot_f32(query, keys, ((1,), (1,))) * scale + offset_ref[z * size + h]
+                skip = jnp.maximum(
+                    score, jnp.log(1.0 + jnp.exp(jnp.minimum(score, 80.0)))
+                )
+                weight = score - skip
+                if masked:
+                    skip = jnp.where(seen, skip, 0.0)
+                beyond = dot_f32(skip.astype(jnp.bfloat16), after[:span, :span])
+                weight = jnp.exp(weight - beyond)
+                if masked:
+                    weight = jnp.where(seen, weight, 0.0)
+                part_out = dot_f32(weight.astype(jnp.bfloat16), values)
+                whole = jnp.broadcast_to(beyond[:, :1] + skip[:, :1], (tile, cols))
+                mixed = part_out if h == 0 else jnp.where(lane // sb_size == h, part_out, mixed)
+                total = whole if h == 0 else jnp.where(lane // sb_size == h, whole, total)
+            if masked:
+                acc[mine, :] = mixed
+                later[mine, :] = total
+            else:
+                passed = later[mine, :]
+                acc[mine, :] = acc[mine, :] + mixed * jnp.exp(-passed)
+                later[mine, :] = passed + total
+
+    span = BLOCK
+    duo = 2 * span
+    blocks = rows // span
+    width = GDN_DIM
+    seg_row = lax.broadcasted_iota(jnp.int32, (rows, rows), 0)
+    seg_col = lax.broadcasted_iota(jnp.int32, (rows, rows), 1)
+    together = seg_row // span == seg_col // span
+    upto = jnp.where(jnp.logical_and(together, seg_row <= seg_col), 1.0, 0.0).astype(jnp.bfloat16)
+    beyond_it = jnp.where(jnp.logical_and(together, seg_row > seg_col), 1.0, 0.0).astype(
+        jnp.bfloat16
+    )
+    prow = lax.broadcasted_iota(jnp.int32, (span, duo), 0)
+    plane = lax.broadcasted_iota(jnp.int32, (span, duo), 1)
+    first = plane < span
+    pcol = jnp.where(first, plane, plane - span)
+    inclusive, strictly = pcol <= prow, pcol < prow
+    unit = jnp.where(pcol == prow, 1.0, 0.0)
+    diagonal = lax.broadcasted_iota(jnp.int32, (width, width), 0) == lax.broadcasted_iota(
+        jnp.int32, (width, width), 1
+    )
+    eighth = lax.broadcasted_iota(jnp.int32, (8, rows), 0)
+
+    def silu(a):
+        return a * (1.0 / (1.0 + jnp.exp(-a)))
+
+    def unit_of(a):
+        return a * lax.rsqrt(jnp.sum(a * a, axis=-1, keepdims=True) + NORM_EPS)
+
+    def apart(a):
+        lanes = lax.broadcasted_iota(jnp.int32, a.shape, 1) < span
+        zero = jnp.zeros_like(a)
+        return jnp.concatenate([jnp.where(lanes, a, zero), jnp.where(lanes, zero, a)], axis=0)
+
+    def squared(left, power):
+        high, low = halves(power)
+        lhigh, llow = halves(left)
+        return folded(
+            dot_f32(
+                jnp.concatenate([lhigh, llow], axis=1), wide_rhs(apart(high), apart(low), 1)
+            )
+        )
+
+    def prepare(b, dq, dk, dv):
+        for side in range(2):
+            gates[side * heads : (side + 1) * heads, :] = dot_f32(
+                gate_w[side], xs[b], ((1,), (1,))
+            )
+        pre = gates[pl.ds(z, 1), :]
+        write = gates[pl.ds(heads + z, 1), :] + write_bias_ref[z]
+        rate = jnp.exp(jnp.full((1, rows), decay_scale_ref[z], jnp.float32))
+        soft = jnp.maximum(pre, 0.0) + jnp.log(1.0 + jnp.exp(-jnp.abs(pre)))
+        decay = shifts_ref[b, pl.ds(z, 1), :] - rate * soft
+        strength = 1.0 / (1.0 + jnp.exp(-write))
+        d1 = decay.astype(jnp.bfloat16).astype(jnp.float32)
+        d2 = (decay - d1).astype(jnp.bfloat16).astype(jnp.float32)
+        d3 = decay - d1 - d2
+        three = jnp.where(
+            eighth == 0, d1, jnp.where(eighth == 1, d2, jnp.where(eighth == 2, d3, 0.0))
+        ).astype(jnp.bfloat16)
+        cum_row = jnp.sum(dot_f32(three, upto), axis=0, keepdims=True)
+        rest_row = jnp.sum(dot_f32(three, beyond_it), axis=0, keepdims=True)
+        stack = jnp.where(
+            eighth == 0, strength,
+            jnp.where(
+                eighth == 1, jnp.exp(cum_row),
+                jnp.where(eighth == 2, jnp.exp(rest_row), cum_row),
+            ),
+        )
+        columns = stack.T
+        s_col, grow, damp, cum = (columns[:, n : n + 1] for n in range(4))
+        q = unit_of(silu(dq)) * width ** (-0.5)
+        k = unit_of(silu(dk))
+        v = silu(dv)
+        boosted = q * grow
+        damped = k * damp
+        right = jnp.concatenate([v * s_col, k * (s_col * grow)], axis=1)
+        kh, kl = halves(k)
+        qh, ql = halves(q)
+        work = []
+        for duo_at in range(rows // duo):
+            lo = duo_at * duo
+            here = slice(lo, lo + duo)
+            left = jnp.concatenate(
+                [
+                    jnp.concatenate([kh[here], kl[here]], axis=1),
+                    jnp.concatenate([qh[here], ql[here]], axis=1),
+                ],
+                axis=0,
+            )
+            gram = folded(
+                dot_f32(left, wide_rhs(kh[here], kl[here], 0), ((1,), (1,)))
+            )
+            spread = (
+                jnp.where(first, cum[lo : lo + span], cum[lo + span : lo + duo])
+                - cum_row[:, here]
+            )
+            table = jnp.where(inclusive, jnp.exp(jnp.where(inclusive, spread, 0.0)), 0.0)
+            scale_col = jnp.where(first, s_col[lo : lo + span], s_col[lo + span : lo + duo])
+            near_k = jnp.where(first, gram[:span], gram[span:duo])
+            near_q = jnp.where(first, gram[duo : duo + span], gram[duo + span :])
+            strict = jnp.where(strictly, near_k * table * scale_col, 0.0)
+            work.append([unit - strict, strict, near_q * table])
+        for w in work:
+            w[1] = squared(w[1], w[1])
+        levels = max(1, (span - 1).bit_length()) - 1
+        for level in range(levels):
+            for w in work:
+                if level + 1 < levels:
+                    both = squared(jnp.concatenate([w[1], w[0]], axis=0), w[1])
+                    w[1], w[0] = both[:span], w[0] + both[span:]
+                else:
+                    w[0] = w[0] + squared(w[0], w[1])
+        for duo_at, (inverse, _, inside) in enumerate(work):
+            lo = duo_at * duo
+            here = slice(lo, lo + duo)
+            ih, il = (apart(a) for a in halves(inverse))
+            rh, rl = halves(right[here])
+            solved = dot_f32(
+                jnp.concatenate([ih, il], axis=1), jnp.concatenate([rh, rh], axis=0)
+            ) + dot_f32(ih, rl)
+            lh, ll = (
+                apart(a) for a in halves(jnp.concatenate([damped[here].T, inside], axis=0))
+            )
+            sh, sl = halves(solved)
+            made = dot_f32(
+                jnp.concatenate([lh, ll], axis=1), jnp.concatenate([sh, sh], axis=0)
+            ) + dot_f32(lh, sl)
+            for side in range(2):
+                at = lo + side * span
+                mine = made[side * (width + span) : (side + 1) * (width + span)]
+                n = b * blocks + 2 * duo_at + side
+                keep = grow[at + span - 1 : at + span]
+                step_map = jnp.where(diagonal, keep, 0.0) - mine[:width, width:]
+                query = boosted[at : at + span] - mine[width:, width:]
+                high, low = halves(jnp.concatenate([step_map, query], axis=0))
+                maps[n, :, :width] = high
+                maps[n, :, width:] = low
+                adds[n] = mine[:, :width]
+
+    def wait_x(way, step):
+        for part in range(parts):
+            if step == sp - 1:
+                x_copy(way, step, part).wait_recv()
+                forward(way, step, part).start()
+        for part in range(parts):
+            forward(way, step, part).wait_recv()
+
+    shorter = jnp.minimum(z, sp - 1 - z)
+    down_last = z > sp - 1 - z
+
+    def event(n, reach):
+        lowest, highest = reach
+        both = n <= 2 * shorter
+        way_n = jnp.where(both, lax.rem(n + 1, 2), jnp.where(down_last, 0, 1))
+        step_n = jnp.where(n == 0, 0, jnp.where(both, (n + 1) // 2, n - shorter))
+        for step in range(1, sp):
+            for way in range(2):
+                @pl.when(jnp.logical_and(step_n == step, way_n == way))
+                def _():
+                    wait_x(way, step)
+        down = jnp.logical_and(way_n == 0, n > 0)
+        b = jnp.where(down, z - step_n, z + step_n)
+        for i in range(0, 3 * cols, 3 * cols // 3):
+            proj[i // cols, at_block(b), :] = dot_f32(
+                xs[b], ws[:, i : i + cols]
+            ).astype(jnp.bfloat16)
+        drows = dot_f32(xs[b], ws[:, 3 * cols :]).astype(jnp.bfloat16).astype(jnp.float32)
+        prepare(b, drows[:, :cols], drows[:, cols : 2 * cols], drows[:, 2 * cols :])
+        pair(b, b, True)
+
+        def off(m, c):
+            i = jnp.where(down, b + 1 + m, b)
+            j = jnp.where(down, b, b - 1 - m)
+            pair(i, j, False)
+            return c
+
+        lowest = jnp.minimum(lowest, b)
+        highest = jnp.maximum(highest, b)
+        lax.fori_loop(0, highest - lowest, off, 0)
+        return lowest, highest
+
+    lax.fori_loop(0, sp, event, (z, z))
+
+    out_copies = []
+
+    def give(kind, out, target):
+        which = 0 if kind == "stick" else 1
+        here = target.at[:, pl.ds(pl.multiple_of(z * cols, cols), cols)]
+
+        def send(g, k):
+            return remote(
+                out.at[g * rows : (g + 1) * rows, :], here,
+                a_send.at[k, which], a_recv.at[k, which], "sp", g,
+            )
+
+        def started(g):
+            for k in range(1, sp):
+                @pl.when(lax.rem(z + k, sp) == g)
+                def _():
+                    send(g, k).start()
+
+        def finished():
+            for g in range(sp):
+                for k in range(1, sp):
+                    @pl.when(lax.rem(z + k, sp) == g)
+                    def _():
+                        send(g, k).wait_send()
+
+        def came():
+            for k in range(1, sp):
+                send(0, k).wait_recv()
+
+        return started, finished, came
+
+    stick_started, stick_finished, stick_came = give("stick", stick_out, sticks)
+    delta_started, delta_finished, delta_came = give("delta", delta_out, deltas)
+
+    for g in range(sp):
+        at = slice(g * rows, (g + 1) * rows)
+        stick_out[at, :] = acc[at, :].astype(jnp.bfloat16)
+        if g > 0:
+            stick_started(g - 1)
+
+    def walk(n, memory):
+        high, low = halves(memory)
+        new = folded(dot_f32(maps[n], wide_rhs(high, low, 1))) + adds[n]
+        made = new[width:]
+        made = made * lax.rsqrt(jnp.mean(made * made, axis=-1, keepdims=True) + NORM_EPS)
+        at = pl.ds(pl.multiple_of(n * span, span), span)
+        delta_out[at, :] = (made * gain_ref[...]).astype(delta_out.dtype)
+        return new[:width]
+
+    memory = jnp.zeros((width, width), jnp.float32)
+    for g in range(sp):
+        memory = lax.fori_loop(g * blocks, (g + 1) * blocks, walk, memory)
+        if g == 0:
+            stick_started(sp - 1)
+        else:
+            delta_started(g - 1)
+
+    mine_z = pl.ds(pl.multiple_of(z * rows, rows), rows)
+    lanes = pl.ds(pl.multiple_of(z * cols, cols), cols)
+    sticks[:, lanes] = stick_out[mine_z, :]
+    deltas[:, lanes] = delta_out[mine_z, :]
+    for c in late:
+        c.wait()
+    delta_started(sp - 1)
+    stick_came()
+    chunks, wide = outgoing.shape[0], outgoing.shape[2]
+    share = rows // tp
+    for c in range(chunks):
+        columns = slice(c * wide, (c + 1) * wide)
+        partial[:, columns] = dot_f32(sticks[...], sw_ref[:, columns])
+    delta_came()
+    mine = pl.ds(pl.multiple_of(t * share, share), share)
+    partner = lax.rem(t + 1, tp)
+    theirs = pl.ds(pl.multiple_of(partner * share, share), share)
+
+    def finish(which, c):
+        columns = slice(c * wide, (c + 1) * wide)
+        return (
+            partial[which, columns] + dot_f32(deltas[which, :], dw_ref[:, columns])
+        ).astype(jnp.bfloat16)
+
+    swaps = [
+        remote(outgoing.at[c], incoming.at[c], c_send.at[c], c_recv.at[c], "tp", partner)
+        for c in range(chunks)
+    ]
+    for c in range(chunks):
+        outgoing[c] = finish(theirs, c)
+        if c > 0:
+            swaps[c - 1].start()
+    for c in range(chunks):
+        own[c] = finish(mine, c)
+        if c == 0:
+            swaps[chunks - 1].start()
+    for c in range(chunks):
+        swaps[c].wait_recv()
+        out_ref[:, c * wide : (c + 1) * wide] = (
+            own[c].astype(jnp.float32) + incoming[c].astype(jnp.float32)
+        ).astype(out_ref.dtype)
+
+    for c in list(w_copies.values()) + relays + s_copies + swaps:
         c.wait_send()
     for part in range(parts):
         forward(0, 0, part).wait_send()
@@ -512,255 +851,13 @@
                 @pl.when(comes(way, step))
                 def _():
                     forward(way, step, part).wait_send()
-
-
-def stick_kernel(offset_ref, p_ref, out_ref):
-    rows = out_ref.shape[0]
-    i = pl.program_id(0)
-    lane = lax.broadcasted_iota(jnp.int32, (rows, out_ref.shape[1]), 1)
-    heads = offset_ref.shape[0]
-    size = out_ref.shape[1] // heads
-    below = lax.broadcasted_iota(jnp.int32, (rows, rows), 0)
-    across = lax.broadcasted_iota(jnp.int32, (rows, rows), 1)
-    after = jnp.where(below >= across, 1.0, 0.0).astype(jnp.bfloat16)
-    scale = size ** (-0.5)
-    q = p_ref[0, pl.ds(pl.multiple_of(i * rows, rows), rows), :]
-    queries = [
-        jnp.where(lane // size == h, q, jnp.zeros_like(q)) for h in range(heads)
-    ]
-
-    def block(j, carry, masked):
-        at = pl.ds(pl.multiple_of(j * rows, rows), rows)
-        keys, values = p_ref[1, at, :], p_ref[2, at, :]
-        new = []
-        for h in range(heads):
-            acc, later = carry[h]
-            score = (
-                lax.dot_general(
-                    queries[h], keys, (((1,), (1,)), ((), ())),
-                    preferred_element_type=jnp.float32,
-                ) * scale + offset_ref[h]
-            )
-            skip = -(jnp.maximum(score, 0.0) + jnp.log(1.0 + jnp.exp(-jnp.abs(score))))
-            if masked:
-                skip = jnp.where(across < below, skip, 0.0)
-            high = skip.astype(jnp.bfloat16)
-            low = (skip - high.astype(jnp.float32)).astype(jnp.bfloat16)
-            total = jnp.dot(high, after, preferred_element_type=jnp.float32) + jnp.dot(
-                low, after, preferred_element_type=jnp.float32
-            )
-            weight = jnp.exp(score + total)
-            if masked:
-                weight = jnp.where(across < below, weight, 0.0)
-            part = jnp.dot(
-                weight.astype(jnp.bfloat16), values, preferred_element_type=jnp.float32
-            )
-            new.append((acc + part * jnp.exp(later), later + total[:, :1]))
-        return tuple(new)
-
-    start = tuple(
-        (jnp.zeros(out_ref.shape, jnp.float32), jnp.zeros((rows, 1), jnp.float32))
-        for h in range(heads)
-    )
-    carry = block(i, start, True)
-    carry = lax.fori_loop(0, i, lambda n, c: block(i - 1 - n, c, False), carry)
-    mixed = carry[0][0]
-    for h in range(1, heads):
-        mixed = jnp.where(lane // size == h, carry[h][0], mixed)
-    out_ref[...] = mixed.astype(out_ref.dtype)
-
-
-def halves(a):
-    high = a.astype(jnp.bfloat16)
-    return high, (a - high.astype(jnp.float32)).astype(jnp.bfloat16)
-
-
-def product(a, b, dims=((1,), (0,))):
-    def one(x, y):
-        return lax.dot_general(x, y, (dims, ((), ())), preferred_element_type=jnp.float32)
-
-    return one(a[0], b[0]) + (one(a[0], b[1]) + one(a[1], b[0]))
-
-
-def delta_kernel(
-    decay_scale_ref, write_bias_ref, p_ref, decay_pre_ref, write_pre_ref, shifts_ref, gain_ref,
-    out_ref, maps, adds, decays, strengths,
-):
-    z = lax.axis_index("sp")
-    length, size = out_ref.shape
-    span = BLOCK
-    group = 4
-    row = lax.broadcasted_iota(jnp.int32, (span, span), 0)
-    col = lax.broadcasted_iota(jnp.int32, (span, span), 1)
-    inclusive, strictly = col <= row, col < row
-    lower = jnp.where(inclusive, 1.0, 0.0)
-    unit = jnp.where(col == row, 1.0, 0.0)
-    diagonal = lax.broadcasted_iota(jnp.int32, (size, size), 0) == lax.broadcasted_iota(
-        jnp.int32, (size, size), 1
-    )
-
-    def silu(a):
-        a = a.astype(jnp.float32)
-        return a * (1.0 / (1.0 + jnp.exp(-a)))
-
-    def unit_of(a):
-        return a * lax.rsqrt(jnp.sum(a * a, axis=-1, keepdims=True) + NORM_EPS)
-
-    heads = decay_pre_ref.shape[1]
-    rows = shifts_ref.shape[2]
-    mine = lax.broadcasted_iota(jnp.int32, (rows, heads), 1) == z
-    square = lax.broadcasted_iota(jnp.int32, (rows, rows), 0) == lax.broadcasted_iota(
-        jnp.int32, (rows, rows), 1
-    )
-    rate = jnp.exp(jnp.full((rows, 1), decay_scale_ref[z], jnp.float32))
-    for part in range(length // rows):
-        at = slice(part * rows, (part + 1) * rows)
-
-        def chosen(ref):
-            return jnp.sum(jnp.where(mine, ref[at, :], 0.0), axis=1, keepdims=True)
-
-        shift = jnp.sum(
-            jnp.where(square, shifts_ref[part, pl.ds(z, 1), :], 0.0), axis=1, keepdims=True
-        )
-        pre = chosen(decay_pre_ref)
-        soft = jnp.maximum(pre, 0.0) + jnp.log(1.0 + jnp.exp(-jnp.abs(pre)))
-        decays[at, :] = shift - rate * soft
-        write = chosen(write_pre_ref) + write_bias_ref[z]
-        strengths[at, :] = 1.0 / (1.0 + jnp.exp(-write))
-
-    def prepare(step, carry):
-        blocks = []
-        for b in range(group):
-            at = pl.ds(pl.multiple_of((step * group + b) * span, span), span)
-            q = unit_of(silu(p_ref[3, at, :])) * size ** (-0.5)
-            k = unit_of(silu(p_ref[4, at, :]))
-            v = silu(p_ref[5, at, :])
-            decay = jnp.broadcast_to(decays[at, :], (span, size))
-            strength = strengths[at, :]
-            cumulative = jnp.dot(lower, decay, precision=EXACT_MATMUL)
-            narrow = cumulative[:, :span]
-            spread = narrow - narrow.T
-            table = jnp.where(inclusive, jnp.exp(jnp.where(inclusive, spread, 0.0)), 0.0)
-            growth = jnp.exp(cumulative)
-            last = cumulative[span - 1 : span, :]
-            beta = k * strength
-            ks = halves(k)
-            near = product(halves(beta), ks, ((1,), (1,)))
-            strict = jnp.where(strictly, near * table, 0.0)
-            inside = product(halves(q), ks, ((1,), (1,))) * table
-            right = jnp.concatenate([v * strength, beta * growth], axis=1)
-            damped = k * jnp.exp(last - cumulative)
-            blocks.append([strict, inside, right, damped, q * growth, jnp.exp(last)])
-        inverses = [unit - b[0] for b in blocks]
-        powers = [halves(b[0]) for b in blocks]
-        for level in range(max(1, (span - 1).bit_length()) - 1):
-            powers = [halves(product(a, a)) for a in powers]
-            inverses = [a + product(halves(a), c) for a, c in zip(inverses, powers)]
-        for b in range(group):
-            strict, inside, right, damped, boosted, keep = blocks[b]
-            solved = halves(product(halves(inverses[b]), halves(right)))
-            state = product(halves(damped), solved, ((0,), (0,)))
-            seen = product(halves(inside), solved)
-            step_map = jnp.where(diagonal, keep, 0.0) - state[:, size:]
-            high, low = halves(step_map)
-            qhigh, qlow = halves(boosted - seen[:, size:])
-            n = step * group + b
-            maps[n, 0, :size, :] = high
-            maps[n, 0, size:, :] = qhigh
-            maps[n, 1, :size, :] = low
-            maps[n, 1, size:, :] = qlow
-            adds[n, :size, :] = state[:, :size]
-            adds[n, size:, :] = seen[:, :size]
-        return carry
-
-    lax.fori_loop(0, length // (span * group), prepare, 0)
-
-    def walk(n, memory):
-        new = product((maps[n, 0], maps[n, 1]), halves(memory)) + adds[n]
-        made = new[size:]
-        made = made * lax.rsqrt(jnp.mean(made * made, axis=-1, keepdims=True) + NORM_EPS)
-        at = pl.ds(pl.multiple_of(n * span, span), span)
-        out_ref[at, :] = (made * gain_ref[...]).astype(out_ref.dtype)
-        return new[:size]
-
-    lax.fori_loop(0, length // span, walk, jnp.zeros((size, size), jnp.float32))
-
-
-def output_kernel(
-    stick_ref, delta_ref, sw_hbm, dw_hbm, out_ref,
-    sticks, deltas, sw_ref, dw_ref, outgoing, incoming, own,
-    a_send, a_recv, l_sem, c_send, c_recv,
-):
-    sp, tp = lax.axis_size("sp"), lax.axis_size("tp")
-    z, t = lax.axis_index("sp"), lax.axis_index("tp")
-    rows = sticks.shape[0]
-    half = rows // tp
-    pieces = ((stick_ref, sticks), (delta_ref, deltas))
-
-    def source(ref, who):
-        return ref.at[pl.ds(pl.multiple_of(who * rows, rows), rows), :]
-
-    def slot(ref):
-        cols = stick_ref.shape[1]
-        return ref.at[:, pl.ds(pl.multiple_of(z * cols, cols), cols)]
-
-    local = [
-        pltpu.make_async_copy(source(a, z), slot(b), l_sem.at[i])
-        for i, (a, b) in enumerate(pieces)
-    ]
-    local += [
-        pltpu.make_async_copy(sw_hbm, sw_ref, l_sem.at[2]),
-        pltpu.make_async_copy(dw_hbm, dw_ref, l_sem.at[3]),
-    ]
-    for c in local:
-        c.start()
-    greet(("sp", "tp"))
-    copies = []
-    for k in range(1, sp):
-        who = lax.rem(z + k, sp)
-        for i, (a, b) in enumerate(pieces):
-            c = remote(source(a, who), slot(b), a_send.at[k, i], a_recv.at[k, i], "sp", who)
-            c.start()
-            copies.append(c)
-    for c in local:
-        c.wait()
-    for c in copies:
-        c.wait_recv()
-    chunks, width = outgoing.shape[0], outgoing.shape[2]
-    mine = pl.ds(pl.multiple_of(t * half, half), half)
-    partner = lax.rem(t + 1, tp)
-    theirs = pl.ds(pl.multiple_of(partner * half, half), half)
-    sends = []
-    for c in range(chunks):
-        columns = slice(c * width, (c + 1) * width)
-        for which, target in ((theirs, outgoing), (mine, own)):
-            target[c] = (
-                jnp.dot(sticks[which, :], sw_ref[:, columns], preferred_element_type=jnp.float32)
-                + jnp.dot(
-                    deltas[which, :], dw_ref[:, columns], preferred_element_type=jnp.float32
-                )
-            ).astype(jnp.bfloat16)
-        sends.append(
-            remote(
-                outgoing.at[c], incoming.at[c], c_send.at[c], c_recv.at[c], "tp", partner
-            )
-        )
-        if c > 0:
-            sends[c - 1].start()
-    for c in copies:
-        c.wait_send()
-    sends[chunks - 1].start()
-    for c in range(chunks):
-        sends[c].wait_recv()
-        out_ref[:, c * width : (c + 1) * width] = (
-            own[c].astype(jnp.float32) + incoming[c].astype(jnp.float32)
-        ).astype(out_ref.dtype)
-    for c in sends:
-        c.wait_send()
+    stick_finished()
+    delta_finished()
 
 
 ANYWHERE = pl.BlockSpec(memory_space=pltpu.HBM)
 ON_CORE = pl.BlockSpec(memory_space=pltpu.VMEM)
+SCALARS = pl.BlockSpec(memory_space=pltpu.SMEM)
 
 
 def on_device_heads(
@@ -769,96 +866,57 @@
     decay_log_scale, decay_shift, head_gain, sb_out_w, delta_out_w,
 ):
     sp, fs, tp = lax.axis_size("sp"), lax.axis_size("fs"), lax.axis_size("tp")
-    z = lax.axis_index("sp")
     rows, half = hidden_in.shape[1:]
     width = half * tp
     length = rows * sp
     heads = decay_log_scale.shape[0]
-    sb_heads = sb_offset.shape[0] // sp
     cols = sb_query_w.shape[1] // sp
-    parts = 2
+    parts, chunks = 2, 4
+    share = rows // tp
+    blocks = length // BLOCK
     dma = pltpu.SemaphoreType.DMA
-    projected, decay_pre, write_pre, shifts = pl.pallas_call(
-        project_kernel,
-        name="project",
-        out_shape=(
-            jax.ShapeDtypeStruct((6, length, cols), jnp.bfloat16),
-            jax.ShapeDtypeStruct((length, heads), jnp.float32),
-            jax.ShapeDtypeStruct((length, heads), jnp.float32),
-            jax.ShapeDtypeStruct((sp, heads, rows), jnp.float32),
-        ),
-        in_specs=[ANYWHERE] * 10,
-        out_specs=(ON_CORE,) * 4,
+    bf16, f32 = jnp.bfloat16, jnp.float32
+    result = pl.pallas_call(
+        layer_kernel,
+        name="layer",
+        out_shape=jax.ShapeDtypeStruct((share, width), bf16),
+        in_specs=[SCALARS] * 3 + [ANYWHERE] * 10 + [ON_CORE] + [ANYWHERE] * 2,
+        out_specs=ON_CORE,
         scratch_shapes=[
-            pltpu.VMEM((sp, rows, width), jnp.bfloat16),
-            pltpu.VMEM((width, 6 * cols), jnp.bfloat16),
-            pltpu.VMEM((heads, width), jnp.bfloat16),
-            pltpu.VMEM((heads, width), jnp.bfloat16),
+            pltpu.VMEM((sp, rows, width), bf16),
+            pltpu.VMEM((width, 6 * cols), bf16),
+            pltpu.VMEM((2, heads, width), bf16),
+            pltpu.VMEM((2 * heads, rows), f32),
+            pltpu.VMEM((sp, heads, rows), f32),
+            pltpu.VMEM((3, length, cols), bf16),
+            pltpu.VMEM((length, cols), f32),
+            pltpu.VMEM((length, cols), f32),
+            pltpu.VMEM((blocks, cols + BLOCK, 2 * cols), bf16),
+            pltpu.VMEM((blocks, cols + BLOCK, cols), f32),
+            pltpu.VMEM((length, cols), bf16),
+            pltpu.VMEM((length, cols), bf16),
+            pltpu.VMEM((rows, cols * sp), bf16),
+            pltpu.VMEM((rows, cols * sp), bf16),
+            pltpu.VMEM(sb_out_w.shape, bf16),
+            pltpu.VMEM(delta_out_w.shape, bf16),
+            pltpu.VMEM((rows, width), f32),
+            pltpu.VMEM((chunks, share, width // chunks), bf16),
+            pltpu.VMEM((chunks, share, width // chunks), bf16),
+            pltpu.VMEM((chunks, share, width // chunks), bf16),
             dma((2, sp, parts)), dma((2, sp, parts)), dma((2, sp, parts)), dma((2, sp, parts)),
-            dma((fs, 6)), dma((fs, 6)), dma((sp,)), dma((sp,)), dma((4,)), dma((6,)),
+            dma((fs, 6)), dma((fs, 6)), dma((sp,)), dma((sp,)), dma((6,)), dma((6,)),
+            dma((sp, 2)), dma((sp, 2)), dma((chunks,)), dma((chunks,)),
         ],
         compiler_params=pltpu.CompilerParams(
             collective_id=0, has_side_effects=True, vmem_limit_bytes=ALL_VMEM
         ),
     )(
+        sb_offset, decay_log_scale, write_bias,
         hidden_in.reshape(rows, half), sb_query_w, sb_key_w, sb_value_w,
-        delta_query_w, delta_key_w, delta_value_w, decay_w.T, write_w.T, decay_shift.reshape(heads, rows),
-    )
-
-    def pick(a, start, count, axis):
-        return lax.dynamic_slice_in_dim(a, start, count, axis)
-
-    stick = pl.pallas_call(
-        stick_kernel,
-        name="stick",
-        grid=(sp,),
-        out_shape=jax.ShapeDtypeStruct((length, cols), jnp.bfloat16),
-        in_specs=[
-            pl.BlockSpec(memory_space=pltpu.SMEM),
-            pl.BlockSpec((3, length, cols), lambda i: (0, 0, 0)),
-        ],
-        out_specs=pl.BlockSpec((rows, cols), lambda i: (i, 0)),
-        compiler_params=pltpu.CompilerParams(vmem_limit_bytes=ALL_VMEM),
-    )(pick(sb_offset, z * sb_heads, sb_heads, 0), projected)
-    delta = pl.pallas_call(
-        delta_kernel,
-        name="delta",
-        out_shape=jax.ShapeDtypeStruct((length, cols), jnp.bfloat16),
-        in_specs=[pl.BlockSpec(memory_space=pltpu.SMEM)] * 2 + [ON_CORE] * 5,
-        out_specs=ON_CORE,
-        scratch_shapes=[
-            pltpu.VMEM((length // BLOCK, 2, cols + BLOCK, cols), jnp.bfloat16),
-            pltpu.VMEM((length // BLOCK, cols + BLOCK, cols), jnp.float32),
-            pltpu.VMEM((length, 1), jnp.float32),
-            pltpu.VMEM((length, 1), jnp.float32),
-        ],
-        compiler_params=pltpu.CompilerParams(vmem_limit_bytes=ALL_VMEM),
-    )(
-        decay_log_scale, write_bias, projected, decay_pre, write_pre, shifts,
-        head_gain.reshape(1, -1),
-    )
-    chunks = 4
-    result = pl.pallas_call(
-        output_kernel,
-        name="output",
-        out_shape=jax.ShapeDtypeStruct((rows // tp, width), jnp.bfloat16),
-        in_specs=[ON_CORE, ON_CORE, ANYWHERE, ANYWHERE],
-        out_specs=ON_CORE,
-        scratch_shapes=[
-            pltpu.VMEM((rows, cols * sp), jnp.bfloat16),
-            pltpu.VMEM((rows, cols * sp), jnp.bfloat16),
-            pltpu.VMEM(sb_out_w.shape, jnp.bfloat16),
-            pltpu.VMEM(delta_out_w.shape, jnp.bfloat16),
-            pltpu.VMEM((chunks, rows // tp, width // chunks), jnp.bfloat16),
-            pltpu.VMEM((chunks, rows // tp, width // chunks), jnp.bfloat16),
-            pltpu.VMEM((chunks, rows // tp, width // chunks), jnp.bfloat16),
-            dma((sp, 2)), dma((sp, 2)), dma((4,)), dma((chunks,)), dma((chunks,)),
-        ],
-        compiler_params=pltpu.CompilerParams(
-            collective_id=1, has_side_effects=True, vmem_limit_bytes=ALL_VMEM
-        ),
-    )(stick, delta, sb_out_w, delta_out_w)
-    return result.reshape(1, rows // tp, width)
+        delta_query_w, delta_key_w, delta_value_w, decay_w.T, write_w.T,
+        decay_shift.reshape(heads, rows), head_gain.reshape(1, -1), sb_out_w, delta_out_w,
+    )
+    return result.reshape(1, share, width)
 
 
 def on_device(*inputs):

time: 100 us -> 76.6 us (0.77)
  Pallas kernels: 96.9 us -> 74.6 us
  local copies, waits for them, and re-layouts: 3.19 us -> 1.88 us
    pallas_call x4 -> x1, Pallas kernels: 96.9 us -> 74.6 us  [on_device_heads(): pl.pallas_call(layer_kernel, name='layer', out_shape=jax.ShapeDtypeStruct...]
    dynamic_slice x1 -> x0, local copies, waits for them, and re-layouts: 1.31 us -> none  [pick(): return lax.dynamic_slice_in_dim(a, start, count, axis)]
where the time goes in v1:
time: 76.6 us; the launch traced here: 76.5 us
  Pallas kernels  74.6 us (97%)
  local copies, waits for them, and re-layouts  1.88 us (2%)
    pallas_call x1, Pallas kernels, on_device_heads(): pl.pallas_call(layer_kernel, name='layer', out_shape=jax.ShapeDtypeStruct...  74.6 us
    unnamed x1, local copies, waits for them, and re-layouts  1.88 us

profile of v1, /device:TPU:0, one launch (start us, length us, event | category | flops | bytes accessed | tf_op | source)
XLA Modules:
  0.0 76.5 jit_solution(3158025159399569705)
XLA Ops:
  0.0 74.6 %layer.1 = bf16[128,2048]{1,0:T(8,128)(2,1)} custom-call(f32[8]{0:T(128)} %offset_ref.1, f32[4]{0:T(128)} %decay_scale_ref.1, f32[4]{0:T(128)} %write_bias_ref.1, bf16[256,1024]{1,0:T(8,128)(2,1)} %bitcast.7, bf16[512,512]{1,0:T(8,128)(2,1)} %w0.1, bf16[512,512]{1,0:T(8,128)(2,1)} %w1.1, bf16[512,512]{1,0:T(8,128)(2,1)} %w2.1, bf16[512,512]{1,0:T(8,128)(2,1)} %w3.1, ...), custom_call_target="tpu_custom_call" | custom-call | tf_op jit(solution)/shard_map/layer/pallas_call | solution.py:879
  74.6 1.9 %copy.18 = bf16[1,128,2048]{2,1,0:T(8,128)(2,1)} copy(bf16[1,128,2048]{2,1,0:T(8,128)(2,1)} %bitcast.6) | data formatting | bytes 1048576

commit v2 on v1

--- a/solution.py
+++ b/solution.py
@@ -364,10 +364,11 @@
 
 
 def layer_kernel(
-    offset_ref, decay_scale_ref, write_bias_ref,
-    x_ref, w0, w1, w2, w3, w4, w5, decay_w_ref, write_w_ref, shift_ref, gain_ref, sw_hbm, dw_hbm,
+    offset_hbm, decay_scale_hbm, write_bias_hbm,
+    x_ref, w0, w1, w2, w3, w4, w5, decay_w_ref, write_w_ref, shift_ref, gain_hbm, sw_hbm, dw_hbm,
     out_ref,
-    xs, ws, gate_w, gates, shifts_ref,
+    offset_ref, decay_scale_ref, write_bias_ref, gain_ref,
+    xs, ws, gate_w, gate_all, gates, shifts_ref,
     proj, acc, later, maps, adds, stick_out, delta_out,
     sticks, deltas, sw_ref, dw_ref, partial, outgoing, incoming, own,
     x_send, x_recv, f_send, f_recv, w_send, w_recv, s_send, s_recv, l_sem, lw_sem,
@@ -387,6 +388,10 @@
         pltpu.make_async_copy(shift_ref, shifts_ref.at[z], l_sem.at[1]),
         pltpu.make_async_copy(decay_w_ref, gate_w.at[0], l_sem.at[2]),
         pltpu.make_async_copy(write_w_ref, gate_w.at[1], l_sem.at[3]),
+        pltpu.make_async_copy(offset_hbm, offset_ref, l_sem.at[6]),
+        pltpu.make_async_copy(decay_scale_hbm, decay_scale_ref, l_sem.at[7]),
+        pltpu.make_async_copy(write_bias_hbm, write_bias_ref, l_sem.at[8]),
+        pltpu.make_async_copy(gain_hbm, gain_ref, l_sem.at[9]),
     ]
     late = [
         pltpu.make_async_copy(sw_hbm, sw_ref, l_sem.at[4]),
@@ -402,13 +407,32 @@
     local += [
         pltpu.make_async_copy(w_src(i), w_at(i, f), lw_sem.at[i]) for i in range(len(weights))
     ]
+    near = (f + 1 - 2 * (f % 2), f + 2 - 4 * (f // 2))
+    count = len(weights)
+    delta_kinds, stick_kinds = (3, 4, 5), (0, 1, 2)
+
+    def onward(way):
+        return z + 1 < sp if way == 0 else z > 0
+
+    def ahead(way):
+        return z + 1 if way == 0 else z - 1
+
+    barrier = pltpu.get_barrier_semaphore()
+    for way in range(2):
+        @pl.when(onward(way))
+        def _():
+            pl.semaphore_signal(
+                barrier, inc=1, device_id={"sp": ahead(way)}, device_id_type=MESH
+            )
+    for side in range(2):
+        pl.semaphore_signal(barrier, inc=1, device_id={"fs": near[side]}, device_id_type=MESH)
+    pl.semaphore_signal(
+        barrier, inc=1, device_id={"tp": lax.rem(t + 1, tp)}, device_id_type=MESH
+    )
     for c in local:
         c.start()
-    greet(("sp", "fs", "tp"))
-
-    near = (f + 1 - 2 * (f % 2), f + 2 - 4 * (f // 2))
-    count = len(weights)
-    orders = (tuple(range(count)), tuple(range(count // 2, count)) + tuple(range(count // 2)))
+    peers = onward(0).astype(jnp.int32) + onward(1).astype(jnp.int32) + 3
+    pl.semaphore_wait(barrier, peers)
 
     def x_copy(way, step, part):
         block = z - (step - 1) if way == 0 else z + (step - 1)
@@ -416,12 +440,16 @@
         there = xs.at[block, piece, slot]
         return remote(
             x_ref.at[piece, :] if step == 1 else there, there,
-            x_send.at[way, step, part], x_recv.at[way, step, part],
-            "sp", z + 1 if way == 0 else z - 1,
+            x_send.at[way, step, part], x_recv.at[way, step, part], "sp", ahead(way),
         )
 
-    def onward(way):
-        return z + 1 < sp if way == 0 else z > 0
+    def shift_copy(way, step):
+        block = z - (step - 1) if way == 0 else z + (step - 1)
+        there = shifts_ref.at[block]
+        return remote(
+            shift_ref if step == 1 else there, there,
+            s_send.at[way, step], s_recv.at[way, step], "sp", ahead(way),
+        )
 
     def comes(way, step):
         return z >= step if way == 0 else z + step < sp
@@ -438,46 +466,36 @@
             f_send.at[way, step, part], f_recv.at[way, step, part], "tp", lax.rem(t + 1, tp),
         )
 
+    def w_copy(side, i):
+        return remote(
+            w_src(i), w_at(i, f), w_send.at[side, i], w_recv.at[side, i], "fs", near[side]
+        )
+
+    def w_relay(side, i):
+        part = depth // 2
+        start = pl.multiple_of(near[side] * depth + side * part, part)
+        there = ws.at[pl.ds(start, part), pl.ds(i * cols, cols)]
+        return remote(
+            there, there, w_send.at[2 + side, i], w_recv.at[2 + side, i], "fs", near[1 - side]
+        )
+
     for part in range(parts):
         for way in range(2):
             @pl.when(onward(way))
             def _():
                 x_copy(way, 1, part).start()
-
-    w_copies = {}
-    for order_at in range(count):
+                if part == 0:
+                    shift_copy(way, 1).start()
+    for i in delta_kinds:
         for side in range(2):
-            i = orders[side][order_at]
-            c = remote(
-                w_src(i), w_at(i, f), w_send.at[side, i], w_recv.at[side, i], "fs", near[side]
-            )
-            c.start()
-            w_copies[side, i] = c
-    s_copies = []
-    for k in range(1, sp):
-        c = remote(
-            shift_ref, shifts_ref.at[z], s_send.at[k], s_recv.at[k], "sp", lax.rem(z + k, sp)
-        )
-        c.start()
-        s_copies.append(c)
+            w_copy(side, i).start()
     for part in range(parts):
         forward(0, 0, part).start()
-    for c in late:
-        c.start()
-
-    relays = []
-
-    def relay(position):
+
+    def relay(i):
         for side in range(2):
-            i = orders[side][position]
-            w_copies[side, i].wait_recv()
-            there = w_at(i, near[side])
-            c = remote(
-                there, there, w_send.at[2 + side, i], w_recv.at[2 + side, i],
-                "fs", near[1 - side],
-            )
-            c.start()
-            relays.append(c)
+            w_copy(side, i).wait_recv()
+            w_relay(side, i).start()
 
     def arrive(step, part):
         for way in range(2):
@@ -489,25 +507,39 @@
                     @pl.when(onward(way))
                     def _():
                         x_copy(way, step + 1, part).start()
+                if part == 0:
+                    shift_copy(way, step).wait_recv()
+                    if step + 1 < sp:
+                        @pl.when(onward(way))
+                        def _():
+                            shift_copy(way, step + 1).start()
 
     early = [(step, part) for step in range(1, sp - 1) for part in range(parts)]
-    relay(0)
+    relay(delta_kinds[0])
     arrive(*early[0])
-    for position in range(1, count // 2):
-        relay(position)
-    for step, part in early[1:]:
+    for i in delta_kinds[1:]:
+        relay(i)
+    for i in stick_kinds:
+        for side in range(2):
+            w_copy(side, i).start()
+    for c in late:
+        c.start()
+    for step, part in early[1:parts]:
         arrive(step, part)
     for c in local:
         c.wait()
-    for side in range(2):
-        for position in range(count // 2, count):
-            w_copies[side, orders[side][position]].wait_recv()
-    for c in relays:
-        c.wait_recv()
-    for c in s_copies:
-        c.wait_recv()
+    gate_all[...] = jnp.concatenate(
+        [gate_w[0].astype(jnp.float32), gate_w[1].astype(jnp.float32)], axis=0
+    ).astype(jnp.bfloat16)
     for part in range(parts):
         forward(0, 0, part).wait_recv()
+
+    def relayed(kinds):
+        for i in kinds:
+            for side in range(2):
+                w_relay(side, i).wait_recv()
+
+    relayed(delta_kinds)
 
     size = offset_ref.shape[0] // sp
     sb_size = cols // size
@@ -599,10 +631,7 @@
         )
 
     def prepare(b, dq, dk, dv):
-        for side in range(2):
-            gates[side * heads : (side + 1) * heads, :] = dot_f32(
-                gate_w[side], xs[b], ((1,), (1,))
-            )
+        gates[...] = dot_f32(gate_all[...], xs[b], ((1,), (1,)))
         pre = gates[pl.ds(z, 1), :]
         write = gates[pl.ds(heads + z, 1), :] + write_bias_ref[z]
         rate = jnp.exp(jnp.full((1, rows), decay_scale_ref[z], jnp.float32))
@@ -700,84 +729,117 @@
             if step == sp - 1:
                 x_copy(way, step, part).wait_recv()
                 forward(way, step, part).start()
+                if part == 0:
+                    shift_copy(way, step).wait_recv()
         for part in range(parts):
             forward(way, step, part).wait_recv()
 
+    def give(which, out, target):
+        here = target.at[:, pl.ds(pl.multiple_of(z * cols, cols), cols)]
+
+        def send(g, k):
+            return remote(
+                out.at[at_block(g), :], here,
+                a_send.at[k, which], a_recv.at[k, which], "sp", g,
+            )
+
+        def started(g):
+            for k in range(1, sp):
+                @pl.when(lax.rem(z + k, sp) == g)
+                def _():
+                    send(lax.rem(z + k, sp), k).start()
+
+        def finished():
+            for k in range(1, sp):
+                send(lax.rem(z + k, sp), k).wait_send()
+
+        def came():
+            for k in range(1, sp):
+                send(lax.rem(z + k, sp), k).wait_recv()
+
+        return started, finished, came
+
+    stick_started, stick_finished, stick_came = give(0, stick_out, sticks)
+    delta_started, delta_finished, delta_came = give(1, delta_out, deltas)
+
     shorter = jnp.minimum(z, sp - 1 - z)
     down_last = z > sp - 1 - z
 
-    def event(n, reach):
-        lowest, highest = reach
+    def place(n):
         both = n <= 2 * shorter
         way_n = jnp.where(both, lax.rem(n + 1, 2), jnp.where(down_last, 0, 1))
         step_n = jnp.where(n == 0, 0, jnp.where(both, (n + 1) // 2, n - shorter))
+        down = jnp.logical_and(way_n == 0, n > 0)
+        return way_n, step_n, down, jnp.where(down, z - step_n, z + step_n)
+
+    def delta_event(n):
+        way_n, step_n, down, b = place(n)
         for step in range(1, sp):
             for way in range(2):
                 @pl.when(jnp.logical_and(step_n == step, way_n == way))
                 def _():
                     wait_x(way, step)
-        down = jnp.logical_and(way_n == 0, n > 0)
-        b = jnp.where(down, z - step_n, z + step_n)
-        for i in range(0, 3 * cols, 3 * cols // 3):
-            proj[i // cols, at_block(b), :] = dot_f32(
-                xs[b], ws[:, i : i + cols]
-            ).astype(jnp.bfloat16)
         drows = dot_f32(xs[b], ws[:, 3 * cols :]).astype(jnp.bfloat16).astype(jnp.float32)
         prepare(b, drows[:, :cols], drows[:, cols : 2 * cols], drows[:, 2 * cols :])
+
+    def stick_event(n, reach):
+        lowest, highest = reach
+        way_n, step_n, down, b = place(n)
+        lowest = jnp.minimum(lowest, b)
+        highest = jnp.maximum(highest, b)
+        out = dot_f32(xs[b], ws[:, : 3 * cols]).astype(jnp.bfloat16)
+        for i in range(3):
+            proj[i, at_block(b), :] = out[:, i * cols : (i + 1) * cols]
         pair(b, b, True)
+
+        def settle(i):
+            stick_out[at_block(i), :] = acc[at_block(i), :].astype(jnp.bfloat16)
+
+        first_key = b == 0
+
+        @pl.when(first_key)
+        def _():
+            settle(b)
 
         def off(m, c):
             i = jnp.where(down, b + 1 + m, b)
             j = jnp.where(down, b, b - 1 - m)
             pair(i, j, False)
+
+            @pl.when(first_key)
+            def _():
+                stick_started(i - 1)
+                settle(i)
             return c
 
-        lowest = jnp.minimum(lowest, b)
-        highest = jnp.maximum(highest, b)
         lax.fori_loop(0, highest - lowest, off, 0)
+
+        @pl.when(jnp.logical_and(lowest == 0, b > 0))
+        def _():
+            settle(b)
+
+        @pl.when(lowest == 0)
+        def _():
+            stick_started(jnp.where(first_key, highest, b))
         return lowest, highest
 
-    lax.fori_loop(0, sp, event, (z, z))
-
-    out_copies = []
-
-    def give(kind, out, target):
-        which = 0 if kind == "stick" else 1
-        here = target.at[:, pl.ds(pl.multiple_of(z * cols, cols), cols)]
-
-        def send(g, k):
-            return remote(
-                out.at[g * rows : (g + 1) * rows, :], here,
-                a_send.at[k, which], a_recv.at[k, which], "sp", g,
-            )
-
-        def started(g):
-            for k in range(1, sp):
-                @pl.when(lax.rem(z + k, sp) == g)
-                def _():
-                    send(g, k).start()
-
-        def finished():
-            for g in range(sp):
-                for k in range(1, sp):
-                    @pl.when(lax.rem(z + k, sp) == g)
-                    def _():
-                        send(g, k).wait_send()
-
-        def came():
-            for k in range(1, sp):
-                send(0, k).wait_recv()
-
-        return started, finished, came
-
-    stick_started, stick_finished, stick_came = give("stick", stick_out, sticks)
-    delta_started, delta_finished, delta_came = give("delta", delta_out, deltas)
-
-    for g in range(sp):
-        at = slice(g * rows, (g + 1) * rows)
-        stick_out[at, :] = acc[at, :].astype(jnp.bfloat16)
-        if g > 0:
-            stick_started(g - 1)
+    def early_delta(n, carry):
+        @pl.when(n == 1)
+        def _():
+            relay(stick_kinds[0])
+
+        @pl.when(n == sp - 2)
+        def _():
+            for c in early[parts:-1]:
+                arrive(*c)
+            for i in stick_kinds[1:]:
+                relay(i)
+            arrive(*early[-1])
+        delta_event(n)
+        return carry
+
+    lax.fori_loop(0, sp - 1, early_delta, 0)
+    relayed(stick_kinds)
 
     def walk(n, memory):
         high, low = halves(memory)
@@ -788,13 +850,19 @@
         delta_out[at, :] = (made * gain_ref[...]).astype(delta_out.dtype)
         return new[:width]
 
-    memory = jnp.zeros((width, width), jnp.float32)
-    for g in range(sp):
-        memory = lax.fori_loop(g * blocks, (g + 1) * blocks, walk, memory)
-        if g == 0:
-            stick_started(sp - 1)
-        else:
-            delta_started(g - 1)
+    def stick_loop(n, reach):
+        @pl.when(n == sp - 1)
+        def _():
+            delta_event(n)
+            memory = jnp.zeros((width, width), jnp.float32)
+            for g in range(sp):
+                memory = lax.fori_loop(g * blocks, (g + 1) * blocks, walk, memory)
+                if g > 0:
+                    delta_started(g - 1)
+            delta_started(sp - 1)
+        return stick_event(n, reach)
+
+    lax.fori_loop(0, sp, stick_loop, (z, z))
 
     mine_z = pl.ds(pl.multiple_of(z * rows, rows), rows)
     lanes = pl.ds(pl.multiple_of(z * cols, cols), cols)
@@ -802,7 +870,6 @@
     deltas[:, lanes] = delta_out[mine_z, :]
     for c in late:
         c.wait()
-    delta_started(sp - 1)
     stick_came()
     chunks, wide = outgoing.shape[0], outgoing.shape[2]
     share = rows // tp
@@ -838,8 +905,12 @@
             own[c].astype(jnp.float32) + incoming[c].astype(jnp.float32)
         ).astype(out_ref.dtype)
 
-    for c in list(w_copies.values()) + relays + s_copies + swaps:
+    for c in swaps:
         c.wait_send()
+    for i in range(count):
+        for side in range(2):
+            w_copy(side, i).wait_send()
+            w_relay(side, i).wait_send()
     for part in range(parts):
         forward(0, 0, part).wait_send()
         for step in range(1, sp):
@@ -847,6 +918,8 @@
                 @pl.when(sends(way, step))
                 def _():
                     x_copy(way, step, part).wait_send()
+                    if part == 0:
+                        shift_copy(way, step).wait_send()
 
                 @pl.when(comes(way, step))
                 def _():
@@ -857,7 +930,6 @@
 
 ANYWHERE = pl.BlockSpec(memory_space=pltpu.HBM)
 ON_CORE = pl.BlockSpec(memory_space=pltpu.VMEM)
-SCALARS = pl.BlockSpec(memory_space=pltpu.SMEM)
 
 
 def on_device_heads(
@@ -880,12 +952,17 @@
         layer_kernel,
         name="layer",
         out_shape=jax.ShapeDtypeStruct((share, width), bf16),
-        in_specs=[SCALARS] * 3 + [ANYWHERE] * 10 + [ON_CORE] + [ANYWHERE] * 2,
+        in_specs=[ANYWHERE] * 16,
         out_specs=ON_CORE,
         scratch_shapes=[
+            pltpu.SMEM(sb_offset.shape, f32),
+            pltpu.SMEM(decay_log_scale.shape, f32),
+            pltpu.SMEM(write_bias.shape, f32),
+            pltpu.VMEM((1, head_gain.shape[0]), f32),
             pltpu.VMEM((sp, rows, width), bf16),
             pltpu.VMEM((width, 6 * cols), bf16),
             pltpu.VMEM((2, heads, width), bf16),
+            pltpu.VMEM((2 * heads, width), bf16),
             pltpu.VMEM((2 * heads, rows), f32),
             pltpu.VMEM((sp, heads, rows), f32),
             pltpu.VMEM((3, length, cols), bf16),
@@ -904,7 +981,7 @@
             pltpu.VMEM((chunks, share, width // chunks), bf16),
             pltpu.VMEM((chunks, share, width // chunks), bf16),
             dma((2, sp, parts)), dma((2, sp, parts)), dma((2, sp, parts)), dma((2, sp, parts)),
-            dma((fs, 6)), dma((fs, 6)), dma((sp,)), dma((sp,)), dma((6,)), dma((6,)),
+            dma((fs, 6)), dma((fs, 6)), dma((2, sp)), dma((2, sp)), dma((10,)), dma((6,)),
             dma((sp, 2)), dma((sp, 2)), dma((chunks,)), dma((chunks,)),
         ],
         compiler_params=pltpu.CompilerParams(

time: 76.6 us -> 66.1 us (0.86)
  Pallas kernels: 74.6 us -> 64.1 us
    pallas_call x1, Pallas kernels: 74.6 us -> 64.1 us  [on_device_heads(): pl.pallas_call(layer_kernel, name='layer', out_shape=jax.ShapeDtypeStruct...]
where the time goes in v2:
time: 66.1 us; the launch traced here: 66 us
  Pallas kernels  64.1 us (97%)
  local copies, waits for them, and re-layouts  1.88 us (3%)
    pallas_call x1, Pallas kernels, on_device_heads(): pl.pallas_call(layer_kernel, name='layer', out_shape=jax.ShapeDtypeStruct...  64.1 us
    unnamed x1, local copies, waits for them, and re-layouts  1.88 us

profile of v2, /device:TPU:0, one launch (start us, length us, event | category | flops | bytes accessed | tf_op | source)
XLA Modules:
  0.0 66.0 jit_solution(4169736314765384567)
XLA Ops:
  0.0 64.1 %layer.1 = bf16[128,2048]{1,0:T(8,128)(2,1)} custom-call(f32[8]{0:T(128)} %offset_hbm.1, f32[4]{0:T(128)} %decay_scale_hbm.1, f32[4]{0:T(128)} %write_bias_hbm.1, bf16[256,1024]{1,0:T(8,128)(2,1)} %bitcast.7, bf16[512,512]{1,0:T(8,128)(2,1)} %w0.1, bf16[512,512]{1,0:T(8,128)(2,1)} %w1.1, bf16[512,512]{1,0:T(8,128)(2,1)} %w2.1, bf16[512,512]{1,0:T(8,128)(2,1)} %w3.1, ...), custom_call_target="tpu_custom_call" | custom-call | tf_op jit(solution)/shard_map/layer/pallas_call | solution.py:951
  64.1 1.9 %copy.18 = bf16[1,128,2048]{2,1,0:T(8,128)(2,1)} copy(bf16[1,128,2048]{2,1,0:T(8,128)(2,1)} %bitcast.6) | data formatting | bytes 1048576

commit v3 on v2

--- a/solution.py
+++ b/solution.py
@@ -366,11 +366,11 @@
 def layer_kernel(
     offset_hbm, decay_scale_hbm, write_bias_hbm,
     x_ref, w0, w1, w2, w3, w4, w5, decay_w_ref, write_w_ref, shift_ref, gain_hbm, sw_hbm, dw_hbm,
-    out_ref,
+    own, incoming,
     offset_ref, decay_scale_ref, write_bias_ref, gain_ref,
     xs, ws, gate_w, gate_all, gates, shifts_ref,
     proj, acc, later, maps, adds, stick_out, delta_out,
-    sticks, deltas, sw_ref, dw_ref, partial, outgoing, incoming, own,
+    sticks, deltas, sw_ref, dw_ref, partial, outgoing,
     x_send, x_recv, f_send, f_recv, w_send, w_recv, s_send, s_recv, l_sem, lw_sem,
     a_send, a_recv, c_send, c_recv,
 ):
@@ -552,16 +552,16 @@
     def at_block(b, start=0, extent=rows):
         return pl.ds(pl.multiple_of(b * rows + start, extent), extent)
 
-    def pair(i, j, masked):
+    def pair(i, j, masked, fresh):
         for part in range(rows // tile):
-            span = (part + 1) * tile if masked else rows
+            span = (part + 1) * tile if fresh else rows
             mine = at_block(i, part * tile, tile)
             q = proj[0, mine, :]
             keys, values = proj[1, at_block(j), :], proj[2, at_block(j), :]
             keys, values = keys[:span], values[:span]
             lane = lax.broadcasted_iota(jnp.int32, (tile, cols), 1)
             if masked:
-                seen = across[:tile, :span] < below[:tile, :span] + part * tile
+                seen = across[:tile, :span] < below[:tile, :span] + part * tile + (i - j) * rows
             mixed = total = None
             for h in range(size):
                 query = jnp.where(lane // sb_size == h, q, jnp.zeros_like(q))
@@ -580,7 +580,7 @@
                 whole = jnp.broadcast_to(beyond[:, :1] + skip[:, :1], (tile, cols))
                 mixed = part_out if h == 0 else jnp.where(lane // sb_size == h, part_out, mixed)
                 total = whole if h == 0 else jnp.where(lane // sb_size == h, whole, total)
-            if masked:
+            if fresh:
                 acc[mine, :] = mixed
                 later[mine, :] = total
             else:
@@ -782,19 +782,21 @@
         drows = dot_f32(xs[b], ws[:, 3 * cols :]).astype(jnp.bfloat16).astype(jnp.float32)
         prepare(b, drows[:, :cols], drows[:, cols : 2 * cols], drows[:, 2 * cols :])
 
+    def settle(i):
+        stick_out[at_block(i), :] = acc[at_block(i), :].astype(jnp.bfloat16)
+
+    def stick_project(b):
+        out = dot_f32(xs[b], ws[:, : 3 * cols]).astype(jnp.bfloat16)
+        for i in range(3):
+            proj[i, at_block(b), :] = out[:, i * cols : (i + 1) * cols]
+
     def stick_event(n, reach):
         lowest, highest = reach
         way_n, step_n, down, b = place(n)
         lowest = jnp.minimum(lowest, b)
         highest = jnp.maximum(highest, b)
-        out = dot_f32(xs[b], ws[:, : 3 * cols]).astype(jnp.bfloat16)
-        for i in range(3):
-            proj[i, at_block(b), :] = out[:, i * cols : (i + 1) * cols]
-        pair(b, b, True)
-
-        def settle(i):
-            stick_out[at_block(i), :] = acc[at_block(i), :].astype(jnp.bfloat16)
-
+        stick_project(b)
+        pair(b, b, True, True)
         first_key = b == 0
 
         @pl.when(first_key)
@@ -804,7 +806,7 @@
         def off(m, c):
             i = jnp.where(down, b + 1 + m, b)
             j = jnp.where(down, b, b - 1 - m)
-            pair(i, j, False)
+            pair(i, j, False, False)
 
             @pl.when(first_key)
             def _():
@@ -850,19 +852,39 @@
         delta_out[at, :] = (made * gain_ref[...]).astype(delta_out.dtype)
         return new[:width]
 
-    def stick_loop(n, reach):
-        @pl.when(n == sp - 1)
+    lax.fori_loop(0, sp - 1, stick_event, (z, z))
+
+    delta_event(sp - 1)
+    _, _, down, b = place(sp - 1)
+    stick_project(b)
+    acc[at_block(b), :] = jnp.zeros((rows, cols), jnp.float32)
+    later[at_block(b), :] = jnp.zeros((rows, cols), jnp.float32)
+
+    def last_pairs(m, memory):
+        i = jnp.where(down, m, b)
+        j = jnp.where(down, b, b - m)
+        pair(i, j, True, False)
+        for n in range(blocks):
+            memory = walk(m * blocks + n, memory)
+        delta_started(m - 1)
+
+        @pl.when(down)
         def _():
-            delta_event(n)
-            memory = jnp.zeros((width, width), jnp.float32)
-            for g in range(sp):
-                memory = lax.fori_loop(g * blocks, (g + 1) * blocks, walk, memory)
-                if g > 0:
-                    delta_started(g - 1)
-            delta_started(sp - 1)
-        return stick_event(n, reach)
-
-    lax.fori_loop(0, sp, stick_loop, (z, z))
+            stick_started(m - 1)
+            settle(i)
+        return memory
+
+    lax.fori_loop(0, sp, last_pairs, jnp.zeros((width, width), jnp.float32))
+    delta_started(sp - 1)
+
+    @pl.when(down)
+    def _():
+        stick_started(sp - 1)
+
+    @pl.when(jnp.logical_not(down))
+    def _():
+        settle(b)
+        stick_started(b)
 
     mine_z = pl.ds(pl.multiple_of(z * rows, rows), rows)
     lanes = pl.ds(pl.multiple_of(z * cols, cols), cols)
@@ -888,7 +910,10 @@
         ).astype(jnp.bfloat16)
 
     swaps = [
-        remote(outgoing.at[c], incoming.at[c], c_send.at[c], c_recv.at[c], "tp", partner)
+        remote(
+            outgoing.at[c], incoming.at[:, c * wide : (c + 1) * wide],
+            c_send.at[c], c_recv.at[c], "tp", partner,
+        )
         for c in range(chunks)
     ]
     for c in range(chunks):
@@ -896,14 +921,11 @@
         if c > 0:
             swaps[c - 1].start()
     for c in range(chunks):
-        own[c] = finish(mine, c)
+        own[:, c * wide : (c + 1) * wide] = finish(mine, c)
         if c == 0:
             swaps[chunks - 1].start()
     for c in range(chunks):
         swaps[c].wait_recv()
-        out_ref[:, c * wide : (c + 1) * wide] = (
-            own[c].astype(jnp.float32) + incoming[c].astype(jnp.float32)
-        ).astype(out_ref.dtype)
 
     for c in swaps:
         c.wait_send()
@@ -948,12 +970,12 @@
     blocks = length // BLOCK
     dma = pltpu.SemaphoreType.DMA
     bf16, f32 = jnp.bfloat16, jnp.float32
-    result = pl.pallas_call(
+    own, incoming = pl.pallas_call(
         layer_kernel,
         name="layer",
-        out_shape=jax.ShapeDtypeStruct((share, width), bf16),
+        out_shape=(pltpu.VMEM((share, width), bf16),) * 2,
         in_specs=[ANYWHERE] * 16,
-        out_specs=ON_CORE,
+        out_specs=(ON_CORE,) * 2,
         scratch_shapes=[
             pltpu.SMEM(sb_offset.shape, f32),
             pltpu.SMEM(decay_log_scale.shape, f32),
@@ -978,14 +1000,13 @@
             pltpu.VMEM(delta_out_w.shape, bf16),
             pltpu.VMEM((rows, width), f32),
             pltpu.VMEM((chunks, share, width // chunks), bf16),
-            pltpu.VMEM((chunks, share, width // chunks), bf16),
-            pltpu.VMEM((chunks, share, width // chunks), bf16),
             dma((2, sp, parts)), dma((2, sp, parts)), dma((2, sp, parts)), dma((2, sp, parts)),
             dma((fs, 6)), dma((fs, 6)), dma((2, sp)), dma((2, sp)), dma((10,)), dma((6,)),
             dma((sp, 2)), dma((sp, 2)), dma((chunks,)), dma((chunks,)),
         ],
         compiler_params=pltpu.CompilerParams(
-            collective_id=0, has_side_effects=True, vmem_limit_bytes=ALL_VMEM
+            collective_id=0, has_side_effects=True,
+            vmem_limit_bytes=ALL_VMEM - 5 * share * width,
         ),
     )(
         sb_offset, decay_log_scale, write_bias,
@@ -993,6 +1014,7 @@
         delta_query_w, delta_key_w, delta_value_w, decay_w.T, write_w.T,
         decay_shift.reshape(heads, rows), head_gain.reshape(1, -1), sb_out_w, delta_out_w,
     )
+    result = (own.astype(f32) + incoming.astype(f32)).astype(bf16)
     return result.reshape(1, share, width)
 
 

time: 66.1 us -> 63.7 us (0.964)
  the two profiles are of different devices: /device:TPU:0 before, /device:TPU:17 now
where the time goes in v3:
time: 63.7 us; the launch traced here: 63.6 us
  Pallas kernels  62.6 us (98%)
  other arithmetic  0.92 us (1%)
    pallas_call x1, Pallas kernels, on_device_heads(): pl.pallas_call(layer_kernel, name='layer', out_shape=(pltpu.VMEM((share,...  62.6 us

profile of v3, /device:TPU:17, one launch (start us, length us, event | category | flops | bytes accessed | tf_op | source)
XLA Modules:
  0.0 63.6 jit_solution(4418694328697057267)
XLA Ops:
  0.0 62.6 %layer.1 = (bf16[128,2048]{1,0:T(8,128)(2,1)S(1)}, bf16[128,2048]{1,0:T(8,128)(2,1)S(1)}) custom-call(f32[8]{0:T(128)} %offset_hbm.1, f32[4]{0:T(128)} %decay_scale_hbm.1, f32[4]{0:T(128)} %write_bias_hbm.1, bf16[256,1024]{1,0:T(8,128)(2,1)} %bitcast.7, bf16[512,512]{1,0:T(8,128)(2,1)} %w0.1, bf16[512,512]{1,0:T(8,128)(2,1)} %w1.1, bf16[512,512]{1,0:T(8,128)(2,1)} %w2.1, ...), custom_call_target="tpu_custom_call" | custom-call | tf_op jit(solution)/shard_map/layer/pallas_call | solution.py:973
  62.6 0.9 %fusion = bf16[1,128,2048]{2,1,0:T(8,128)(2,1)} fusion(bf16[128,2048]{1,0:T(8,128)(2,1)S(1)} %get-tuple-element.8, bf16[128,2048]{1,0:T(8,128)(2,1)S(1)} %get-tuple-element.7), kind=kLoop, calls=%fused_computation.1 | loop fusion | flops 1048576 | bytes 1572864 | tf_op jit(solution)/shard_map/reshape | solution.py:1018

commit v4 on v3

--- a/solution.py
+++ b/solution.py
@@ -368,7 +368,7 @@
     x_ref, w0, w1, w2, w3, w4, w5, decay_w_ref, write_w_ref, shift_ref, gain_hbm, sw_hbm, dw_hbm,
     own, incoming,
     offset_ref, decay_scale_ref, write_bias_ref, gain_ref,
-    xs, ws, gate_w, gate_all, gates, shifts_ref,
+    xs, ws, gate_w, gate_all, gates, shifts_ref, after,
     proj, acc, later, maps, adds, stick_out, delta_out,
     sticks, deltas, sw_ref, dw_ref, partial, outgoing,
     x_send, x_recv, f_send, f_recv, w_send, w_recv, s_send, s_recv, l_sem, lw_sem,
@@ -547,7 +547,8 @@
     tile = rows // 2
     below = lax.broadcasted_iota(jnp.int32, (rows, rows), 0)
     across = lax.broadcasted_iota(jnp.int32, (rows, rows), 1)
-    after = jnp.where(below > across, 1.0, 0.0).astype(jnp.bfloat16)
+    after[:, :rows] = jnp.where(below > across, 1.0, 0.0).astype(jnp.bfloat16)
+    after[:, rows:] = jnp.ones((rows, cols), jnp.bfloat16)
 
     def at_block(b, start=0, extent=rows):
         return pl.ds(pl.multiple_of(b * rows + start, extent), extent)
@@ -560,26 +561,36 @@
             keys, values = proj[1, at_block(j), :], proj[2, at_block(j), :]
             keys, values = keys[:span], values[:span]
             lane = lax.broadcasted_iota(jnp.int32, (tile, cols), 1)
+            query = jnp.concatenate(
+                [jnp.where(lane // sb_size == h, q, jnp.zeros_like(q)) for h in range(size)], axis=0
+            )
+            score = dot_f32(query, keys, ((1,), (1,)))
+            score = jnp.concatenate(
+                [
+                    score[h * tile : (h + 1) * tile] * scale + offset_ref[z * size + h]
+                    for h in range(size)
+                ],
+                axis=0,
+            )
+            skip = jnp.maximum(score, jnp.log(1.0 + jnp.exp(jnp.minimum(score, 80.0))))
+            weight = score - skip
             if masked:
                 seen = across[:tile, :span] < below[:tile, :span] + part * tile + (i - j) * rows
-            mixed = total = None
-            for h in range(size):
-                query = jnp.where(lane // sb_size == h, q, jnp.zeros_like(q))
-                score = dot_f32(query, keys, ((1,), (1,))) * scale + offset_ref[z * size + h]
-                skip = jnp.maximum(
-                    score, jnp.log(1.0 + jnp.exp(jnp.minimum(score, 80.0)))
-                )
-                weight = score - skip
-                if masked:
-                    skip = jnp.where(seen, skip, 0.0)
-                beyond = dot_f32(skip.astype(jnp.bfloat16), after[:span, :span])
-                weight = jnp.exp(weight - beyond)
-                if masked:
-                    weight = jnp.where(seen, weight, 0.0)
-                part_out = dot_f32(weight.astype(jnp.bfloat16), values)
-                whole = jnp.broadcast_to(beyond[:, :1] + skip[:, :1], (tile, cols))
-                mixed = part_out if h == 0 else jnp.where(lane // sb_size == h, part_out, mixed)
-                total = whole if h == 0 else jnp.where(lane // sb_size == h, whole, total)
+                seen = jnp.concatenate([seen] * size, axis=0)
+                skip = jnp.where(seen, skip, 0.0)
+            suffix = after[:span, :]
+            if span < rows:
+                suffix = jnp.concatenate([suffix[:, :span], suffix[:, rows:]], axis=1)
+            sums = dot_f32(skip.astype(jnp.bfloat16), suffix)
+            weight = jnp.exp(weight - sums[:, :span])
+            if masked:
+                weight = jnp.where(seen, weight, 0.0)
+            out = dot_f32(weight.astype(jnp.bfloat16), values)
+            mixed, total = out[:tile], sums[:tile, span:]
+            for h in range(1, size):
+                at = slice(h * tile, (h + 1) * tile)
+                mixed = jnp.where(lane // sb_size == h, out[at], mixed)
+                total = jnp.where(lane // sb_size == h, sums[at, span:], total)
             if fresh:
                 acc[mine, :] = mixed
                 later[mine, :] = total
@@ -726,12 +737,6 @@
 
     def wait_x(way, step):
         for part in range(parts):
-            if step == sp - 1:
-                x_copy(way, step, part).wait_recv()
-                forward(way, step, part).start()
-                if part == 0:
-                    shift_copy(way, step).wait_recv()
-        for part in range(parts):
             forward(way, step, part).wait_recv()
 
     def give(which, out, target):
@@ -771,6 +776,8 @@
         step_n = jnp.where(n == 0, 0, jnp.where(both, (n + 1) // 2, n - shorter))
         down = jnp.logical_and(way_n == 0, n > 0)
         return way_n, step_n, down, jnp.where(down, z - step_n, z + step_n)
+
+    last_way = jnp.logical_or(z == 0, z == sp - 1)
 
     def delta_event(n):
         way_n, step_n, down, b = place(n)
@@ -790,11 +797,23 @@
         for i in range(3):
             proj[i, at_block(b), :] = out[:, i * cols : (i + 1) * cols]
 
+    def stick_place(n):
+        down = n > sp - 1 - z
+        return down, jnp.where(down, sp - 1 - n, z + n)
+
     def stick_event(n, reach):
         lowest, highest = reach
-        way_n, step_n, down, b = place(n)
+        down, b = stick_place(n)
         lowest = jnp.minimum(lowest, b)
         highest = jnp.maximum(highest, b)
+
+        @pl.when(last_way)
+        def _():
+            for part in range(2):
+                @pl.when(n == sp - 3 + part)
+                def _():
+                    arrive(sp - 1, part)
+
         stick_project(b)
         pair(b, b, True, True)
         first_key = b == 0
@@ -803,14 +822,18 @@
         def _():
             settle(b)
 
+        @pl.when(jnp.logical_and(last_way, n == sp - 2))
+        def _():
+            arrive(sp - 1, 2)
+
         def off(m, c):
-            i = jnp.where(down, b + 1 + m, b)
+            i = jnp.where(down, highest - m, b)
             j = jnp.where(down, b, b - 1 - m)
             pair(i, j, False, False)
 
             @pl.when(first_key)
             def _():
-                stick_started(i - 1)
+                stick_started(jnp.where(m == 0, b, i + 1))
                 settle(i)
             return c
 
@@ -822,7 +845,7 @@
 
         @pl.when(lowest == 0)
         def _():
-            stick_started(jnp.where(first_key, highest, b))
+            stick_started(jnp.where(jnp.logical_and(first_key, highest > b), b + 1, b))
         return lowest, highest
 
     def early_delta(n, carry):
@@ -840,8 +863,8 @@
         delta_event(n)
         return carry
 
-    lax.fori_loop(0, sp - 1, early_delta, 0)
-    relayed(stick_kinds)
+    events = jnp.where(last_way, sp - 1, sp)
+    lax.fori_loop(0, events, early_delta, 0)
 
     def walk(n, memory):
         high, low = halves(memory)
@@ -852,39 +875,55 @@
         delta_out[at, :] = (made * gain_ref[...]).astype(delta_out.dtype)
         return new[:width]
 
-    lax.fori_loop(0, sp - 1, stick_event, (z, z))
-
-    delta_event(sp - 1)
-    _, _, down, b = place(sp - 1)
-    stick_project(b)
-    acc[at_block(b), :] = jnp.zeros((rows, cols), jnp.float32)
-    later[at_block(b), :] = jnp.zeros((rows, cols), jnp.float32)
-
-    def last_pairs(m, memory):
-        i = jnp.where(down, m, b)
-        j = jnp.where(down, b, b - m)
-        pair(i, j, True, False)
+    def walk_group(g, memory):
         for n in range(blocks):
-            memory = walk(m * blocks + n, memory)
-        delta_started(m - 1)
+            memory = walk(g * blocks + n, memory)
+        delta_started(g - 1)
+        return memory
+
+    empty = jnp.zeros((width, width), jnp.float32)
+
+    @pl.when(jnp.logical_not(last_way))
+    def _():
+        lax.fori_loop(0, sp, walk_group, empty)
+        delta_started(sp - 1)
+
+    relayed(stick_kinds)
+    lax.fori_loop(0, events, stick_event, (z, z))
+
+    @pl.when(last_way)
+    def _():
+        for part in range(3, parts):
+            arrive(sp - 1, part)
+        delta_event(sp - 1)
+        down, b = stick_place(sp - 1)
+        stick_project(b)
+        acc[at_block(b), :] = jnp.zeros((rows, cols), jnp.float32)
+        later[at_block(b), :] = jnp.zeros((rows, cols), jnp.float32)
+
+        def last_pairs(m, memory):
+            i = jnp.where(down, m, b)
+            j = jnp.where(down, b, b - m)
+            pair(i, j, True, False)
+            memory = walk_group(m, memory)
+
+            @pl.when(down)
+            def _():
+                stick_started(m - 1)
+                settle(i)
+            return memory
+
+        lax.fori_loop(0, sp, last_pairs, empty)
+        delta_started(sp - 1)
 
         @pl.when(down)
         def _():
-            stick_started(m - 1)
-            settle(i)
-        return memory
-
-    lax.fori_loop(0, sp, last_pairs, jnp.zeros((width, width), jnp.float32))
-    delta_started(sp - 1)
-
-    @pl.when(down)
-    def _():
-        stick_started(sp - 1)
-
-    @pl.when(jnp.logical_not(down))
-    def _():
-        settle(b)
-        stick_started(b)
+            stick_started(sp - 1)
+
+        @pl.when(jnp.logical_not(down))
+        def _():
+            settle(b)
+            stick_started(b)
 
     mine_z = pl.ds(pl.multiple_of(z * rows, rows), rows)
     lanes = pl.ds(pl.multiple_of(z * cols, cols), cols)
@@ -965,7 +1004,7 @@
     length = rows * sp
     heads = decay_log_scale.shape[0]
     cols = sb_query_w.shape[1] // sp
-    parts, chunks = 2, 4
+    parts, chunks = 4, 4
     share = rows // tp
     blocks = length // BLOCK
     dma = pltpu.SemaphoreType.DMA
@@ -987,6 +1026,7 @@
             pltpu.VMEM((2 * heads, width), bf16),
             pltpu.VMEM((2 * heads, rows), f32),
             pltpu.VMEM((sp, heads, rows), f32),
+            pltpu.VMEM((rows, rows + cols), bf16),
             pltpu.VMEM((3, length, cols), bf16),
             pltpu.VMEM((length, cols), f32),
             pltpu.VMEM((length, cols), f32),

time: 63.7 us -> 63.1 us (level)
  the two profiles are of different devices: /device:TPU:17 before, /device:TPU:0 now
where the time goes in v4:
time: 63.1 us; the launch traced here: 62.9 us
  Pallas kernels  62 us (98%)
  other arithmetic  0.92 us (1%)
    pallas_call x1, Pallas kernels, on_device_heads(): pl.pallas_call(layer_kernel, name='layer', out_shape=(pltpu.VMEM((share,...  62 us

profile of v4, /device:TPU:0, one launch (start us, length us, event | category | flops | bytes accessed | tf_op | source)
XLA Modules:
  0.0 62.9 jit_solution(4226926557643013900)
XLA Ops:
  0.0 62.0 %layer.1 = (bf16[128,2048]{1,0:T(8,128)(2,1)S(1)}, bf16[128,2048]{1,0:T(8,128)(2,1)S(1)}) custom-call(f32[8]{0:T(128)} %offset_hbm.1, f32[4]{0:T(128)} %decay_scale_hbm.1, f32[4]{0:T(128)} %write_bias_hbm.1, bf16[256,1024]{1,0:T(8,128)(2,1)} %bitcast.7, bf16[512,512]{1,0:T(8,128)(2,1)} %w0.1, bf16[512,512]{1,0:T(8,128)(2,1)} %w1.1, bf16[512,512]{1,0:T(8,128)(2,1)} %w2.1, ...), custom_call_target="tpu_custom_call" | custom-call | tf_op jit(solution)/shard_map/layer/pallas_call | solution.py:1012
  62.0 0.9 %fusion = bf16[1,128,2048]{2,1,0:T(8,128)(2,1)} fusion(bf16[128,2048]{1,0:T(8,128)(2,1)S(1)} %get-tuple-element.8, bf16[128,2048]{1,0:T(8,128)(2,1)S(1)} %get-tuple-element.7), kind=kLoop, calls=%fused_computation.1 | loop fusion | flops 1048576 | bytes 1572864 | tf_op jit(solution)/shard_map/reshape | solution.py:1058

commit v5 on v4

--- a/solution.py
+++ b/solution.py
@@ -369,10 +369,10 @@
     own, incoming,
     offset_ref, decay_scale_ref, write_bias_ref, gain_ref,
     xs, ws, gate_w, gate_all, gates, shifts_ref, after,
-    proj, acc, later, maps, adds, stick_out, delta_out,
+    proj, acc, later, memory_ref, maps, adds, stick_out, delta_out,
     sticks, deltas, sw_ref, dw_ref, partial, outgoing,
-    x_send, x_recv, f_send, f_recv, w_send, w_recv, s_send, s_recv, l_sem, lw_sem,
-    a_send, a_recv, c_send, c_recv,
+    x_send, x_recv, f_send, f_recv, w_send, w_recv, r_recv, s_send, s_recv, l_sem,
+    a_send, a_recv, c_sem,
 ):
     weights = (w0, w1, w2, w3, w4, w5)
     sp, tp = lax.axis_size("sp"), lax.axis_size("tp")
@@ -380,7 +380,7 @@
     rows, half = x_ref.shape
     depth = w0.shape[0]
     cols = ws.shape[1] // len(weights)
-    parts = x_send.shape[2]
+    parts = x_recv.shape[2]
     heads = decay_w_ref.shape[0]
     slot = pl.ds(pl.multiple_of(t * half, half), half)
     local = [
@@ -404,8 +404,8 @@
     def w_at(i, who):
         return ws.at[pl.ds(pl.multiple_of(who * depth, depth), depth), pl.ds(i * cols, cols)]
 
-    local += [
-        pltpu.make_async_copy(w_src(i), w_at(i, f), lw_sem.at[i]) for i in range(len(weights))
+    local_w = [
+        pltpu.make_async_copy(w_src(i), w_at(i, f), l_sem.at[10]) for i in range(len(weights))
     ]
     near = (f + 1 - 2 * (f % 2), f + 2 - 4 * (f // 2))
     count = len(weights)
@@ -429,7 +429,7 @@
     pl.semaphore_signal(
         barrier, inc=1, device_id={"tp": lax.rem(t + 1, tp)}, device_id_type=MESH
     )
-    for c in local:
+    for c in local + local_w:
         c.start()
     peers = onward(0).astype(jnp.int32) + onward(1).astype(jnp.int32) + 3
     pl.semaphore_wait(barrier, peers)
@@ -440,7 +440,7 @@
         there = xs.at[block, piece, slot]
         return remote(
             x_ref.at[piece, :] if step == 1 else there, there,
-            x_send.at[way, step, part], x_recv.at[way, step, part], "sp", ahead(way),
+            x_send.at[way], x_recv.at[way, step - 1, part], "sp", ahead(way),
         )
 
     def shift_copy(way, step):
@@ -448,7 +448,7 @@
         there = shifts_ref.at[block]
         return remote(
             shift_ref if step == 1 else there, there,
-            s_send.at[way, step], s_recv.at[way, step], "sp", ahead(way),
+            s_send.at[way], s_recv.at[way, step - 1], "sp", ahead(way),
         )
 
     def comes(way, step):
@@ -463,12 +463,12 @@
         there = xs.at[block, piece, slot]
         return remote(
             x_ref.at[piece, :] if step == 0 else there, there,
-            f_send.at[way, step, part], f_recv.at[way, step, part], "tp", lax.rem(t + 1, tp),
+            f_send.at[0], f_recv.at[way * (sp - 1) + step], "tp", lax.rem(t + 1, tp),
         )
 
     def w_copy(side, i):
         return remote(
-            w_src(i), w_at(i, f), w_send.at[side, i], w_recv.at[side, i], "fs", near[side]
+            w_src(i), w_at(i, f), w_send.at[0], w_recv.at[side, i], "fs", near[side]
         )
 
     def w_relay(side, i):
@@ -476,7 +476,7 @@
         start = pl.multiple_of(near[side] * depth + side * part, part)
         there = ws.at[pl.ds(start, part), pl.ds(i * cols, cols)]
         return remote(
-            there, there, w_send.at[2 + side, i], w_recv.at[2 + side, i], "fs", near[1 - side]
+            there, there, w_send.at[0], r_recv.at[i // 3], "fs", near[1 - side]
         )
 
     for part in range(parts):
@@ -528,16 +528,25 @@
         arrive(step, part)
     for c in local:
         c.wait()
+    own_w = ws.at[pl.ds(pl.multiple_of(f * depth, depth), depth), :]
+    pltpu.make_async_copy(own_w, own_w, l_sem.at[10]).wait()
     gate_all[...] = jnp.concatenate(
         [gate_w[0].astype(jnp.float32), gate_w[1].astype(jnp.float32)], axis=0
     ).astype(jnp.bfloat16)
-    for part in range(parts):
-        forward(0, 0, part).wait_recv()
+    def all_sent(ref, sem):
+        remote(ref, ref, sem, sem, "tp", lax.rem(t + 1, tp)).wait_send()
+
+    def all_came(ref, sem):
+        remote(ref, ref, sem, sem, "tp", lax.rem(t + 1, tp)).wait_recv()
+
+    def block_came(way, step):
+        all_came(xs.at[z, :, slot], f_recv.at[way * (sp - 1) + step])
+
+    block_came(0, 0)
 
     def relayed(kinds):
-        for i in kinds:
-            for side in range(2):
-                w_relay(side, i).wait_recv()
+        first = kinds[0] * cols
+        all_came(ws.at[pl.ds(0, depth), pl.ds(first, len(kinds) * cols)], r_recv.at[kinds[0] // 3])
 
     relayed(delta_kinds)
 
@@ -736,8 +745,7 @@
                 adds[n] = mine[:, :width]
 
     def wait_x(way, step):
-        for part in range(parts):
-            forward(way, step, part).wait_recv()
+        block_came(way, step)
 
     def give(which, out, target):
         here = target.at[:, pl.ds(pl.multiple_of(z * cols, cols), cols)]
@@ -745,7 +753,7 @@
         def send(g, k):
             return remote(
                 out.at[at_block(g), :], here,
-                a_send.at[k, which], a_recv.at[k, which], "sp", g,
+                a_send.at[which], a_recv.at[which], "sp", g,
             )
 
         def started(g):
@@ -754,18 +762,13 @@
                 def _():
                     send(lax.rem(z + k, sp), k).start()
 
-        def finished():
-            for k in range(1, sp):
-                send(lax.rem(z + k, sp), k).wait_send()
-
         def came():
-            for k in range(1, sp):
-                send(lax.rem(z + k, sp), k).wait_recv()
-
-        return started, finished, came
-
-    stick_started, stick_finished, stick_came = give(0, stick_out, sticks)
-    delta_started, delta_finished, delta_came = give(1, delta_out, deltas)
+            all_came(out.at[pl.ds(0, (sp - 1) * rows), :], a_recv.at[which])
+
+        return started, came
+
+    stick_started, stick_came = give(0, stick_out, sticks)
+    delta_started, delta_came = give(1, delta_out, deltas)
 
     shorter = jnp.minimum(z, sp - 1 - z)
     down_last = z > sp - 1 - z
@@ -786,6 +789,9 @@
                 @pl.when(jnp.logical_and(step_n == step, way_n == way))
                 def _():
                     wait_x(way, step)
+        delta_block(b)
+
+    def delta_block(b):
         drows = dot_f32(xs[b], ws[:, 3 * cols :]).astype(jnp.bfloat16).astype(jnp.float32)
         prepare(b, drows[:, :cols], drows[:, cols : 2 * cols], drows[:, 2 * cols :])
 
@@ -875,18 +881,25 @@
         delta_out[at, :] = (made * gain_ref[...]).astype(delta_out.dtype)
         return new[:width]
 
-    def walk_group(g, memory):
-        for n in range(blocks):
-            memory = walk(g * blocks + n, memory)
-        delta_started(g - 1)
-        return memory
-
-    empty = jnp.zeros((width, width), jnp.float32)
+    def walk_groups(start, stop):
+        def group(g, c):
+            @pl.when(g > start)
+            def _():
+                delta_started(g - 1)
+            memory = memory_ref[...]
+            for n in range(blocks):
+                memory = walk(g * blocks + n, memory)
+            memory_ref[...] = memory
+            return c
+
+        lax.fori_loop(start, stop, group, 0)
+        delta_started(stop - 1)
+
+    memory_ref[...] = jnp.zeros((width, width), jnp.float32)
 
     @pl.when(jnp.logical_not(last_way))
     def _():
-        lax.fori_loop(0, sp, walk_group, empty)
-        delta_started(sp - 1)
+        walk_groups(0, sp)
 
     relayed(stick_kinds)
     lax.fori_loop(0, events, stick_event, (z, z))
@@ -895,35 +908,42 @@
     def _():
         for part in range(3, parts):
             arrive(sp - 1, part)
-        delta_event(sp - 1)
+        walked = jnp.where(z == 0, sp - 1, 0)
+
+        @pl.when(z == 0)
+        def _():
+            walk_groups(0, sp - 1)
+        for way in range(2):
+            @pl.when(comes(way, sp - 1))
+            def _():
+                block_came(way, sp - 1)
         down, b = stick_place(sp - 1)
         stick_project(b)
         acc[at_block(b), :] = jnp.zeros((rows, cols), jnp.float32)
         later[at_block(b), :] = jnp.zeros((rows, cols), jnp.float32)
 
-        def last_pairs(m, memory):
+        def last_pairs(m, c):
             i = jnp.where(down, m, b)
             j = jnp.where(down, b, b - m)
-            pair(i, j, True, False)
-            memory = walk_group(m, memory)
 
             @pl.when(down)
             def _():
                 stick_started(m - 1)
+            pair(i, j, True, False)
+
+            @pl.when(down)
+            def _():
                 settle(i)
-            return memory
-
-        lax.fori_loop(0, sp, last_pairs, empty)
-        delta_started(sp - 1)
-
-        @pl.when(down)
-        def _():
-            stick_started(sp - 1)
+            return c
+
+        lax.fori_loop(0, sp, last_pairs, 0)
 
         @pl.when(jnp.logical_not(down))
         def _():
             settle(b)
             stick_started(b)
+        delta_block(b)
+        walk_groups(walked, sp)
 
     mine_z = pl.ds(pl.multiple_of(z * rows, rows), rows)
     lanes = pl.ds(pl.multiple_of(z * cols, cols), cols)
@@ -951,7 +971,7 @@
     swaps = [
         remote(
             outgoing.at[c], incoming.at[:, c * wide : (c + 1) * wide],
-            c_send.at[c], c_recv.at[c], "tp", partner,
+            c_sem.at[0], c_sem.at[1], "tp", partner,
         )
         for c in range(chunks)
     ]
@@ -963,30 +983,19 @@
         own[:, c * wide : (c + 1) * wide] = finish(mine, c)
         if c == 0:
             swaps[chunks - 1].start()
-    for c in range(chunks):
-        swaps[c].wait_recv()
-
-    for c in swaps:
-        c.wait_send()
-    for i in range(count):
-        for side in range(2):
-            w_copy(side, i).wait_send()
-            w_relay(side, i).wait_send()
-    for part in range(parts):
-        forward(0, 0, part).wait_send()
-        for step in range(1, sp):
-            for way in range(2):
-                @pl.when(sends(way, step))
-                def _():
-                    x_copy(way, step, part).wait_send()
-                    if part == 0:
-                        shift_copy(way, step).wait_send()
-
-                @pl.when(comes(way, step))
-                def _():
-                    forward(way, step, part).wait_send()
-    stick_finished()
-    delta_finished()
+    all_came(incoming, c_sem.at[1])
+    all_sent(incoming, c_sem.at[0])
+    all_sent(ws.at[pl.ds(0, 3 * depth), :], w_send.at[0])
+    all_sent(xs.at[:, :, slot], f_send.at[0])
+    for which, out in enumerate((stick_out, delta_out)):
+        all_sent(out.at[pl.ds(0, (sp - 1) * rows), :], a_send.at[which])
+    for c in range(sp):
+        @pl.when(z == c)
+        def _():
+            for way, passed in enumerate((c + 1 if c + 1 < sp else 0, sp - c if c > 0 else 0)):
+                if passed:
+                    all_sent(xs.at[pl.ds(0, passed), :, slot], x_send.at[way])
+                    all_sent(shifts_ref.at[pl.ds(0, passed)], s_send.at[way])
 
 
 ANYWHERE = pl.BlockSpec(memory_space=pltpu.HBM)
@@ -1030,6 +1039,7 @@
             pltpu.VMEM((3, length, cols), bf16),
             pltpu.VMEM((length, cols), f32),
             pltpu.VMEM((length, cols), f32),
+            pltpu.VMEM((cols, cols), f32),
             pltpu.VMEM((blocks, cols + BLOCK, 2 * cols), bf16),
             pltpu.VMEM((blocks, cols + BLOCK, cols), f32),
             pltpu.VMEM((length, cols), bf16),
@@ -1040,9 +1050,9 @@
             pltpu.VMEM(delta_out_w.shape, bf16),
             pltpu.VMEM((rows, width), f32),
             pltpu.VMEM((chunks, share, width // chunks), bf16),
-            dma((2, sp, parts)), dma((2, sp, parts)), dma((2, sp, parts)), dma((2, sp, parts)),
-            dma((fs, 6)), dma((fs, 6)), dma((2, sp)), dma((2, sp)), dma((10,)), dma((6,)),
-            dma((sp, 2)), dma((sp, 2)), dma((chunks,)), dma((chunks,)),
+            dma((2,)), dma((2, sp - 1, parts)), dma((1,)), dma((2 * sp - 1,)),
+            dma((1,)), dma((2, 6)), dma((2,)), dma((2,)), dma((2, sp - 1)), dma((11,)),
+            dma((2,)), dma((2,)), dma((2,)),
         ],
         compiler_params=pltpu.CompilerParams(
             collective_id=0, has_side_effects=True,

time: 63.1 us -> 59.3 us (0.940)
  Pallas kernels: 62 us -> 58.2 us
    pallas_call x1, Pallas kernels: 62 us -> 58.2 us  [on_device_heads(): pl.pallas_call(layer_kernel, name='layer', out_shape=(pltpu.VMEM((share,...]
where the time goes in v5:
time: 59.3 us; the launch traced here: 59.1 us
  Pallas kernels  58.2 us (98%)
  other arithmetic  0.92 us (2%)
    pallas_call x1, Pallas kernels, on_device_heads(): pl.pallas_call(layer_kernel, name='layer', out_shape=(pltpu.VMEM((share,...  58.2 us

profile of v5, /device:TPU:0, one launch (start us, length us, event | category | flops | bytes accessed | tf_op | source)
XLA Modules:
  0.0 59.1 jit_solution(1421467786430117744)
XLA Ops:
  0.0 58.2 %layer.1 = (bf16[128,2048]{1,0:T(8,128)(2,1)S(1)}, bf16[128,2048]{1,0:T(8,128)(2,1)S(1)}) custom-call(f32[8]{0:T(128)} %offset_hbm.1, f32[4]{0:T(128)} %decay_scale_hbm.1, f32[4]{0:T(128)} %write_bias_hbm.1, bf16[256,1024]{1,0:T(8,128)(2,1)} %bitcast.7, bf16[512,512]{1,0:T(8,128)(2,1)} %w0.1, bf16[512,512]{1,0:T(8,128)(2,1)} %w1.1, bf16[512,512]{1,0:T(8,128)(2,1)} %w2.1, ...), custom_call_target="tpu_custom_call" | custom-call | tf_op jit(solution)/shard_map/layer/pallas_call | solution.py:1021
  58.2 0.9 %fusion = bf16[1,128,2048]{2,1,0:T(8,128)(2,1)} fusion(bf16[128,2048]{1,0:T(8,128)(2,1)S(1)} %get-tuple-element.8, bf16[128,2048]{1,0:T(8,128)(2,1)S(1)} %get-tuple-element.7), kind=kLoop, calls=%fused_computation.1 | loop fusion | flops 1048576 | bytes 1572864 | tf_op jit(solution)/shard_map/reshape | solution.py:1068

commit v6 on v5

--- a/solution.py
+++ b/solution.py
@@ -514,6 +514,13 @@
                         def _():
                             shift_copy(way, step + 1).start()
 
+    below = lax.broadcasted_iota(jnp.int32, (rows, rows), 0)
+    across = lax.broadcasted_iota(jnp.int32, (rows, rows), 1)
+    after[:, :rows] = jnp.where(below > across, 1.0, 0.0).astype(jnp.bfloat16)
+    after[:, rows:] = jnp.ones((rows, cols), jnp.bfloat16)
+    acc[...] = jnp.zeros_like(acc)
+    later[...] = jnp.zeros_like(later)
+    memory_ref[...] = jnp.zeros_like(memory_ref)
     early = [(step, part) for step in range(1, sp - 1) for part in range(parts)]
     relay(delta_kinds[0])
     arrive(*early[0])
@@ -554,21 +561,15 @@
     sb_size = cols // size
     scale = sb_size ** (-0.5)
     tile = rows // 2
-    below = lax.broadcasted_iota(jnp.int32, (rows, rows), 0)
-    across = lax.broadcasted_iota(jnp.int32, (rows, rows), 1)
-    after[:, :rows] = jnp.where(below > across, 1.0, 0.0).astype(jnp.bfloat16)
-    after[:, rows:] = jnp.ones((rows, cols), jnp.bfloat16)
 
     def at_block(b, start=0, extent=rows):
         return pl.ds(pl.multiple_of(b * rows + start, extent), extent)
 
-    def pair(i, j, masked, fresh):
+    def pair(i, j):
         for part in range(rows // tile):
-            span = (part + 1) * tile if fresh else rows
             mine = at_block(i, part * tile, tile)
             q = proj[0, mine, :]
             keys, values = proj[1, at_block(j), :], proj[2, at_block(j), :]
-            keys, values = keys[:span], values[:span]
             lane = lax.broadcasted_iota(jnp.int32, (tile, cols), 1)
             query = jnp.concatenate(
                 [jnp.where(lane // sb_size == h, q, jnp.zeros_like(q)) for h in range(size)], axis=0
@@ -583,30 +584,20 @@
             )
             skip = jnp.maximum(score, jnp.log(1.0 + jnp.exp(jnp.minimum(score, 80.0))))
             weight = score - skip
-            if masked:
-                seen = across[:tile, :span] < below[:tile, :span] + part * tile + (i - j) * rows
-                seen = jnp.concatenate([seen] * size, axis=0)
-                skip = jnp.where(seen, skip, 0.0)
-            suffix = after[:span, :]
-            if span < rows:
-                suffix = jnp.concatenate([suffix[:, :span], suffix[:, rows:]], axis=1)
-            sums = dot_f32(skip.astype(jnp.bfloat16), suffix)
-            weight = jnp.exp(weight - sums[:, :span])
-            if masked:
-                weight = jnp.where(seen, weight, 0.0)
+            seen = across[:tile] < below[:tile] + (part * tile + (i - j) * rows)
+            seen = jnp.concatenate([seen] * size, axis=0)
+            skip = jnp.where(seen, skip, 0.0)
+            sums = dot_f32(skip.astype(jnp.bfloat16), after[...])
+            weight = jnp.where(seen, jnp.exp(weight - sums[:, :rows]), 0.0)
             out = dot_f32(weight.astype(jnp.bfloat16), values)
-            mixed, total = out[:tile], sums[:tile, span:]
+            mixed, total = out[:tile], sums[:tile, rows:]
             for h in range(1, size):
                 at = slice(h * tile, (h + 1) * tile)
                 mixed = jnp.where(lane // sb_size == h, out[at], mixed)
-                total = jnp.where(lane // sb_size == h, sums[at, span:], total)
-            if fresh:
-                acc[mine, :] = mixed
-                later[mine, :] = total
-            else:
-                passed = later[mine, :]
-                acc[mine, :] = acc[mine, :] + mixed * jnp.exp(-passed)
-                later[mine, :] = passed + total
+                total = jnp.where(lane // sb_size == h, sums[at, rows:], total)
+            passed = later[mine, :]
+            acc[mine, :] = acc[mine, :] + mixed * jnp.exp(-passed)
+            later[mine, :] = passed + total
 
     span = BLOCK
     duo = 2 * span
@@ -707,16 +698,20 @@
             near_q = jnp.where(first, gram[duo : duo + span], gram[duo + span :])
             strict = jnp.where(strictly, near_k * table * scale_col, 0.0)
             work.append([unit - strict, strict, near_q * table])
+        yield
         for w in work:
             w[1] = squared(w[1], w[1])
         levels = max(1, (span - 1).bit_length()) - 1
         for level in range(levels):
+            if level == levels // 2:
+                yield
             for w in work:
                 if level + 1 < levels:
                     both = squared(jnp.concatenate([w[1], w[0]], axis=0), w[1])
                     w[1], w[0] = both[:span], w[0] + both[span:]
                 else:
                     w[0] = w[0] + squared(w[0], w[1])
+        yield
         for duo_at, (inverse, _, inside) in enumerate(work):
             lo = duo_at * duo
             here = slice(lo, lo + duo)
@@ -744,9 +739,6 @@
                 maps[n, :, width:] = low
                 adds[n] = mine[:, :width]
 
-    def wait_x(way, step):
-        block_came(way, step)
-
     def give(which, out, target):
         here = target.at[:, pl.ds(pl.multiple_of(z * cols, cols), cols)]
 
@@ -782,23 +774,21 @@
 
     last_way = jnp.logical_or(z == 0, z == sp - 1)
 
-    def delta_event(n):
+    def block_ready(n):
         way_n, step_n, down, b = place(n)
         for step in range(1, sp):
             for way in range(2):
                 @pl.when(jnp.logical_and(step_n == step, way_n == way))
                 def _():
-                    wait_x(way, step)
-        delta_block(b)
+                    block_came(way, step)
+        return b
 
     def delta_block(b):
         drows = dot_f32(xs[b], ws[:, 3 * cols :]).astype(jnp.bfloat16).astype(jnp.float32)
-        prepare(b, drows[:, :cols], drows[:, cols : 2 * cols], drows[:, 2 * cols :])
-
-    def settle(i):
-        stick_out[at_block(i), :] = acc[at_block(i), :].astype(jnp.bfloat16)
-
-    def stick_project(b):
+        return prepare(b, drows[:, :cols], drows[:, cols : 2 * cols], drows[:, 2 * cols :])
+
+    def stick_project(n):
+        b = stick_place(n)[1]
         out = dot_f32(xs[b], ws[:, : 3 * cols]).astype(jnp.bfloat16)
         for i in range(3):
             proj[i, at_block(b), :] = out[:, i * cols : (i + 1) * cols]
@@ -807,79 +797,30 @@
         down = n > sp - 1 - z
         return down, jnp.where(down, sp - 1 - n, z + n)
 
-    def stick_event(n, reach):
-        lowest, highest = reach
+    def settle(i):
+        stick_out[at_block(i), :] = acc[at_block(i), :].astype(jnp.bfloat16)
+
+    def stick_pair(p):
+        n = sum(((p >= e * (e + 1) // 2) * 1 for e in range(1, sp)), 0)
+        r = p - n * (n + 1) // 2
         down, b = stick_place(n)
-        lowest = jnp.minimum(lowest, b)
-        highest = jnp.maximum(highest, b)
-
-        @pl.when(last_way)
+        other = jnp.where(z == sp - 1, b + r, sp - r)
+        i = jnp.where(jnp.logical_and(down, r > 0), other, b)
+        j = jnp.where(down, b, b - r)
+        pair(i, j)
+
+        @pl.when(j == 0)
         def _():
-            for part in range(2):
-                @pl.when(n == sp - 3 + part)
-                def _():
-                    arrive(sp - 1, part)
-
-        stick_project(b)
-        pair(b, b, True, True)
-        first_key = b == 0
-
-        @pl.when(first_key)
-        def _():
-            settle(b)
-
-        @pl.when(jnp.logical_and(last_way, n == sp - 2))
-        def _():
-            arrive(sp - 1, 2)
-
-        def off(m, c):
-            i = jnp.where(down, highest - m, b)
-            j = jnp.where(down, b, b - 1 - m)
-            pair(i, j, False, False)
-
-            @pl.when(first_key)
-            def _():
-                stick_started(jnp.where(m == 0, b, i + 1))
-                settle(i)
-            return c
-
-        lax.fori_loop(0, highest - lowest, off, 0)
-
-        @pl.when(jnp.logical_and(lowest == 0, b > 0))
-        def _():
-            settle(b)
-
-        @pl.when(lowest == 0)
-        def _():
-            stick_started(jnp.where(jnp.logical_and(first_key, highest > b), b + 1, b))
-        return lowest, highest
-
-    def early_delta(n, carry):
+            settle(i)
+            stick_started(i)
+
+    def plain_delta(n, c):
         @pl.when(n == 1)
         def _():
             relay(stick_kinds[0])
-
-        @pl.when(n == sp - 2)
-        def _():
-            for c in early[parts:-1]:
-                arrive(*c)
-            for i in stick_kinds[1:]:
-                relay(i)
-            arrive(*early[-1])
-        delta_event(n)
-        return carry
-
-    events = jnp.where(last_way, sp - 1, sp)
-    lax.fori_loop(0, events, early_delta, 0)
-
-    def walk(n, memory):
-        high, low = halves(memory)
-        new = folded(dot_f32(maps[n], wide_rhs(high, low, 1))) + adds[n]
-        made = new[width:]
-        made = made * lax.rsqrt(jnp.mean(made * made, axis=-1, keepdims=True) + NORM_EPS)
-        at = pl.ds(pl.multiple_of(n * span, span), span)
-        delta_out[at, :] = (made * gain_ref[...]).astype(delta_out.dtype)
-        return new[:width]
+        for _ in delta_block(block_ready(n)):
+            pass
+        return c
 
     def walk_groups(start, stop):
         def group(g, c):
@@ -895,55 +836,83 @@
         lax.fori_loop(start, stop, group, 0)
         delta_started(stop - 1)
 
-    memory_ref[...] = jnp.zeros((width, width), jnp.float32)
+    def walk(n, memory):
+        high, low = halves(memory)
+        new = folded(dot_f32(maps[n], wide_rhs(high, low, 1))) + adds[n]
+        made = new[width:]
+        made = made * lax.rsqrt(jnp.mean(made * made, axis=-1, keepdims=True) + NORM_EPS)
+        at = pl.ds(pl.multiple_of(n * span, span), span)
+        delta_out[at, :] = (made * gain_ref[...]).astype(delta_out.dtype)
+        return new[:width]
+
+    last_way = jnp.logical_or(z == 0, z == sp - 1)
+
+    lax.fori_loop(0, 2, plain_delta, 0)
+    for c in early[parts:-1]:
+        arrive(*c)
+    for i in stick_kinds[1:]:
+        relay(i)
+    arrive(*early[-1])
+    block_ready(2)
+    relayed(stick_kinds)
 
     @pl.when(jnp.logical_not(last_way))
     def _():
-        walk_groups(0, sp)
-
-    relayed(stick_kinds)
-    lax.fori_loop(0, events, stick_event, (z, z))
-
-    @pl.when(last_way)
+        block_ready(sp - 1)
+
+    def project_each(n, c):
+        stick_project(n)
+        return c
+
+    lax.fori_loop(0, jnp.where(last_way, sp - 1, sp), project_each, 0)
+    before = sp * (sp - 1) // 2
+
+    def stream(start, stop):
+        def one(p, c):
+            stick_pair(p)
+            return c
+
+        lax.fori_loop(start, stop, one, 0)
+
+    def both(n, c):
+        final = jnp.logical_and(last_way, n == sp - 1)
+
+        @pl.when(final)
+        def _():
+            arrive(sp - 1, 0)
+            stream(sp * (sp - 3), before - 1)
+            arrive(sp - 1, 1)
+            arrive(sp - 1, 2)
+            stream(before - 1, before)
+
+            @pl.when(z == 0)
+            def _():
+                walk_groups(0, sp - 2)
+            for part in range(3, parts):
+                arrive(sp - 1, part)
+
+            @pl.when(z == 0)
+            def _():
+                walk_groups(sp - 2, sp - 1)
+            for way in range(2):
+                @pl.when(comes(way, sp - 1))
+                def _():
+                    block_came(way, sp - 1)
+            stick_project(sp - 1)
+        stages = delta_block(place(n)[3])
+        first = jnp.where(final, before, (n - 2) * sp)
+        for u in range(sp):
+            next(stages, None)
+            stick_pair(first + u)
+        return c
+
+    lax.fori_loop(2, sp, both, 0)
+
+    @pl.when(jnp.logical_not(last_way))
     def _():
-        for part in range(3, parts):
-            arrive(sp - 1, part)
-        walked = jnp.where(z == 0, sp - 1, 0)
-
-        @pl.when(z == 0)
-        def _():
-            walk_groups(0, sp - 1)
-        for way in range(2):
-            @pl.when(comes(way, sp - 1))
-            def _():
-                block_came(way, sp - 1)
-        down, b = stick_place(sp - 1)
-        stick_project(b)
-        acc[at_block(b), :] = jnp.zeros((rows, cols), jnp.float32)
-        later[at_block(b), :] = jnp.zeros((rows, cols), jnp.float32)
-
-        def last_pairs(m, c):
-            i = jnp.where(down, m, b)
-            j = jnp.where(down, b, b - m)
-
-            @pl.when(down)
-            def _():
-                stick_started(m - 1)
-            pair(i, j, True, False)
-
-            @pl.when(down)
-            def _():
-                settle(i)
-            return c
-
-        lax.fori_loop(0, sp, last_pairs, 0)
-
-        @pl.when(jnp.logical_not(down))
-        def _():
-            settle(b)
-            stick_started(b)
-        delta_block(b)
-        walk_groups(walked, sp)
+        stream(sp * (sp - 2), before + sp)
+
+    walk_groups(jnp.where(z == 0, sp - 1, 0), sp)
 
     mine_z = pl.ds(pl.multiple_of(z * rows, rows), rows)
     lanes = pl.ds(pl.multiple_of(z * cols, cols), cols)
@@ -1070,7 +1039,7 @@
 
 def on_device(*inputs):
     delta_heads = inputs[11].shape[0]
-    square = lax.axis_size("fs") == 4 and lax.axis_size("tp") == 2
+    square = lax.axis_size("sp") == lax.axis_size("fs") == 4 and lax.axis_size("tp") == 2
     if square and delta_heads == lax.axis_size("sp") and inputs[4].shape[0] % delta_heads == 0:
         return on_device_heads(*inputs)
     return on_device_split(*inputs)

time: 59.3 us -> 61.7 us (1.040)
  Pallas kernels: 58.2 us -> 60.6 us
    pallas_call x1, Pallas kernels: 58.2 us -> 60.6 us  [on_device_heads(): pl.pallas_call(layer_kernel, name='layer', out_shape=(pltpu.VMEM((share,...]
where the time goes in v6:
time: 61.7 us; the launch traced here: 61.5 us
  Pallas kernels  60.6 us (98%)
  other arithmetic  0.92 us (1%)
    pallas_call x1, Pallas kernels, on_device_heads(): pl.pallas_call(layer_kernel, name='layer', out_shape=(pltpu.VMEM((share,...  60.6 us

profile of v6, /device:TPU:0, one launch (start us, length us, event | category | flops | bytes accessed | tf_op | source)
XLA Modules:
  0.0 61.5 jit_solution(4592049361372600282)
XLA Ops:
  0.0 60.6 %layer.1 = (bf16[128,2048]{1,0:T(8,128)(2,1)S(1)}, bf16[128,2048]{1,0:T(8,128)(2,1)S(1)}) custom-call(f32[8]{0:T(128)} %offset_hbm.1, f32[4]{0:T(128)} %decay_scale_hbm.1, f32[4]{0:T(128)} %write_bias_hbm.1, bf16[256,1024]{1,0:T(8,128)(2,1)} %bitcast.7, bf16[512,512]{1,0:T(8,128)(2,1)} %w0.1, bf16[512,512]{1,0:T(8,128)(2,1)} %w1.1, bf16[512,512]{1,0:T(8,128)(2,1)} %w2.1, ...), custom_call_target="tpu_custom_call" | custom-call | tf_op jit(solution)/shard_map/layer/pallas_call | solution.py:990
  60.6 0.9 %fusion = bf16[1,128,2048]{2,1,0:T(8,128)(2,1)} fusion(bf16[128,2048]{1,0:T(8,128)(2,1)S(1)} %get-tuple-element.8, bf16[128,2048]{1,0:T(8,128)(2,1)S(1)} %get-tuple-element.7), kind=kLoop, calls=%fused_computation.1 | loop fusion | flops 1048576 | bytes 1572864 | tf_op jit(solution)/shard_map/reshape | solution.py:1037

commit v7 on v6

--- a/solution.py
+++ b/solution.py
@@ -794,8 +794,8 @@
             proj[i, at_block(b), :] = out[:, i * cols : (i + 1) * cols]
 
     def stick_place(n):
-        down = n > sp - 1 - z
-        return down, jnp.where(down, sp - 1 - n, z + n)
+        down = z == sp - 1
+        return down, jnp.where(down, sp - 1 - n, n)
 
     def settle(i):
         stick_out[at_block(i), :] = acc[at_block(i), :].astype(jnp.bfloat16)
@@ -804,8 +804,7 @@
         n = sum(((p >= e * (e + 1) // 2) * 1 for e in range(1, sp)), 0)
         r = p - n * (n + 1) // 2
         down, b = stick_place(n)
-        other = jnp.where(z == sp - 1, b + r, sp - r)
-        i = jnp.where(jnp.logical_and(down, r > 0), other, b)
+        i = jnp.where(down, b + r, b)
         j = jnp.where(down, b, b - r)
         pair(i, j)
 
@@ -818,13 +817,21 @@
         @pl.when(n == 1)
         def _():
             relay(stick_kinds[0])
+
+        @pl.when(n == sp - 2)
+        def _():
+            for c in early[parts:-1]:
+                arrive(*c)
+            for i in stick_kinds[1:]:
+                relay(i)
+            arrive(*early[-1])
         for _ in delta_block(block_ready(n)):
             pass
         return c
 
-    def walk_groups(start, stop):
+    def walk_groups(start, stop, held=False):
         def group(g, c):
-            @pl.when(g > start)
+            @pl.when(g > start + held)
             def _():
                 delta_started(g - 1)
             memory = memory_ref[...]
@@ -847,72 +854,55 @@
 
     last_way = jnp.logical_or(z == 0, z == sp - 1)
 
-    lax.fori_loop(0, 2, plain_delta, 0)
-    for c in early[parts:-1]:
-        arrive(*c)
-    for i in stick_kinds[1:]:
-        relay(i)
-    arrive(*early[-1])
-    block_ready(2)
-    relayed(stick_kinds)
+    before = sp * (sp - 1) // 2
+    events = jnp.where(last_way, sp - 1, sp)
+    lax.fori_loop(0, events, plain_delta, 0)
 
     @pl.when(jnp.logical_not(last_way))
     def _():
-        block_ready(sp - 1)
-
-    def project_each(n, c):
+        walk_groups(0, sp, held=True)
+
+    relayed(stick_kinds)
+
+    def stick_event(n, c):
+        for part in range(2):
+            @pl.when(jnp.logical_and(last_way, n == part + 1))
+            def _():
+                arrive(sp - 1, part)
+
+        @pl.when(jnp.logical_and(jnp.logical_not(last_way), n == 1))
+        def _():
+            delta_started(0)
         stick_project(n)
-        return c
-
-    lax.fori_loop(0, jnp.where(last_way, sp - 1, sp), project_each, 0)
-    before = sp * (sp - 1) // 2
-
-    def stream(start, stop):
+
         def one(p, c):
+            for part in range(2, parts):
+                @pl.when(jnp.logical_and(last_way, p == before - parts + part))
+                def _():
+                    arrive(sp - 1, part)
             stick_pair(p)
             return c
 
-        lax.fori_loop(start, stop, one, 0)
-
-    def both(n, c):
-        final = jnp.logical_and(last_way, n == sp - 1)
-
-        @pl.when(final)
+        first = n * (n + 1) // 2
+        return lax.fori_loop(first, first + n + 1, one, c)
+
+    lax.fori_loop(0, events, stick_event, 0)
+
+    @pl.when(last_way)
+    def _():
+        @pl.when(z == 0)
         def _():
-            arrive(sp - 1, 0)
-            stream(sp * (sp - 3), before - 1)
-            arrive(sp - 1, 1)
-            arrive(sp - 1, 2)
-            stream(before - 1, before)
-
-            @pl.when(z == 0)
+            walk_groups(0, sp - 1)
+        for way in range(2):
+            @pl.when(comes(way, sp - 1))
             def _():
-                walk_groups(0, sp - 2)
-            for part in range(3, parts):
-                arrive(sp - 1, part)
-
-            @pl.when(z == 0)
-            def _():
-                walk_groups(sp - 2, sp - 1)
-            for way in range(2):
-                @pl.when(comes(way, sp - 1))
-                def _():
-                    block_came(way, sp - 1)
-            stick_project(sp - 1)
-        stages = delta_block(place(n)[3])
-        first = jnp.where(final, before, (n - 2) * sp)
+                block_came(way, sp - 1)
+        stick_project(sp - 1)
+        stages = delta_block(stick_place(sp - 1)[1])
         for u in range(sp):
             next(stages, None)
-            stick_pair(first + u)
-        return c
-
-    lax.fori_loop(2, sp, both, 0)
-
-    @pl.when(jnp.logical_not(last_way))
-    def _():
-        stream(sp * (sp - 2), before + sp)
-
-    walk_groups(jnp.where(z == 0, sp - 1, 0), sp)
+            stick_pair(before + u)
+        walk_groups(jnp.where(z == 0, sp - 1, 0), sp)
 
     mine_z = pl.ds(pl.multiple_of(z * rows, rows), rows)
     lanes = pl.ds(pl.multiple_of(z * cols, cols), cols)

time: 61.7 us -> 58.4 us (0.947)
  Pallas kernels: 60.6 us -> 56.7 us
    pallas_call x1, Pallas kernels: 60.6 us -> 56.7 us  [on_device_heads(): pl.pallas_call(layer_kernel, name='layer', out_shape=(pltpu.VMEM((share,...]
where the time goes in v7:
time: 58.4 us; the launch traced here: 57.6 us
  Pallas kernels  56.7 us (97%)
  other arithmetic  0.92 us (2%)
    pallas_call x1, Pallas kernels, on_device_heads(): pl.pallas_call(layer_kernel, name='layer', out_shape=(pltpu.VMEM((share,...  56.7 us

profile of v7, /device:TPU:0, one launch (start us, length us, event | category | flops | bytes accessed | tf_op | source)
XLA Modules:
  0.0 57.6 jit_solution(4914279900867046407)
XLA Ops:
  0.0 56.7 %layer.1 = (bf16[128,2048]{1,0:T(8,128)(2,1)S(1)}, bf16[128,2048]{1,0:T(8,128)(2,1)S(1)}) custom-call(f32[8]{0:T(128)} %offset_hbm.1, f32[4]{0:T(128)} %decay_scale_hbm.1, f32[4]{0:T(128)} %write_bias_hbm.1, bf16[256,1024]{1,0:T(8,128)(2,1)} %bitcast.7, bf16[512,512]{1,0:T(8,128)(2,1)} %w0.1, bf16[512,512]{1,0:T(8,128)(2,1)} %w1.1, bf16[512,512]{1,0:T(8,128)(2,1)} %w2.1, ...), custom_call_target="tpu_custom_call" | custom-call | tf_op jit(solution)/shard_map/layer/pallas_call | solution.py:980
  56.7 0.9 %fusion = bf16[1,128,2048]{2,1,0:T(8,128)(2,1)} fusion(bf16[128,2048]{1,0:T(8,128)(2,1)S(1)} %get-tuple-element.8, bf16[128,2048]{1,0:T(8,128)(2,1)S(1)} %get-tuple-element.7), kind=kLoop, calls=%fused_computation.1 | loop fusion | flops 1048576 | bytes 1572864 | tf_op jit(solution)/shard_map/reshape | solution.py:1027

commit v8 on v7

--- a/solution.py
+++ b/solution.py
@@ -742,25 +742,36 @@
     def give(which, out, target):
         here = target.at[:, pl.ds(pl.multiple_of(z * cols, cols), cols)]
 
-        def send(g, k):
+        def send(g, k, sem):
             return remote(
                 out.at[at_block(g), :], here,
-                a_send.at[which], a_recv.at[which], "sp", g,
+                a_send.at[which], a_recv.at[sem], "sp", g,
             )
 
         def started(g):
             for k in range(1, sp):
-                @pl.when(lax.rem(z + k, sp) == g)
-                def _():
-                    send(lax.rem(z + k, sp), k).start()
-
-        def came():
-            all_came(out.at[pl.ds(0, (sp - 1) * rows), :], a_recv.at[which])
-
-        return started, came
-
-    stick_started, stick_came = give(0, stick_out, sticks)
-    delta_started, delta_came = give(1, delta_out, deltas)
+                there = lax.rem(z + k, sp)
+                if which == 0:
+                    @pl.when(there == g)
+                    def _():
+                        send(there, k, 0).start()
+                else:
+                    slow = jnp.logical_or(
+                        z == sp - 1, jnp.logical_and(z == 0, there == sp - 1)
+                    )
+
+                    @pl.when(jnp.logical_and(there == g, slow))
+                    def _():
+                        send(there, k, 2).start()
+
+                    @pl.when(jnp.logical_and(there == g, jnp.logical_not(slow)))
+                    def _():
+                        send(there, k, 1).start()
+
+        return started
+
+    stick_started = give(0, stick_out, sticks)
+    delta_started = give(1, delta_out, deltas)
 
     shorter = jnp.minimum(z, sp - 1 - z)
     down_last = z > sp - 1 - z
@@ -787,47 +798,34 @@
         drows = dot_f32(xs[b], ws[:, 3 * cols :]).astype(jnp.bfloat16).astype(jnp.float32)
         return prepare(b, drows[:, :cols], drows[:, cols : 2 * cols], drows[:, 2 * cols :])
 
+    last_way = jnp.logical_or(z == 0, z == sp - 1)
+    from_top = z == sp - 1
+
     def stick_project(n):
-        b = stick_place(n)[1]
+        b = jnp.where(from_top, sp - 1 - n, n)
         out = dot_f32(xs[b], ws[:, : 3 * cols]).astype(jnp.bfloat16)
         for i in range(3):
             proj[i, at_block(b), :] = out[:, i * cols : (i + 1) * cols]
 
     def stick_place(n):
-        down = z == sp - 1
-        return down, jnp.where(down, sp - 1 - n, n)
+        between = jnp.where(
+            n == 0, sp - 1, jnp.where(n == 1, 0, jnp.where(n == 2, sp - 1 - z, z))
+        )
+        return jnp.where(from_top, sp - 1 - n, jnp.where(last_way, n, between))
 
     def settle(i):
         stick_out[at_block(i), :] = acc[at_block(i), :].astype(jnp.bfloat16)
 
-    def stick_pair(p):
-        n = sum(((p >= e * (e + 1) // 2) * 1 for e in range(1, sp)), 0)
-        r = p - n * (n + 1) // 2
-        down, b = stick_place(n)
-        i = jnp.where(down, b + r, b)
-        j = jnp.where(down, b, b - r)
+    def stick_pair(n, r):
+        b = stick_place(n)
+        i = jnp.where(from_top, b + r, b)
+        j = jnp.where(from_top, b, b - r)
         pair(i, j)
 
         @pl.when(j == 0)
         def _():
             settle(i)
             stick_started(i)
-
-    def plain_delta(n, c):
-        @pl.when(n == 1)
-        def _():
-            relay(stick_kinds[0])
-
-        @pl.when(n == sp - 2)
-        def _():
-            for c in early[parts:-1]:
-                arrive(*c)
-            for i in stick_kinds[1:]:
-                relay(i)
-            arrive(*early[-1])
-        for _ in delta_block(block_ready(n)):
-            pass
-        return c
 
     def walk_groups(start, stop, held=False):
         def group(g, c):
@@ -852,9 +850,26 @@
         delta_out[at, :] = (made * gain_ref[...]).astype(delta_out.dtype)
         return new[:width]
 
-    last_way = jnp.logical_or(z == 0, z == sp - 1)
-
-    before = sp * (sp - 1) // 2
+    def plain_delta(n, c):
+        @pl.when(n == 1)
+        def _():
+            relay(stick_kinds[0])
+
+        @pl.when(n == sp - 2)
+        def _():
+            for c in early[parts:-1]:
+                arrive(*c)
+            relay(stick_kinds[1])
+
+            @pl.when(z == 0)
+            def _():
+                walk_groups(0, 2)
+            relay(stick_kinds[2])
+            arrive(*early[-1])
+        for _ in delta_block(block_ready(n)):
+            pass
+        return c
+
     events = jnp.where(last_way, sp - 1, sp)
     lax.fori_loop(0, events, plain_delta, 0)
 
@@ -870,21 +885,32 @@
             def _():
                 arrive(sp - 1, part)
 
-        @pl.when(jnp.logical_and(jnp.logical_not(last_way), n == 1))
+        def project_one(m, c):
+            stick_project(m)
+            return c
+
+        all_now = jnp.where(n == 0, sp, 0)
+        lax.fori_loop(
+            jnp.where(last_way, n, 0), jnp.where(last_way, n + 1, all_now), project_one, 0
+        )
+
+        @pl.when(jnp.logical_and(jnp.logical_not(last_way), n == 0))
         def _():
             delta_started(0)
-        stick_project(n)
-
-        def one(p, c):
+
+        def one(r, c):
             for part in range(2, parts):
-                @pl.when(jnp.logical_and(last_way, p == before - parts + part))
+                @pl.when(
+                    jnp.logical_and(
+                        last_way, jnp.logical_and(n == sp - 2, r == sp - 1 - parts + part)
+                    )
+                )
                 def _():
                     arrive(sp - 1, part)
-            stick_pair(p)
+            stick_pair(n, r)
             return c
 
-        first = n * (n + 1) // 2
-        return lax.fori_loop(first, first + n + 1, one, c)
+        return lax.fori_loop(0, jnp.where(last_way, n, stick_place(n)) + 1, one, c)
 
     lax.fori_loop(0, events, stick_event, 0)
 
@@ -892,16 +918,16 @@
     def _():
         @pl.when(z == 0)
         def _():
-            walk_groups(0, sp - 1)
+            walk_groups(2, sp - 1)
         for way in range(2):
             @pl.when(comes(way, sp - 1))
             def _():
                 block_came(way, sp - 1)
         stick_project(sp - 1)
-        stages = delta_block(stick_place(sp - 1)[1])
+        stages = delta_block(stick_place(sp - 1))
         for u in range(sp):
             next(stages, None)
-            stick_pair(before + u)
+            stick_pair(sp - 1, u)
         walk_groups(jnp.where(z == 0, sp - 1, 0), sp)
 
     mine_z = pl.ds(pl.multiple_of(z * rows, rows), rows)
@@ -910,13 +936,28 @@
     deltas[:, lanes] = delta_out[mine_z, :]
     for c in late:
         c.wait()
-    stick_came()
+    all_sent(ws.at[pl.ds(0, 3 * depth), :], w_send.at[0])
+    all_sent(xs.at[:, :, slot], f_send.at[0])
+    for c in range(sp):
+        @pl.when(z == c)
+        def _():
+            for way, passed in enumerate((c + 1 if c + 1 < sp else 0, sp - c if c > 0 else 0)):
+                if passed:
+                    all_sent(xs.at[pl.ds(0, passed), :, slot], x_send.at[way])
+                    all_sent(shifts_ref.at[pl.ds(0, passed)], s_send.at[way])
+    all_came(stick_out.at[pl.ds(0, (sp - 1) * rows), :], a_recv.at[0])
     chunks, wide = outgoing.shape[0], outgoing.shape[2]
     share = rows // tp
     for c in range(chunks):
         columns = slice(c * wide, (c + 1) * wide)
         partial[:, columns] = dot_f32(sticks[...], sw_ref[:, columns])
-    delta_came()
+    all_came(delta_out.at[pl.ds(0, (sp - 2) * rows), :], a_recv.at[1])
+    soon = pl.ds(pl.multiple_of(jnp.where(from_top, 1, 0) * cols, cols), (sp - 1) * cols)
+    for c in range(chunks):
+        columns = slice(c * wide, (c + 1) * wide)
+        partial[:, columns] += dot_f32(deltas[:, soon], dw_ref[soon, columns])
+    all_came(delta_out.at[pl.ds(0, rows), :], a_recv.at[2])
+    final = pl.ds(pl.multiple_of(jnp.where(from_top, 0, sp - 1) * cols, cols), cols)
     mine = pl.ds(pl.multiple_of(t * share, share), share)
     partner = lax.rem(t + 1, tp)
     theirs = pl.ds(pl.multiple_of(partner * share, share), share)
@@ -924,7 +965,7 @@
     def finish(which, c):
         columns = slice(c * wide, (c + 1) * wide)
         return (
-            partial[which, columns] + dot_f32(deltas[which, :], dw_ref[:, columns])
+            partial[which, columns] + dot_f32(deltas[which, final], dw_ref[final, columns])
         ).astype(jnp.bfloat16)
 
     swaps = [
@@ -944,17 +985,8 @@
             swaps[chunks - 1].start()
     all_came(incoming, c_sem.at[1])
     all_sent(incoming, c_sem.at[0])
-    all_sent(ws.at[pl.ds(0, 3 * depth), :], w_send.at[0])
-    all_sent(xs.at[:, :, slot], f_send.at[0])
     for which, out in enumerate((stick_out, delta_out)):
         all_sent(out.at[pl.ds(0, (sp - 1) * rows), :], a_send.at[which])
-    for c in range(sp):
-        @pl.when(z == c)
-        def _():
-            for way, passed in enumerate((c + 1 if c + 1 < sp else 0, sp - c if c > 0 else 0)):
-                if passed:
-                    all_sent(xs.at[pl.ds(0, passed), :, slot], x_send.at[way])
-                    all_sent(shifts_ref.at[pl.ds(0, passed)], s_send.at[way])
 
 
 ANYWHERE = pl.BlockSpec(memory_space=pltpu.HBM)
@@ -1011,7 +1043,7 @@
             pltpu.VMEM((chunks, share, width // chunks), bf16),
             dma((2,)), dma((2, sp - 1, parts)), dma((1,)), dma((2 * sp - 1,)),
             dma((1,)), dma((2, 6)), dma((2,)), dma((2,)), dma((2, sp - 1)), dma((11,)),
-            dma((2,)), dma((2,)), dma((2,)),
+            dma((2,)), dma((3,)), dma((2,)),
         ],
         compiler_params=pltpu.CompilerParams(
             collective_id=0, has_side_effects=True,

time: 58.4 us -> 58.6 us (level)
  no operation moved by 1% of the time
where the time goes in v8:
time: 58.6 us; the launch traced here: 57.5 us
  Pallas kernels  56.5 us (96%)
  other arithmetic  0.92 us (2%)
    pallas_call x1, Pallas kernels, on_device_heads(): pl.pallas_call(layer_kernel, name='layer', out_shape=(pltpu.VMEM((share,...  56.5 us

profile of v8, /device:TPU:0, one launch (start us, length us, event | category | flops | bytes accessed | tf_op | source)
XLA Modules:
  0.0 57.5 jit_solution(15391617201346302536)
XLA Ops:
  0.0 56.5 %layer.1 = (bf16[128,2048]{1,0:T(8,128)(2,1)S(1)}, bf16[128,2048]{1,0:T(8,128)(2,1)S(1)}) custom-call(f32[8]{0:T(128)} %offset_hbm.1, f32[4]{0:T(128)} %decay_scale_hbm.1, f32[4]{0:T(128)} %write_bias_hbm.1, bf16[256,1024]{1,0:T(8,128)(2,1)} %bitcast.7, bf16[512,512]{1,0:T(8,128)(2,1)} %w0.1, bf16[512,512]{1,0:T(8,128)(2,1)} %w1.1, bf16[512,512]{1,0:T(8,128)(2,1)} %w2.1, ...), custom_call_target="tpu_custom_call" | custom-call | tf_op jit(solution)/shard_map/layer/pallas_call | solution.py:1012
  56.5 0.9 %fusion = bf16[1,128,2048]{2,1,0:T(8,128)(2,1)} fusion(bf16[128,2048]{1,0:T(8,128)(2,1)S(1)} %get-tuple-element.8, bf16[128,2048]{1,0:T(8,128)(2,1)S(1)} %get-tuple-element.7), kind=kLoop, calls=%fused_computation.1 | loop fusion | flops 1048576 | bytes 1572864 | tf_op jit(solution)/shard_map/reshape | solution.py:1059

commit v9 on v8

--- a/solution.py
+++ b/solution.py
@@ -808,8 +808,15 @@
             proj[i, at_block(b), :] = out[:, i * cols : (i + 1) * cols]
 
     def stick_place(n):
+        lower = z < sp // 2
         between = jnp.where(
-            n == 0, sp - 1, jnp.where(n == 1, 0, jnp.where(n == 2, sp - 1 - z, z))
+            n == 0,
+            jnp.where(lower, sp - 1, 0),
+            jnp.where(
+                n == 1,
+                jnp.where(lower, sp - 2, 1),
+                jnp.where(n == 2, jnp.where(lower, 0, sp - 1), z),
+            ),
         )
         return jnp.where(from_top, sp - 1 - n, jnp.where(last_way, n, between))
 
@@ -889,10 +896,8 @@
             stick_project(m)
             return c
 
-        all_now = jnp.where(n == 0, sp, 0)
-        lax.fori_loop(
-            jnp.where(last_way, n, 0), jnp.where(last_way, n + 1, all_now), project_one, 0
-        )
+        needed = jnp.where(from_top, n, stick_place(n)) + 1
+        lax.fori_loop(c, needed, project_one, 0)
 
         @pl.when(jnp.logical_and(jnp.logical_not(last_way), n == 0))
         def _():
@@ -910,7 +915,8 @@
             stick_pair(n, r)
             return c
 
-        return lax.fori_loop(0, jnp.where(last_way, n, stick_place(n)) + 1, one, c)
+        lax.fori_loop(0, jnp.where(last_way, n, stick_place(n)) + 1, one, 0)
+        return jnp.maximum(c, needed)
 
     lax.fori_loop(0, events, stick_event, 0)
 

time: 58.6 us -> 57.5 us (0.981); the launches traced: 57.5 us -> 57.4 us
  no operation moved by 1% of the time
where the time goes in v9:
time: 57.5 us; the launch traced here: 57.4 us
  Pallas kernels  56.4 us (98%)
  other arithmetic  0.92 us (2%)
    pallas_call x1, Pallas kernels, on_device_heads(): pl.pallas_call(layer_kernel, name='layer', out_shape=(pltpu.VMEM((share,...  56.4 us

profile of v9, /device:TPU:0, one launch (start us, length us, event | category | flops | bytes accessed | tf_op | source)
XLA Modules:
  0.0 57.4 jit_solution(11595252316667534797)
XLA Ops:
  0.0 56.4 %layer.1 = (bf16[128,2048]{1,0:T(8,128)(2,1)S(1)}, bf16[128,2048]{1,0:T(8,128)(2,1)S(1)}) custom-call(f32[8]{0:T(128)} %offset_hbm.1, f32[4]{0:T(128)} %decay_scale_hbm.1, f32[4]{0:T(128)} %write_bias_hbm.1, bf16[256,1024]{1,0:T(8,128)(2,1)} %bitcast.7, bf16[512,512]{1,0:T(8,128)(2,1)} %w0.1, bf16[512,512]{1,0:T(8,128)(2,1)} %w1.1, bf16[512,512]{1,0:T(8,128)(2,1)} %w2.1, ...), custom_call_target="tpu_custom_call" | custom-call | tf_op jit(solution)/shard_map/layer/pallas_call | solution.py:1018
  56.4 0.9 %fusion = bf16[1,128,2048]{2,1,0:T(8,128)(2,1)} fusion(bf16[128,2048]{1,0:T(8,128)(2,1)S(1)} %get-tuple-element.8, bf16[128,2048]{1,0:T(8,128)(2,1)S(1)} %get-tuple-element.7), kind=kLoop, calls=%fused_computation.1 | loop fusion | flops 1048576 | bytes 1572864 | tf_op jit(solution)/shard_map/reshape | solution.py:1065

commit v10 on v9

--- a/solution.py
+++ b/solution.py
@@ -457,13 +457,18 @@
     def sends(way, step):
         return jnp.logical_and(onward(way), comes(way, step - 1))
 
+    def f_slot(way, step, part):
+        if step == sp - 1 and part < parts // 2:
+            return 2 * sp - 1 + way
+        return way * (sp - 1) + step
+
     def forward(way, step, part):
         block = z - step if way == 0 else z + step
         piece = pl.ds(part * (rows // parts), rows // parts)
         there = xs.at[block, piece, slot]
         return remote(
             x_ref.at[piece, :] if step == 0 else there, there,
-            f_send.at[0], f_recv.at[way * (sp - 1) + step], "tp", lax.rem(t + 1, tp),
+            f_send.at[0], f_recv.at[f_slot(way, step, part)], "tp", lax.rem(t + 1, tp),
         )
 
     def w_copy(side, i):
@@ -547,7 +552,11 @@
         remote(ref, ref, sem, sem, "tp", lax.rem(t + 1, tp)).wait_recv()
 
     def block_came(way, step):
-        all_came(xs.at[z, :, slot], f_recv.at[way * (sp - 1) + step])
+        extent = rows // 2 if step == sp - 1 else rows
+        all_came(xs.at[z, pl.ds(0, extent), slot], f_recv.at[way * (sp - 1) + step])
+
+    def half_came(way):
+        all_came(xs.at[z, pl.ds(0, rows // 2), slot], f_recv.at[2 * sp - 1 + way])
 
     block_came(0, 0)
 
@@ -641,27 +650,29 @@
             )
         )
 
-    def prepare(b, dq, dk, dv):
-        gates[...] = dot_f32(gate_all[...], xs[b], ((1,), (1,)))
-        pre = gates[pl.ds(z, 1), :]
-        write = gates[pl.ds(heads + z, 1), :] + write_bias_ref[z]
-        rate = jnp.exp(jnp.full((1, rows), decay_scale_ref[z], jnp.float32))
+    def prepare(b, dq, dk, dv, begin, extent):
+        lanes_at = slice(begin, begin + extent)
+        order = eighth[:, :extent]
+        gates[:, lanes_at] = dot_f32(gate_all[...], xs[b, lanes_at, :], ((1,), (1,)))
+        pre = gates[pl.ds(z, 1), :][:, lanes_at]
+        write = gates[pl.ds(heads + z, 1), :][:, lanes_at] + write_bias_ref[z]
+        rate = jnp.exp(jnp.full((1, extent), decay_scale_ref[z], jnp.float32))
         soft = jnp.maximum(pre, 0.0) + jnp.log(1.0 + jnp.exp(-jnp.abs(pre)))
-        decay = shifts_ref[b, pl.ds(z, 1), :] - rate * soft
+        decay = shifts_ref[b, pl.ds(z, 1), :][:, lanes_at] - rate * soft
         strength = 1.0 / (1.0 + jnp.exp(-write))
         d1 = decay.astype(jnp.bfloat16).astype(jnp.float32)
         d2 = (decay - d1).astype(jnp.bfloat16).astype(jnp.float32)
         d3 = decay - d1 - d2
         three = jnp.where(
-            eighth == 0, d1, jnp.where(eighth == 1, d2, jnp.where(eighth == 2, d3, 0.0))
+            order == 0, d1, jnp.where(order == 1, d2, jnp.where(order == 2, d3, 0.0))
         ).astype(jnp.bfloat16)
-        cum_row = jnp.sum(dot_f32(three, upto), axis=0, keepdims=True)
-        rest_row = jnp.sum(dot_f32(three, beyond_it), axis=0, keepdims=True)
+        cum_row = jnp.sum(dot_f32(three, upto[:extent, :extent]), axis=0, keepdims=True)
+        rest_row = jnp.sum(dot_f32(three, beyond_it[:extent, :extent]), axis=0, keepdims=True)
         stack = jnp.where(
-            eighth == 0, strength,
+            order == 0, strength,
             jnp.where(
-                eighth == 1, jnp.exp(cum_row),
-                jnp.where(eighth == 2, jnp.exp(rest_row), cum_row),
+                order == 1, jnp.exp(cum_row),
+                jnp.where(order == 2, jnp.exp(rest_row), cum_row),
             ),
         )
         columns = stack.T
@@ -675,7 +686,7 @@
         kh, kl = halves(k)
         qh, ql = halves(q)
         work = []
-        for duo_at in range(rows // duo):
+        for duo_at in range(extent // duo):
             lo = duo_at * duo
             here = slice(lo, lo + duo)
             left = jnp.concatenate(
@@ -730,7 +741,7 @@
             for side in range(2):
                 at = lo + side * span
                 mine = made[side * (width + span) : (side + 1) * (width + span)]
-                n = b * blocks + 2 * duo_at + side
+                n = b * blocks + begin // span + 2 * duo_at + side
                 keep = grow[at + span - 1 : at + span]
                 step_map = jnp.where(diagonal, keep, 0.0) - mine[:width, width:]
                 query = boosted[at : at + span] - mine[width:, width:]
@@ -794,18 +805,21 @@
                     block_came(way, step)
         return b
 
-    def delta_block(b):
-        drows = dot_f32(xs[b], ws[:, 3 * cols :]).astype(jnp.bfloat16).astype(jnp.float32)
-        return prepare(b, drows[:, :cols], drows[:, cols : 2 * cols], drows[:, 2 * cols :])
+    def delta_block(b, begin=0, extent=rows):
+        drows = dot_f32(xs[b, begin : begin + extent, :], ws[:, 3 * cols :])
+        drows = drows.astype(jnp.bfloat16).astype(jnp.float32)
+        return prepare(
+            b, drows[:, :cols], drows[:, cols : 2 * cols], drows[:, 2 * cols :], begin, extent
+        )
 
     last_way = jnp.logical_or(z == 0, z == sp - 1)
     from_top = z == sp - 1
 
-    def stick_project(n):
+    def stick_project(n, begin=0, extent=rows):
         b = jnp.where(from_top, sp - 1 - n, n)
-        out = dot_f32(xs[b], ws[:, : 3 * cols]).astype(jnp.bfloat16)
+        out = dot_f32(xs[b, begin : begin + extent, :], ws[:, : 3 * cols]).astype(jnp.bfloat16)
         for i in range(3):
-            proj[i, at_block(b), :] = out[:, i * cols : (i + 1) * cols]
+            proj[i, at_block(b, begin, extent), :] = out[:, i * cols : (i + 1) * cols]
 
     def stick_place(n):
         lower = z < sp // 2
@@ -911,6 +925,14 @@
                     )
                 )
                 def _():
+                    if part == parts - 1:
+                        for way in range(2):
+                            @pl.when(comes(way, sp - 1))
+                            def _():
+                                half_came(way)
+                        for _ in delta_block(stick_place(sp - 1), 0, rows // 2):
+                            pass
+                        stick_project(sp - 1, 0, rows // 2)
                     arrive(sp - 1, part)
             stick_pair(n, r)
             return c
@@ -929,8 +951,8 @@
             @pl.when(comes(way, sp - 1))
             def _():
                 block_came(way, sp - 1)
-        stick_project(sp - 1)
-        stages = delta_block(stick_place(sp - 1))
+        stick_project(sp - 1, rows // 2, rows // 2)
+        stages = delta_block(stick_place(sp - 1), rows // 2, rows // 2)
         for u in range(sp):
             next(stages, None)
             stick_pair(sp - 1, u)
@@ -1047,7 +1069,7 @@
             pltpu.VMEM(delta_out_w.shape, bf16),
             pltpu.VMEM((rows, width), f32),
             pltpu.VMEM((chunks, share, width // chunks), bf16),
-            dma((2,)), dma((2, sp - 1, parts)), dma((1,)), dma((2 * sp - 1,)),
+            dma((2,)), dma((2, sp - 1, parts)), dma((1,)), dma((2 * sp + 1,)),
             dma((1,)), dma((2, 6)), dma((2,)), dma((2,)), dma((2, sp - 1)), dma((11,)),
             dma((2,)), dma((3,)), dma((2,)),
         ],

time: 57.5 us -> 58.4 us (1.016)
  Pallas kernels: 56.4 us -> 57.3 us
    pallas_call x1, Pallas kernels: 56.4 us -> 57.3 us  [on_device_heads(): pl.pallas_call(layer_kernel, name='layer', out_shape=(pltpu.VMEM((share,...]
where the time goes in v10:
time: 58.4 us; the launch traced here: 58.3 us
  Pallas kernels  57.3 us (98%)
  other arithmetic  0.92 us (2%)
    pallas_call x1, Pallas kernels, on_device_heads(): pl.pallas_call(layer_kernel, name='layer', out_shape=(pltpu.VMEM((share,...  57.3 us

profile of v10, /device:TPU:0, one launch (start us, length us, event | category | flops | bytes accessed | tf_op | source)
XLA Modules:
  0.0 58.3 jit_solution(5127294776908003021)
XLA Ops:
  0.0 57.3 %layer.1 = (bf16[128,2048]{1,0:T(8,128)(2,1)S(1)}, bf16[128,2048]{1,0:T(8,128)(2,1)S(1)}) custom-call(f32[8]{0:T(128)} %offset_hbm.1, f32[4]{0:T(128)} %decay_scale_hbm.1, f32[4]{0:T(128)} %write_bias_hbm.1, bf16[256,1024]{1,0:T(8,128)(2,1)} %bitcast.7, bf16[512,512]{1,0:T(8,128)(2,1)} %w0.1, bf16[512,512]{1,0:T(8,128)(2,1)} %w1.1, bf16[512,512]{1,0:T(8,128)(2,1)} %w2.1, ...), custom_call_target="tpu_custom_call" | custom-call | tf_op jit(solution)/shard_map/layer/pallas_call | solution.py:1040
  57.3 0.9 %fusion = bf16[1,128,2048]{2,1,0:T(8,128)(2,1)} fusion(bf16[128,2048]{1,0:T(8,128)(2,1)S(1)} %get-tuple-element.8, bf16[128,2048]{1,0:T(8,128)(2,1)S(1)} %get-tuple-element.7), kind=kLoop, calls=%fused_computation.1 | loop fusion | flops 1048576 | bytes 1572864 | tf_op jit(solution)/shard_map/reshape | solution.py:1087

commit v11 on v9

--- a/solution.py
+++ b/solution.py
@@ -930,10 +930,13 @@
             def _():
                 block_came(way, sp - 1)
         stick_project(sp - 1)
+        stick_pair(sp - 1, 0)
         stages = delta_block(stick_place(sp - 1))
-        for u in range(sp):
-            next(stages, None)
+        for u in range(1, sp):
+            next(stages)
             stick_pair(sp - 1, u)
+        for _ in stages:
+            pass
         walk_groups(jnp.where(z == 0, sp - 1, 0), sp)
 
     mine_z = pl.ds(pl.multiple_of(z * rows, rows), rows)

time: 57.5 us -> 58.2 us (1.012)
  Pallas kernels: 56.4 us -> 57.1 us
    pallas_call x1, Pallas kernels: 56.4 us -> 57.1 us  [on_device_heads(): pl.pallas_call(layer_kernel, name='layer', out_shape=(pltpu.VMEM((share,...]
where the time goes in v11:
time: 58.2 us; the launch traced here: 58 us
  Pallas kernels  57.1 us (98%)
  other arithmetic  0.92 us (2%)
    pallas_call x1, Pallas kernels, on_device_heads(): pl.pallas_call(layer_kernel, name='layer', out_shape=(pltpu.VMEM((share,...  57.1 us

profile of v11, /device:TPU:0, one launch (start us, length us, event | category | flops | bytes accessed | tf_op | source)
XLA Modules:
  0.0 58.0 jit_solution(3827455506068220918)
XLA Ops:
  0.0 57.1 %layer.1 = (bf16[128,2048]{1,0:T(8,128)(2,1)S(1)}, bf16[128,2048]{1,0:T(8,128)(2,1)S(1)}) custom-call(f32[8]{0:T(128)} %offset_hbm.1, f32[4]{0:T(128)} %decay_scale_hbm.1, f32[4]{0:T(128)} %write_bias_hbm.1, bf16[256,1024]{1,0:T(8,128)(2,1)} %bitcast.7, bf16[512,512]{1,0:T(8,128)(2,1)} %w0.1, bf16[512,512]{1,0:T(8,128)(2,1)} %w1.1, bf16[512,512]{1,0:T(8,128)(2,1)} %w2.1, ...), custom_call_target="tpu_custom_call" | custom-call | tf_op jit(solution)/shard_map/layer/pallas_call | solution.py:1021
  57.1 0.9 %fusion = bf16[1,128,2048]{2,1,0:T(8,128)(2,1)} fusion(bf16[128,2048]{1,0:T(8,128)(2,1)S(1)} %get-tuple-element.8, bf16[128,2048]{1,0:T(8,128)(2,1)S(1)} %get-tuple-element.7), kind=kLoop, calls=%fused_computation.1 | loop fusion | flops 1048576 | bytes 1572864 | tf_op jit(solution)/shard_map/reshape | solution.py:1068

commit v12 on v9

--- a/solution.py
+++ b/solution.py
@@ -582,13 +582,12 @@
                 ],
                 axis=0,
             )
+            seen = across[:tile] < below[:tile] + (part * tile + (i - j) * rows)
+            score = jnp.where(jnp.concatenate([seen] * size, axis=0), score, -1e30)
             skip = jnp.maximum(score, jnp.log(1.0 + jnp.exp(jnp.minimum(score, 80.0))))
             weight = score - skip
-            seen = across[:tile] < below[:tile] + (part * tile + (i - j) * rows)
-            seen = jnp.concatenate([seen] * size, axis=0)
-            skip = jnp.where(seen, skip, 0.0)
             sums = dot_f32(skip.astype(jnp.bfloat16), after[...])
-            weight = jnp.where(seen, jnp.exp(weight - sums[:, :rows]), 0.0)
+            weight = jnp.exp(weight - sums[:, :rows])
             out = dot_f32(weight.astype(jnp.bfloat16), values)
             mixed, total = out[:tile], sums[:tile, rows:]
             for h in range(1, size):
@@ -929,8 +928,14 @@
             @pl.when(comes(way, sp - 1))
             def _():
                 block_came(way, sp - 1)
-        stick_project(sp - 1)
-        stages = delta_block(stick_place(sp - 1))
+        b = stick_place(sp - 1)
+        pieces = []
+        for i in range(0, count, 2):
+            out = dot_f32(xs[b], ws[:, i * cols : (i + 2) * cols]).astype(jnp.bfloat16)
+            pieces += [out[:, :cols], out[:, cols:]]
+        for i in range(3):
+            proj[i, at_block(b), :] = pieces[i]
+        stages = prepare(b, *(piece.astype(jnp.float32) for piece in pieces[3:]))
         for u in range(sp):
             next(stages, None)
             stick_pair(sp - 1, u)

time: 57.5 us -> 57.1 us (level)
  no operation moved by 1% of the time
where the time goes in v12:
time: 57.1 us; the launch traced here: 57 us
  Pallas kernels  56.1 us (98%)
  other arithmetic  0.92 us (2%)
    pallas_call x1, Pallas kernels, on_device_heads(): pl.pallas_call(layer_kernel, name='layer', out_shape=(pltpu.VMEM((share,...  56.1 us

profile of v12, /device:TPU:0, one launch (start us, length us, event | category | flops | bytes accessed | tf_op | source)
XLA Modules:
  0.0 57.0 jit_solution(14353583512352092236)
XLA Ops:
  0.0 56.1 %layer.1 = (bf16[128,2048]{1,0:T(8,128)(2,1)S(1)}, bf16[128,2048]{1,0:T(8,128)(2,1)S(1)}) custom-call(f32[8]{0:T(128)} %offset_hbm.1, f32[4]{0:T(128)} %decay_scale_hbm.1, f32[4]{0:T(128)} %write_bias_hbm.1, bf16[256,1024]{1,0:T(8,128)(2,1)} %bitcast.7, bf16[512,512]{1,0:T(8,128)(2,1)} %w0.1, bf16[512,512]{1,0:T(8,128)(2,1)} %w1.1, bf16[512,512]{1,0:T(8,128)(2,1)} %w2.1, ...), custom_call_target="tpu_custom_call" | custom-call | tf_op jit(solution)/shard_map/layer/pallas_call | solution.py:1023
  56.1 0.9 %fusion = bf16[1,128,2048]{2,1,0:T(8,128)(2,1)} fusion(bf16[128,2048]{1,0:T(8,128)(2,1)S(1)} %get-tuple-element.8, bf16[128,2048]{1,0:T(8,128)(2,1)S(1)} %get-tuple-element.7), kind=kLoop, calls=%fused_computation.1 | loop fusion | flops 1048576 | bytes 1572864 | tf_op jit(solution)/shard_map/reshape | solution.py:1070

commit v13 on v12

--- a/solution.py
+++ b/solution.py
@@ -560,7 +560,7 @@
     size = offset_ref.shape[0] // sp
     sb_size = cols // size
     scale = sb_size ** (-0.5)
-    tile = rows // 2
+    tile = rows
 
     def at_block(b, start=0, extent=rows):
         return pl.ds(pl.multiple_of(b * rows + start, extent), extent)

time: 57.1 us -> 56.6 us (level)
  Pallas kernels: 56.1 us -> 55.5 us
where the time goes in v13:
time: 56.6 us; the launch traced here: 56.4 us
  Pallas kernels  55.5 us (98%)
  other arithmetic  0.92 us (2%)
    pallas_call x1, Pallas kernels, on_device_heads(): pl.pallas_call(layer_kernel, name='layer', out_shape=(pltpu.VMEM((share,...  55.5 us

profile of v13, /device:TPU:0, one launch (start us, length us, event | category | flops | bytes accessed | tf_op | source)
XLA Modules:
  0.0 56.4 jit_solution(7486720231147306384)
XLA Ops:
  0.0 55.5 %layer.1 = (bf16[128,2048]{1,0:T(8,128)(2,1)S(1)}, bf16[128,2048]{1,0:T(8,128)(2,1)S(1)}) custom-call(f32[8]{0:T(128)} %offset_hbm.1, f32[4]{0:T(128)} %decay_scale_hbm.1, f32[4]{0:T(128)} %write_bias_hbm.1, bf16[256,1024]{1,0:T(8,128)(2,1)} %bitcast.7, bf16[512,512]{1,0:T(8,128)(2,1)} %w0.1, bf16[512,512]{1,0:T(8,128)(2,1)} %w1.1, bf16[512,512]{1,0:T(8,128)(2,1)} %w2.1, ...), custom_call_target="tpu_custom_call" | custom-call | tf_op jit(solution)/shard_map/layer/pallas_call | solution.py:1023
  55.5 0.9 %fusion = bf16[1,128,2048]{2,1,0:T(8,128)(2,1)} fusion(bf16[128,2048]{1,0:T(8,128)(2,1)S(1)} %get-tuple-element.8, bf16[128,2048]{1,0:T(8,128)(2,1)S(1)} %get-tuple-element.7), kind=kLoop, calls=%fused_computation.1 | loop fusion | flops 1048576 | bytes 1572864 | tf_op jit(solution)/shard_map/reshape | solution.py:1070
